TPU v7x, 128 devices: a whole 4x4x4 slice. The times are simulated.
128 devices in a mesh: sp: 16 (over z, y), fs: 4 (over x), tp: 2 (over core).
Axes of the slice: x: 4, y: 4, z: 4, core: 2. Of those that a mesh axis runs over, the one named last changes fastest.
Arguments:
- tokens: bfloat16 [4, 6144, 2048], P('fs', 'sp', 'tp'), may hold values from -6 to 6
- in_gain: float32 [2048], replicated, may hold values from 0.1 to 1.9
- w_query: bfloat16 [2048, 1024], P('fs', 'tp'), may hold values from -0.125 to 0.125
- w_key: bfloat16 [2048, 1024], P('fs', 'tp'), may hold values from -0.125 to 0.125
- w_value: bfloat16 [2048, 1024], P('fs', 'tp'), may hold values from -0.125 to 0.125
- w_outgate: bfloat16 [2048, 1024], P('fs', 'tp'), may hold values from -0.125 to 0.125
- w_ingate: bfloat16 [2048, 1024], P('fs', 'tp'), may hold values from -0.125 to 0.125
- w_conv_in: bfloat16 [2048, 1024], P('fs', 'tp'), may hold values from -0.125 to 0.125
- score_offset: float32 [16], P('tp'), may hold values from 3.5 to 12
- conv_taps: float32 [3, 1024], P(None, 'tp'), may hold values from -3.5 to 3.5
- att_gain: float32 [1024], P('tp'), may hold values from 0.1 to 1.9
- conv_gain: float32 [1024], P('tp'), may hold values from 0.1 to 1.9
- out_att: bfloat16 [1024, 2048], P('tp'), may hold values from -0.125 to 0.125
- out_conv: bfloat16 [1024, 2048], P('tp'), may hold values from -0.125 to 0.125
Outputs:
- mixed: bfloat16 [4, 6144, 2048], P('fs', ('sp', 'tp'))
- log_mass: float32 [4, 6144, 16], P('fs', 'sp', 'tp')
All inputs are finite; a program needn't handle non-finite values.
Results may differ from a plain program's by a relative error of at most 0.012.
Values may be sent and summed in bfloat16 or wider, within the bound.
A program may use at most 128 MiB of HBM per device.

v0:
```python
import jax
import jax.numpy as jnp
from jax import lax
from jax.sharding import PartitionSpec as P

D = 2048
CONV_CH = 1024
ATT_WIDTH = 1024


epsilon = 1e-06


def sent_together(arrays, axis, dim, along):
    ends, at = ([], 0)
    for a in arrays[:-1]:
        at += a.shape[along]
        ends.append(at)
    both = jnp.concatenate(arrays, axis=along)
    return tuple(jnp.split(lax.all_gather(both, axis, axis=dim, tiled=True), ends, axis=along))


def in_order(blocks, dim):
    blocks = jnp.moveaxis(blocks, 0, dim)
    shape = blocks.shape
    return blocks.reshape(*shape[:dim], shape[dim] * shape[dim + 1], *shape[dim + 2 :])


def from_everyone(shard, axis):
    devices = lax.axis_size(axis)
    return lax.all_to_all(
        jnp.broadcast_to(shard[None], (devices, *shard.shape)), axis, 0, 0, tiled=True
    )


def gather_directly(shard, axis, dim):
    return in_order(from_everyone(shard, axis), dim)


def passed_along(shard, axis, by):
    devices = lax.axis_size(axis)
    pairs = [(i, i + by) for i in range(devices) if 0 <= i + by < devices]
    return lax.ppermute(shard, axis, pairs)


def visit(carry, queries, key_block, value_block, offsets, validity):
    attended, weight_sum, kept_log = carry
    heads = offsets.shape[0]
    key_heads = key_block.reshape(key_block.shape[0], heads, -1)
    value_heads = value_block.reshape(value_block.shape[0], heads, -1)
    scores = jnp.einsum("qhd,khd->hqk", queries, key_heads, preferred_element_type=jnp.float32)
    scores = scores * queries.shape[2] ** (-0.5) - offsets[:, None, None]
    log_keep = jnp.where(validity, -jax.nn.softplus(scores), 0.0)
    later = lax.cumsum(log_keep, axis=2, reverse=True) - log_keep
    log_weight = -jax.nn.softplus(-scores) + later + kept_log[:, :, None]
    weights = jnp.where(validity, jnp.exp(log_weight), 0.0)
    attended = attended + jnp.einsum(
        "hqk,khd->qhd",
        weights.astype(jnp.bfloat16),
        value_heads,
        preferred_element_type=jnp.float32,
    )
    return (attended, weight_sum + jnp.sum(weights, axis=2), kept_log + jnp.sum(log_keep, axis=2))


def per_device(
    tokens,
    in_gain,
    w_query,
    w_key,
    w_value,
    w_outgate,
    w_ingate,
    w_conv_in,
    score_offset,
    conv_taps,
    att_gain,
    conv_gain,
    out_att,
    out_conv,
):
    local_rows = tokens[0]
    length = local_rows.shape[0]
    matrices = sent_together((w_query, w_key, w_value, w_outgate, w_ingate, w_conv_in), "fs", 0, 1)
    widened = gather_directly(local_rows, "tp", 1).astype(jnp.float32)
    scaled = (widened * in_gain).astype(jnp.bfloat16)
    totals = tuple(
        (jnp.dot(scaled, matrix, preferred_element_type=jnp.float32) for matrix in matrices)
    )
    totals, squares = (totals, jnp.sum(widened * widened, axis=1))
    in_scale = lax.rsqrt(squares / D + epsilon)
    query, key_rows, value_rows, outgate, ingate, conv_input = [
        (total * in_scale[:, None]).astype(jnp.bfloat16) for total in totals
    ]
    heads = score_offset.shape[0]
    queries = query.reshape(length, heads, -1)
    head_size = queries.shape[2]
    positions = lax.iota(jnp.int32, length)
    causal = positions[None, :] < positions[:, None]
    empty = (
        jnp.zeros((length, heads, head_size), jnp.float32),
        jnp.zeros((heads, length), jnp.float32),
        jnp.zeros((heads, length), jnp.float32),
    )
    carry = visit(empty, queries, key_rows, value_rows, score_offset, causal)
    pairs = jnp.stack((key_rows, value_rows))
    ranking = lax.axis_index("sp")
    every = jnp.ones((1, 1, 1), jnp.bool_)
    gathered = lax.all_gather(pairs, "sp", axis=1, tiled=True)

    def advance(section, inner):
        source = ranking - section
        block = lax.dynamic_slice_in_dim(gathered, source * length, length, 1)
        return visit(inner, queries, block[0], block[1], score_offset, every)

    carry = lax.fori_loop(1, ranking + 1, advance, carry)
    attended, weight_sum, kept_log = carry
    log_mass = jnp.log(1.0 + weight_sum).T[None]
    attention = attended.reshape(length, -1)
    taps = conv_taps.shape[0]
    gated_input = ingate.astype(jnp.float32) * conv_input.astype(jnp.float32)
    before = passed_along(gated_input[length - (taps - 1) :], "sp", 1)
    extended = jnp.concatenate((before, gated_input), axis=0)
    convolved = sum(
        (
            conv_taps[tap_index] * extended[tap_index : tap_index + length]
            for tap_index in range(taps)
        )
    )
    conv_out = outgate.astype(jnp.float32) * convolved
    branch_sums = lax.psum(
        (jnp.sum(attention * attention, axis=1), jnp.sum(conv_out * conv_out, axis=1)), "tp"
    )
    att_scale = lax.rsqrt(branch_sums[0] / ATT_WIDTH + epsilon)
    conv_scale = lax.rsqrt(branch_sums[1] / CONV_CH + epsilon)
    att_scaled = (attention * att_gain).astype(jnp.bfloat16)
    conv_scaled = (conv_out * conv_gain).astype(jnp.bfloat16)
    share = length // lax.axis_size("tp")
    both_parts = lax.psum_scatter(
        jnp.concatenate(
            (
                jnp.dot(att_scaled, out_att, preferred_element_type=jnp.float32),
                jnp.dot(conv_scaled, out_conv, preferred_element_type=jnp.float32),
            ),
            axis=1,
        ),
        "tp",
        scatter_dimension=0,
        tiled=True,
    )
    first_row = lax.axis_index("tp") * share
    att_mine = lax.dynamic_slice_in_dim(att_scale, first_row, share, 0)
    conv_mine = lax.dynamic_slice_in_dim(conv_scale, first_row, share, 0)
    width = out_att.shape[1]
    mixed = att_mine[:, None] * both_parts[:, :width] + conv_mine[:, None] * both_parts[:, width:]
    return (mixed.astype(jnp.bfloat16)[None], log_mass)


def solution(mesh):
    return jax.shard_map(
        per_device,
        mesh=mesh,
        in_specs=(
            P("fs", "sp", "tp"),
            P(),
            P("fs", "tp"),
            P("fs", "tp"),
            P("fs", "tp"),
            P("fs", "tp"),
            P("fs", "tp"),
            P("fs", "tp"),
            P("tp"),
            P(None, "tp"),
            P("tp"),
            P("tp"),
            P("tp", None),
            P("tp", None),
        ),
        out_specs=(P("fs", ("sp", "tp"), None), P("fs", "sp", "tp")),
        check_vma=False,
    )
```

profile of v0, /device:TPU:1, one launch (start us, length us, event | category | flops | bytes accessed | tf_op | source)
XLA Modules:
  0.0 658.4 jit_solution(15294109769012042955)
XLA Ops:
  7.2 0.0 all-gather.3.cloned.1.call-start
  7.2 2.1 constant_dynamic-update-slice_fusion.5
  9.3 1.9 constant_dynamic-update-slice_fusion.4
  11.2 1.9 constant_dynamic-update-slice_fusion.3
  13.2 1.9 constant_dynamic-update-slice_fusion.2
  15.1 1.9 constant_dynamic-update-slice_fusion.1
  17.0 0.8 constant_dynamic-update-slice_fusion
  17.9 0.0 all-gather.5.cloned.1.call-start
  18.0 1.5 copy.30
  19.5 0.1 broadcast_in_dim.33
  19.6 6.0 all_to_all.5
  25.6 0.4 multiply_reduce_fusion
  26.0 1.6 fusion.27
  27.6 112.0 %all-gather.3.cloned.1.call-done = bf16[2048,3072]{1,0:T(8,128)(2,1)} async-done(((bf16[512,3072]{1,0:T(8,128)(2,1)}), bf16[2048,3072]{1,0:T(8,128)(2,1)}) %all-gather.3.cloned.1.call-update) | async-done | bytes 12582928 | tf_op jit(solution)/shard_map/all_gather | solution.py:20
  139.6 3.2 fusion.92
  142.8 2.6 fusion.86
  145.4 1.0 pad_maximum_fusion.2
  146.4 0.0 all-gather.5.cloned.1.call-update
  146.4 0.0 reduce-scatter.2.cloned.1.call-start
  146.5 0.2 copy.31
  146.8 0.9 copy.33
  147.7 3.2 fusion.77
  150.9 2.6 fusion.71
  153.5 3.1 collective-permute-start
  156.7 3.5 fusion.89
  160.2 1.9 copy.32
  162.1 2.7 fusion.95
  164.9 3.5 fusion.111
  168.4 11.5 %fusion.25 = f32[8,384,3,128]{1,0,3,2:T(8,128)S(1)} fusion(f32[8,384,3,128]{1,3,2,0:T(8,128)S(1)} %bitcast.115), kind=kOutput, calls=%fused_computation.38 | output fusion | flops 149815296 | bytes 9437184 | tf_op jit(solution)/shard_map/reduce-window.2
  179.9 0.2 fusion.108
  180.1 0.3 broadcast_add_fusion.1
  180.4 0.9 copy.35
  181.4 4.3 fusion.112
  185.7 0.5 fusion.44
  186.3 2.9 multiply_reduce_fusion.1
  189.1 2.7 fusion.104
  191.8 45.7 %all-gather.5.cloned.1.call-done = bf16[2,6144,512]{2,1,0:T(8,128)(2,1)} async-done(((bf16[2,384,512]{2,1,0:T(8,128)(2,1)}), bf16[2,6144,512]{2,1,0:T(8,128)(2,1)}) %all-gather.5.cloned.1.call-update) | async-done | bytes 12582928 | tf_op jit(solution)/shard_map/all_gather | solution.py:109
  237.5 0.7 copy-done.14
  238.1 0.1 fusion.103
  238.3 2.7 fusion.115
  241.0 3.1 pad_maximum_fusion
  244.1 0.1 multiply_reduce_fusion.2
  244.2 3.1 all-reduce
  247.3 0.1 dynamic_slice.10
  247.4 0.1 dynamic_slice.9
  247.5 0.6 log_bitcast_fusion
  248.1 400.8 %reduce-scatter.2.cloned.1.call-done = f32[192,4096]{1,0:T(8,128)} async-done(((f32[384,4096]{1,0:T(8,128)}), f32[192,4096]{1,0:T(8,128)}) %reduce-scatter.2.cloned.1.call-update) | async-done | bytes 3145744 | tf_op jit(solution)/shard_map/reduce_scatter | solution.py:139
  648.9 3.0 fusion.101
  (39 shorter events, 0.2 us)
Async XLA Ops:
  7.2 182.0 %copy-start = (bf16[512,2048]{1,0:T(8,128)(2,1)S(1)}, bf16[512,2048]{1,0:T(8,128)(2,1)}, u32[]{:S(2)}) copy-start(bf16[512,2048]{1,0:T(8,128)(2,1)} %param.29) | copy-start | bytes 6291460
  7.2 9.8 %copy-start.8 = (bf16[512,512]{1,0:T(8,128)(2,1)S(1)}, bf16[512,512]{1,0:T(8,128)(2,1)}, u32[]{:S(2)}) copy-start(bf16[512,512]{1,0:T(8,128)(2,1)} %param.23) | copy-start | bytes 1572868
  7.2 132.4 %all-gather.3.cloned.1.call-start = ((), (), s32[]{:S(2)}) async-start(), calls=%async_computation.2 | async-start | bytes 15728640 | tf_op jit(solution)/shard_map/all_gather | solution.py:20
  17.9 8.1 %copy-start.11 = (f32[2048]{0:T(1024)S(1)}, f32[2048]{0:T(1024)}, u32[]{:S(2)}) copy-start(f32[2048]{0:T(1024)} %param.17) | copy-start | bytes 24580
  17.9 219.5 %all-gather.5.cloned.1.call-start = ((), (), s32[]{:S(2)}) async-start(), calls=%async_computation.3 | async-start | bytes 13369344 | tf_op jit(solution)/shard_map/all_gather | solution.py:109
  139.6 3.2 copy-start.3
  142.8 3.7 copy-start.13
  146.4 502.5 %reduce-scatter.2.cloned.1.call-start = ((), (), s32[]{:S(2)}) async-start(), calls=%async_computation.4 | async-start | bytes 9437184 | tf_op jit(solution)/shard_map/reduce_scatter | solution.py:139
  147.7 3.2 copy-start.4
  150.9 11.2 %copy-start.10 = (f32[8]{0:T(128)S(1)}, f32[8]{0:T(128)}, u32[]{:S(2)}) copy-start(f32[8]{0:T(128)} %param.24) | copy-start | bytes 100
  153.5 11.3 %copy-start.6 = (f32[384,512]{1,0:T(8,128)}, f32[384,512]{1,0:T(8,128)S(1)}, u32[]{:S(2)}) copy-start(f32[384,512]{1,0:T(8,128)S(1)} %fusion.71) | copy-start | bytes 2359300
  153.5 32.7 %collective-permute-start = (f32[2,512]{1,0:T(2,128)S(1)}, f32[2,512]{1,0:T(2,128)S(1)}, u32[]{:S(2)}, u32[]{:S(2)}) collective-permute-start(f32[2,512]{1,0:T(2,128)S(1)} %slice.56), channel_id=1, source_target_pairs={{0,8},{8,16},{16,24},{24,32},{32,40},{40,48},{48,56},{56,64},{64,7... | collective-permute-start | bytes 12296 | tf_op jit(solution)/shard_map/ppermute | solution.py:43
  181.3 4.9 copy-start.5
  181.4 4.9 copy-start.7
  185.7 3.4 copy-start.12
  189.1 48.4 %copy-start.9 = (bf16[384,512]{0,1:T(8,128)(2,1)S(1)}, bf16[384,512]{0,1:T(8,128)(2,1)}, u32[]{:S(2)}) copy-start(bf16[384,512]{0,1:T(8,128)(2,1)} %copy.32) | copy-start | bytes 1179652
  237.5 0.7 copy-start.14
  237.5 3.6 copy-start.2
  244.1 407.8 %copy-start.1 = (bf16[512,2048]{1,0:T(8,128)(2,1)S(1)}, bf16[512,2048]{1,0:T(8,128)(2,1)}, u32[]{:S(2)}) copy-start(bf16[512,2048]{1,0:T(8,128)(2,1)} %param.29) | copy-start | bytes 6291460
Sparse Core Ops, SparseCore 0:
  18.0 121.5 all-gather.2
  146.5 90.8 all-gather.4
  244.2 404.6 reduce-scatter.1
where the time goes:
time: 659 us; the launch traced here: 658 us
  waiting for transfers between devices  559 us (85%)
  other arithmetic  29.8 us (5%)
  matrix products  26.6 us (4%)
  local copies, waits for them, and re-layouts  17.2 us (3%)
  between operations  14.1 us (2%)
  blocking collectives  9.09 us (1%)
    reduce_scatter x1, waiting for transfers between devices, per_device(): lax.psum_scatter(jnp.concatenate((jnp.dot(att_scaled, out_att, preferred_...  401 us
    all_gather x1, waiting for transfers between devices, sent_together(): lax.all_gather(both, axis, axis=dim, tiled=True)  112 us
    all_gather x1, waiting for transfers between devices, per_device(): gathered = lax.all_gather(pairs, 'sp', axis=1, tiled=True)  45.7 us
    dot_general x6, matrix products, per_device(): jnp.dot(scaled, matrix, preferred_element_type=jnp.float32)  18 us
  transfers between devices with their start and end apart: 4, of which 3 were waited for; matrix products, arithmetic and copies ran while one was open for 7% of the time, Pallas kernels for 0%

commit v1 on v0

v1 whole, which is shorter than its diff:
```python
import functools

import jax
import jax.numpy as jnp
from jax import lax
from jax.experimental import pallas as pl
from jax.experimental.pallas import tpu as pltpu
from jax.sharding import PartitionSpec as P

D = 2048
CONV_CH = 1024
ATT_WIDTH = 1024
SEQS = 4
ROWS = 384
HALF = 192
BLOCKS = 16
HD = 64
MESSAGE = ROWS + HALF // 2
epsilon = 1e-06
LOG2E = 1.4426950408889634
F32 = jnp.float32
BF16 = jnp.bfloat16


def dot(a, b):
    return jnp.dot(a, b, preferred_element_type=F32)


def dot_nt(a, b):
    return lax.dot_general(a, b, (((1,), (1,)), ((), ())), preferred_element_type=F32)


def three_parts(x):
    a = x.astype(BF16)
    rest = x - a.astype(F32)
    b = rest.astype(BF16)
    return a, b, (rest - b.astype(F32)).astype(BF16)


def project_kernel(tok_ref, gain_ref, w_ref, msg_ref, gated_ref, outgate_ref):
    flip = lax.rem(lax.axis_index("sp"), 2)
    low = tok_ref[0, 0].astype(F32)
    high = tok_ref[0, 1].astype(F32)
    squares = jnp.sum(low * low, axis=1, keepdims=True) + jnp.sum(high * high, axis=1, keepdims=True)
    scale = lax.rsqrt(squares / D + epsilon)
    total = dot((low * gain_ref[0:1, :]).astype(BF16), w_ref[0:1024, :]) + dot(
        (high * gain_ref[1:2, :]).astype(BF16), w_ref[1024:2048, :]
    )
    out = (total * scale).astype(BF16)
    query, key, value = out[:, 0:128], out[:, 128:256], out[:, 256:384]
    for head in range(2):
        mine = slice(head * HD, (head + 1) * HD)
        pair = jnp.concatenate((key[:, mine], value[:, mine]), axis=1)
        for half in range(2):
            msg_ref[2 * head + half, 0:ROWS, :] = pair
        halves = [
            jnp.concatenate(
                (query[i * HALF : i * HALF + 96, mine], query[i * HALF + 96 : (i + 1) * HALF, mine]),
                axis=1,
            )
            for i in range(2)
        ]

        @pl.when(flip == 0)
        def _():
            msg_ref[2 * head, ROWS:MESSAGE, :] = halves[0]
            msg_ref[2 * head + 1, ROWS:MESSAGE, :] = halves[1]

        @pl.when(flip == 1)
        def _():
            msg_ref[2 * head, ROWS:MESSAGE, :] = halves[1]
            msg_ref[2 * head + 1, ROWS:MESSAGE, :] = halves[0]

    outgate_ref[0] = out[:, 384:512]
    gated_ref[0] = out[:, 512:640].astype(F32) * out[:, 640:768].astype(F32)


def project(tok, gains, weights):
    return pl.pallas_call(
        project_kernel,
        grid=(SEQS,),
        in_specs=[
            pl.BlockSpec((1, 2, ROWS, 1024), lambda s: (s, 0, 0, 0)),
            pl.BlockSpec((2, 1024), lambda s: (0, 0)),
            pl.BlockSpec((D, 768), lambda s: (0, 0)),
        ],
        out_specs=[
            pl.BlockSpec((4, MESSAGE, 128), lambda s: (s, 0, 0)),
            pl.BlockSpec((1, ROWS, 128), lambda s: (s, 0, 0)),
            pl.BlockSpec((1, ROWS, 128), lambda s: (s, 0, 0)),
        ],
        out_shape=[
            jax.ShapeDtypeStruct((16, MESSAGE, 128), BF16),
            jax.ShapeDtypeStruct((SEQS, ROWS, 128), F32),
            jax.ShapeDtypeStruct((SEQS, ROWS, 128), BF16),
        ],
        compiler_params=pltpu.CompilerParams(vmem_limit_bytes=48 << 20),
        cost_estimate=pl.CostEstimate(flops=4_800_000_000, bytes_accessed=13_000_000, transcendentals=0),
        name="project",
    )(tok, gains, weights)


def attend_kernel(
    offset_ref, gain_ref, recv_ref, out_ref, keys, values, queries, scores, decays, weights, total
):
    place = lax.axis_index("sp")
    half = lax.rem(place, 2)
    head = 2 * lax.axis_index("fs") + lax.rem(place // 2, 2)
    lanes = lambda shape: lax.broadcasted_iota(jnp.int32, shape, 1)
    rows = lambda shape: lax.broadcasted_iota(jnp.int32, shape, 0)
    offset = jnp.full((HALF, 128), offset_ref[head] * LOG2E, F32)
    o1, o2, o3 = (part.astype(F32) for part in three_parts(offset))
    lane_q = lanes((HALF, 128))
    offset_row = jnp.where(
        lane_q == 0, -o1, jnp.where(lane_q == 1, -o2, jnp.where(lane_q == 2, -o3, 0.0))
    ).astype(BF16)
    square = (ROWS, ROWS)
    permute = (
        (lanes(square) == lax.rem(rows(square), 8) * 48 + rows(square) // 8).astype(F32).astype(BF16)
    )
    shape = (128, 128)
    twice_low = (rows(shape) == lax.rem(lanes(shape), HD)).astype(F32).astype(BF16)
    twice_high = (rows(shape) == lax.rem(lanes(shape), HD) + HD).astype(F32).astype(BF16)
    take_high = (lanes((HD, 128)) == rows((HD, 128)) + HD).astype(F32).astype(BF16)
    ones = (lanes((ROWS, 128)) < 3).astype(F32).astype(BF16)
    for block in range(BLOCKS):
        pair = dot(permute, recv_ref[block, 0:ROWS, :]).astype(BF16)
        keys[block * ROWS : (block + 1) * ROWS, 0:128] = dot(pair, twice_low).astype(BF16)
        keys[block * ROWS : (block + 1) * ROWS, 128:256] = ones
        values[block] = dot_nt(take_high, pair).astype(BF16)
        packed = recv_ref[block, ROWS:MESSAGE, :]
        q = jnp.concatenate((dot(packed, twice_low), dot(packed, twice_high)), axis=0) * (LOG2E / 8)
        q_high = q.astype(BF16).astype(F32)
        at = slice((block % 2) * HALF, (block % 2 + 1) * HALF)
        queries[block // 2, at, 0:128] = jnp.where(lane_q < HD, q_high, q - q_high).astype(BF16)
        queries[block // 2, at, 128:256] = offset_row

    sub = rows((8, ROWS))
    lane = lanes((8, ROWS))
    where_q = lane + jnp.where(half == 1, HALF, jnp.where(lane < HALF, 0, ROWS))

    def tile(tile_index, block, carry, ahead, slot):
        begin = pl.multiple_of(block * ROWS, ROWS)
        z_ref, d_ref, w_ref = scores.at[slot], decays.at[slot], weights.at[slot]
        z_ref[...] = dot_nt(keys[pl.ds(begin, ROWS), :], queries[tile_index])
        run = jnp.zeros((8, ROWS), F32)
        for r in reversed(range(48)):
            z = z_ref[8 * r : 8 * r + 8, :]
            soft = jnp.maximum(z, jnp.log2(1.0 + jnp.exp2(jnp.minimum(z, 126.0))))
            if ahead is not None:
                valid = ahead > r
                soft = jnp.where(valid, soft, 0.0)
            run = run + soft
            decay = jnp.exp2(z - run)
            if ahead is not None:
                decay = jnp.where(valid, decay, 0.0)
            d_ref[8 * r : 8 * r + 8, :] = decay
        suffix = run
        for step in (1, 2, 4):
            moved = pltpu.roll(suffix, 8 - step, 0)
            suffix = suffix + jnp.where(sub < 8 - step, moved, 0.0)
        after = jnp.where(sub < 7, pltpu.roll(suffix, 7, 0), 0.0)
        kept = jnp.exp2(-(carry + after))
        for i in range(24):
            both = jnp.concatenate(
                (d_ref[16 * i : 16 * i + 8, :] * kept, d_ref[16 * i + 8 : 16 * i + 16, :] * kept), axis=0
            )
            w_ref[16 * i : 16 * i + 16, :] = both.astype(BF16)
        total[...] += dot(values[block], w_ref[...])
        return carry + jnp.broadcast_to(suffix[0:1], (8, ROWS))

    gain = gain_ref[...]
    gain_lane = lanes((8, 512))
    out_lane = lanes((ROWS, 128))

    def one_tile(m, _):
        total[...] = jnp.zeros_like(total)
        carry = jnp.zeros((8, ROWS), F32)
        carry = tile(m, 2 * m + 1, carry, where_q - ROWS - 48 * sub, 0)
        carry = tile(m, 2 * m, carry, where_q - 48 * sub, 1)

        def before(i, carry):
            at = 2 * (m - 1 - i)
            carry = tile(m, at + 1, carry, None, 0)
            return tile(m, at, carry, None, 1)

        carry = lax.fori_loop(0, m, before, carry)
        attended = total[...]
        squares = jnp.sum(attended * attended, axis=0, keepdims=True)
        parts = [p.astype(F32) for p in three_parts(carry[0:1]) + three_parts(squares)]
        side = jnp.concatenate(parts + [jnp.zeros((HD - 6, ROWS), F32)], axis=0)
        message = jnp.concatenate((attended, side), axis=0).T
        message = message * jnp.where(out_lane < HD, gain, 1.0)
        message = message.astype(BF16)
        out_ref[2 * m] = message[0:HALF]
        out_ref[2 * m + 1] = message[HALF:ROWS]
        return 0

    lax.fori_loop(0, BLOCKS // 2, one_tile, 0)


def attend(recv, offsets, gain):
    whole = pl.BlockSpec(memory_space=pltpu.VMEM)
    return pl.pallas_call(
        attend_kernel,
        in_specs=[pl.BlockSpec(memory_space=pltpu.SMEM), whole, whole],
        out_specs=whole,
        out_shape=jax.ShapeDtypeStruct((BLOCKS, HALF, 128), BF16),
        scratch_shapes=[
            pltpu.VMEM((BLOCKS * ROWS, 256), BF16),
            pltpu.VMEM((BLOCKS, HD, ROWS), BF16),
            pltpu.VMEM((BLOCKS // 2, ROWS, 256), BF16),
            pltpu.VMEM((2, ROWS, ROWS), F32),
            pltpu.VMEM((2, ROWS, ROWS), F32),
            pltpu.VMEM((2, ROWS, ROWS), BF16),
            pltpu.VMEM((HD, ROWS), F32),
        ],
        compiler_params=pltpu.CompilerParams(vmem_limit_bytes=48 << 20),
        cost_estimate=pl.CostEstimate(
            flops=10_000_000_000, bytes_accessed=3_000_000, transcendentals=30_000_000
        ),
        name="attend",
    )(offsets, gain, recv)


def per_device(
    tokens,
    in_gain,
    w_query,
    w_key,
    w_value,
    w_outgate,
    w_ingate,
    w_conv_in,
    score_offset,
    conv_taps,
    att_gain,
    conv_gain,
    out_att,
    out_conv,
):
    place = lax.axis_index("sp")
    column = lax.axis_index("fs")
    core = lax.axis_index("tp")
    tok = lax.all_gather(tokens[0], ("fs", "tp")).reshape(SEQS, 2, ROWS, 1024)
    mats = [
        w.reshape(512, 4, 128) for w in (w_query, w_key, w_value, w_outgate, w_ingate, w_conv_in)
    ]
    spread = jnp.moveaxis(jnp.stack(mats, axis=2), 1, 0).reshape(4, 512, 768)
    mine = lax.all_to_all(spread, "fs", 0, 0, tiled=True).reshape(D, 768)
    messages, gated, outgate = project(tok, in_gain.reshape(2, 1024), mine)

    recv = lax.all_to_all(messages, "sp", 0, 0, tiled=True)
    head = 2 * column + lax.rem(place // 2, 2)
    gain = lax.dynamic_slice_in_dim(att_gain, head * HD, HD, 0)
    gain = jnp.concatenate((gain, jnp.ones((HD,), F32)))[None]
    sent = attend(recv, score_offset, gain)
    back = lax.all_to_all(sent, "sp", 0, 0, tiled=True)

    pairs = [(i, i + 1) for i in range(BLOCKS - 1)]
    before = lax.ppermute(gated[:, ROWS - 2 :], "sp", pairs)
    extended = jnp.concatenate((before, gated), axis=1)
    taps = lax.dynamic_slice_in_dim(conv_taps, column * 128, 128, 1)
    convolved = sum(taps[j] * extended[:, j : j + ROWS] for j in range(3))
    conv_out = outgate.astype(F32) * convolved
    conv_squares = jnp.sum(conv_out * conv_out, axis=2)
    conv_mine = lax.dynamic_slice_in_dim(conv_gain, column * 128, 128, 0)
    conv_scaled = (conv_out * conv_mine).astype(BF16)

    att = back.reshape(SEQS, 2, 2, HALF, 128)
    att = jnp.where(lax.rem(place, 2) == 0, att, att[:, :, ::-1])
    pieces = jnp.stack(three_parts(conv_squares), axis=-1).reshape(SEQS, 2, HALF, 3)
    other = att[:, :, ::-1, :, HD : HD + 3]
    both = jnp.concatenate((att[:, 0, :, :, :HD], att[:, 1, :, :, :HD]), axis=-1)
    side = jnp.concatenate(
        [att[:, 0, :, :, HD : HD + 6], att[:, 1, :, :, HD : HD + 6]]
        + [other[:, 0], other[:, 1], pieces, jnp.zeros((SEQS, 2, HALF, 128 - 21), BF16)],
        axis=-1,
    )
    outbound = jnp.stack((both, conv_scaled.reshape(SEQS, 2, HALF, 128), side), axis=2)
    home = lax.all_to_all(outbound.reshape(8, 3, HALF, 128), ("fs", "tp"), 0, 0, tiled=True)
    home = home.reshape(4, 2, 3, HALF, 128)

    wide = lambda a: a.transpose(2, 1, 0, 3).reshape(HALF, 1024)
    att_mat, conv_mat = wide(home[:, :, 0]), wide(home[:, :, 1])
    extra = home[:, :, 2].astype(F32)
    joined = lambda at: extra[..., at] + extra[..., at + 1] + extra[..., at + 2]
    att_sum = jnp.sum(joined(3) + joined(9), axis=(0, 1))
    conv_sum = jnp.sum(joined(18), axis=(0, 1))
    att_scale = lax.rsqrt(att_sum / ATT_WIDTH + epsilon)
    conv_scale = lax.rsqrt(conv_sum / CONV_CH + epsilon)
    out_weights = lax.all_gather(jnp.stack((out_att, out_conv)), "tp", axis=1, tiled=True)
    mixed = att_scale[:, None] * dot(att_mat, out_weights[0]) + conv_scale[:, None] * dot(
        conv_mat, out_weights[1]
    )

    here = lax.dynamic_index_in_dim(extra, core, 1, keepdims=False)
    pick = lambda at: here[..., at] + here[..., at + 1] + here[..., at + 2]
    own = jnp.stack((pick(0), pick(6)), axis=1).reshape(8, HALF)
    far = jnp.stack((pick(12), pick(15)), axis=1).reshape(8, HALF)
    decayed = jnp.where(
        core == 0, jnp.concatenate((own, far), axis=1), jnp.concatenate((far, own), axis=1)
    )
    log_mass = jnp.log(2.0 - jnp.exp2(-decayed)).T
    return (mixed.astype(BF16)[None], log_mass[None])


def solution(mesh):
    return jax.shard_map(
        per_device,
        mesh=mesh,
        in_specs=(
            P("fs", "sp", "tp"),
            P(),
            P("fs", "tp"),
            P("fs", "tp"),
            P("fs", "tp"),
            P("fs", "tp"),
            P("fs", "tp"),
            P("fs", "tp"),
            P("tp"),
            P(None, "tp"),
            P("tp"),
            P("tp"),
            P("tp", None),
            P("tp", None),
        ),
        out_specs=(P("fs", ("sp", "tp"), None), P("fs", "sp", "tp")),
        check_vma=False,
    )
```

time: 659 us -> 248 us (0.38)
  waiting for transfers between devices: 559 us -> 108 us
  Pallas kernels: 0 us -> 55.9 us
  starting transfers between devices: 3.23 us -> 25.9 us
  matrix products: 26.6 us -> 7.32 us
  other arithmetic: 29.8 us -> 13.9 us
  blocking collectives: 9.09 us -> 0 us
    reduce_scatter x1 -> x0, waiting for transfers between devices: 401 us -> none  [per_device(): lax.psum_scatter(jnp.concatenate((jnp.dot(att_scaled, out_att, preferred_...]
    all_gather x2, waiting for transfers between devices: 158 us -> 0.02 us  [the longest x1 0.02 us: per_device(): lax.all_gather(jnp.stack((out_att, out_conv)), 'tp', axis=1, tiled=True)]
    all_to_all x0 -> x4, waiting for transfers between devices: none -> 107 us  [the longest x1 56.9 us: per_device(): mine = lax.all_to_all(spread, 'fs', 0, 0, tiled=True).reshape(D, 768)]
    pallas_call x0 -> x2, Pallas kernels: none -> 55.9 us  [the longest x1 46.2 us: attend(): pl.pallas_call(attend_kernel, in_specs=[pl.BlockSpec(memory_space=pltpu.S...]
    all_to_all x0 -> x4, starting transfers between devices: none -> 22.6 us  [the longest x1 7.15 us: per_device(): recv = lax.all_to_all(messages, 'sp', 0, 0, tiled=True)]
    dot_general x10 -> x2, matrix products: 26.6 us -> 7.32 us  [dot(): return jnp.dot(a, b, preferred_element_type=F32)]
  transfers between devices with their start and end apart: 4 -> 7, of which waited for: 3 -> 4; matrix products, arithmetic and copies ran while one was open for 7% -> 13% of each run, Pallas kernels for 0% -> 23%
where the time goes in v1:
time: 248 us
  waiting for transfers between devices  108 us (44%)
  Pallas kernels  55.9 us (23%)
  starting transfers between devices  25.9 us (10%)
  local copies, waits for them, and re-layouts  22.2 us (9%)
  between operations  14.4 us (6%)
  other arithmetic  13.9 us (6%)
  matrix products  7.32 us (3%)
    all_to_all x1, waiting for transfers between devices, per_device(): mine = lax.all_to_all(spread, 'fs', 0, 0, tiled=True).reshape(D, 768)  56.9 us
    pallas_call x1, Pallas kernels, attend(): pl.pallas_call(attend_kernel, in_specs=[pl.BlockSpec(memory_space=pltpu.S...  46.2 us
    all_to_all x1, waiting for transfers between devices, per_device(): recv = lax.all_to_all(messages, 'sp', 0, 0, tiled=True)  24 us
    all_to_all x1, waiting for transfers between devices, per_device(): lax.all_to_all(outbound.reshape(8, 3, HALF, 128), ('fs', 'tp'), 0, 0, til...  16.4 us
    unnamed x31, local copies, waits for them, and re-layouts  10.5 us
    all_to_all x1, waiting for transfers between devices, per_device(): back = lax.all_to_all(sent, 'sp', 0, 0, tiled=True)  9.83 us
    pallas_call x1, Pallas kernels, project(): pl.pallas_call(project_kernel, grid=(SEQS,), in_specs=[pl.BlockSpec((1, 2...  9.74 us
    dot_general x2, matrix products, dot(): return jnp.dot(a, b, preferred_element_type=F32)  7.32 us
  transfers between devices with their start and end apart: 7, of which 4 were waited for; matrix products, arithmetic and copies ran while one was open for 13% of the time, Pallas kernels for 23%

profile of v1, /device:TPU:1, one launch (start us, length us, event | category | flops | bytes accessed | tf_op | source)
XLA Modules:
  0.0 247.5 jit_solution(18235596424471861591)
XLA Ops:
  7.3 0.7 all-gather.3.cloned.1.call-update
  7.9 1.3 copy.77
  9.2 1.3 copy.78
  10.5 0.2 copy.79
  10.7 1.0 copy.80
  11.7 1.0 copy.81
  12.7 2.1 copy.82
  14.9 0.9 copy-done.5
  15.8 0.1 copy-done.4
  16.0 0.1 copy-done.3
  16.2 1.7 copy-done.2
  17.8 4.8 %all-to-all-start = ((bf16[4,512,768]{1,2,0:T(8,128)(2,1)}), bf16[4,512,768]{1,2,0:T(8,128)(2,1)S(1)}, u32[]{:S(2)}, u32[]{:S(2)}) async-start(bf16[4,512,768]{1,2,0:T(8,128)(2,1)} %bitcast.73), calls=%async_computation | async-start | bytes 6291456 | tf_op jit(solution)/shard_map/all_to_all | solution.py:250
  22.7 5.2 %pad_maximum_fusion = bf16[2,512,2048]{2,1,0:T(8,128)(2,1)} fusion(bf16[1,512,2048]{2,1,0:T(8,128)(2,1)} %bitcast.82, bf16[1,512,2048]{2,1,0:T(8,128)(2,1)} %bitcast.83), kind=kLoop, calls=%fused_computation.4 | loop fusion | flops 2097152 | bytes 8388608 | tf_op jit(solution)/shard_map/stack | solution.py:292
  27.9 0.7 copy-done.9
  28.5 56.9 %all-to-all-done = bf16[4,512,768]{1,2,0:T(8,128)(2,1)S(1)} async-done(((bf16[4,512,768]{1,2,0:T(8,128)(2,1)}), bf16[4,512,768]{1,2,0:T(8,128)(2,1)S(1)}, u32[]{:S(2)}, u32[]{:S(2)}) %all-to-all-start) | async-done | bytes 3145760 | tf_op jit(solution)/shard_map/all_to_all | solution.py:250
  85.4 2.8 %copy.83 = bf16[4,512,768]{2,1,0:T(8,128)(2,1)} copy(bf16[4,512,768]{1,2,0:T(8,128)(2,1)S(1)} %all-to-all-done) | data formatting | bytes 6291456 | tf_op jit(solution)/shard_map/all_to_all | solution.py:250
  88.2 9.7 %project.1 = (bf16[16,480,128]{2,1,0:T(8,128)(2,1)}, f32[4,384,128]{2,1,0:T(8,128)S(1)}, bf16[4,384,128]{2,1,0:T(8,128)(2,1)S(1)}) custom-call(bf16[4,2,384,1024]{3,2,1,0:T(8,128)(2,1)} %bitcast.95, f32[2,1024]{1,0:T(2,128)S(1)} %reshape.255.gain_ref, bf16[2048,768]{1,0:T(8,128)(2,1)} %bitcast.74), custom_call_target="tpu_custom_call" | custom-call | flops 4800000000 | bytes 13000000 | tf_op jit(solution)/shard_map/project/pallas_call | solution.py:79
  98.0 7.1 %all-to-all-start.1 = ((bf16[16,480,128]{2,1,0:T(8,128)(2,1)}), bf16[16,480,128]{2,1,0:T(8,128)(2,1)S(1)}, u32[]{:S(2)}, u32[]{:S(2)}) async-start(bf16[16,480,128]{2,1,0:T(8,128)(2,1)} %get-tuple-element.5), calls=%async_computation.1 | async-start | bytes 3932160 | tf_op jit(solution)/shard_map/all_to_all | solution.py:253
  105.2 0.8 dynamic_slice.13
  106.0 3.2 %collective-permute-start = (f32[4,2,128]{2,1,0:T(2,128)S(1)}, f32[4,2,128]{2,1,0:T(2,128)S(1)}, u32[]{:S(2)}, u32[]{:S(2)}) collective-permute-start(f32[4,2,128]{2,1,0:T(2,128)S(1)} %slice.126), channel_id=1, source_target_pairs={{0,8},{8,16},{16,24},{24,32},{32,40},{40,48},{48,56},{56,64},{64,7... | collective-permute-start | bytes 12296 | tf_op jit(solution)/shard_map/ppermute | solution.py:261
  109.2 24.0 %all-to-all-done.1.recv_ref = bf16[16,480,128]{2,1,0:T(8,128)(2,1)S(1)} async-done(((bf16[16,480,128]{2,1,0:T(8,128)(2,1)}), bf16[16,480,128]{2,1,0:T(8,128)(2,1)S(1)}, u32[]{:S(2)}, u32[]{:S(2)}) %all-to-all-start.1) | async-done | bytes 1966112 | tf_op jit(solution)/shard_map/all_to_all | solution.py:253
  133.2 46.2 %attend.1 = bf16[16,192,128]{2,1,0:T(8,128)(2,1)} custom-call(f32[8]{0:T(128)S(1)} %copy-done.1, f32[1,128]{1,0:T(1,128)S(1)} %pad_bitcast_fusion.gain_ref, bf16[16,480,128]{2,1,0:T(8,128)(2,1)S(1)} %all-to-all-done.1.recv_ref), custom_call_target="tpu_custom_call" | custom-call | flops 10000000000 | bytes 3000000 | tf_op jit(solution)/shard_map/attend/pallas_call | solution.py:204
  179.4 4.7 %all-to-all-start.2 = ((bf16[16,192,128]{2,1,0:T(8,128)(2,1)}), bf16[16,192,128]{2,1,0:T(8,128)(2,1)S(1)}, u32[]{:S(2)}, u32[]{:S(2)}) async-start(bf16[16,192,128]{2,1,0:T(8,128)(2,1)} %attend.1), calls=%async_computation.2 | async-start | bytes 1572864 | tf_op jit(solution)/shard_map/all_to_all | solution.py:258
  184.2 0.8 dynamic_slice.15
  184.9 1.1 multiply_convert_fusion
  186.0 0.3 multiply_reduce_fusion
  186.4 0.3 copy.84
  186.7 0.3 copy.85
  187.0 0.3 copy.86
  187.2 9.8 %all-to-all-done.2 = bf16[16,192,128]{2,1,0:T(8,128)(2,1)S(1)} async-done(((bf16[16,192,128]{2,1,0:T(8,128)(2,1)}), bf16[16,192,128]{2,1,0:T(8,128)(2,1)S(1)}, u32[]{:S(2)}, u32[]{:S(2)}) %all-to-all-start.2) | async-done | bytes 786464 | tf_op jit(solution)/shard_map/all_to_all | solution.py:258
  197.1 0.2 reverse_select_fusion
  197.3 0.3 fusion.30
  197.7 0.3 fusion.31
  198.0 0.8 broadcast_in_dim.17
  198.8 3.7 %concatenate.44 = bf16[8,1,192,128]{3,2,1,0:T(8,128)(2,1)} concatenate(bf16[8,1,192,6]{3,2,1,0:T(8,128)(2,1)S(1)} %bitcast.87, bf16[8,1,192,6]{3,2,1,0:T(8,128)(2,1)S(1)} %bitcast.86, bf16[8,1,192,3]{3,2,1,0:T(8,128)(2,1)S(1)} %bitcast.84, bf16[8,1,192,3]{3,2,1,0:T(8,128)(2,1)S(1)} %bitcast.85, bf16[8,1,192,1]{3,2,1,0:T(8,128)(2,1)S(1)} %copy.84, ...), dimensions={3} | concatenate | bytes 786432 | tf_op jit(solution)/shard_map/concatenate | solution.py:275
  202.5 2.5 %pad_maximum_fusion.1 = bf16[8,3,192,128]{3,2,1,0:T(8,128)(2,1)} fusion(bf16[8,1,192,128]{3,2,1,0:T(8,128)(2,1)} %concatenate.44, bf16[8,1,192,128]{3,2,1,0:T(8,128)(2,1)} %bitcast.90, bf16[8,1,192,64]{3,2,1,0:T(8,128)(2,1)S(1)} %bitcast.89, bf16[8,1,192,64]{3,2,1,0:T(8,128)(2,1)S(1)} %bitcast.88), kind=kLoop, calls=%fused_computation.11 | loop fusion | flops 4718592 | bytes 2359296 | tf_op jit(solution)/shard_map/stack | solution.py:280
  205.0 5.9 %all-to-all-start.3 = ((bf16[8,3,192,128]{3,2,1,0:T(8,128)(2,1)}), bf16[8,3,192,128]{3,2,1,0:T(8,128)(2,1)S(1)}, u32[]{:S(2)}, u32[]{:S(2)}) async-start(bf16[8,3,192,128]{3,2,1,0:T(8,128)(2,1)} %pad_maximum_fusion.1), calls=%async_computation.3 | async-start | bytes 2359296 | tf_op jit(solution)/shard_map/all_to_all | solution.py:281
  210.9 16.4 %all-to-all-done.3 = bf16[8,3,192,128]{3,2,1,0:T(8,128)(2,1)S(1)} async-done(((bf16[8,3,192,128]{3,2,1,0:T(8,128)(2,1)}), bf16[8,3,192,128]{3,2,1,0:T(8,128)(2,1)S(1)}, u32[]{:S(2)}, u32[]{:S(2)}) %all-to-all-start.3) | async-done | bytes 1179680 | tf_op jit(solution)/shard_map/all_to_all | solution.py:281
  227.3 0.2 slice_convert_fusion
  227.6 1.8 fusion.19
  229.4 0.3 copy.89
  229.7 0.3 reshape.261
  230.0 0.3 copy.88
  230.3 0.3 reshape.260
  230.6 0.7 fusion.26
  231.3 2.0 fusion.14
  233.4 3.2 %fusion.4 = f32[192,2048]{1,0:T(8,128)S(1)} fusion(bf16[192,1024]{1,0:T(8,128)(2,1)S(1)} %reshape.261, bf16[2,1024,2048]{2,1,0:T(8,128)(2,1)} %all-gather.5.cloned.1.call-done, f32[192]{0:T(256)S(1)} %get-tuple-element.32), kind=kOutput, calls=%fused_computation.7 | convolution fusion | flops 805699584 | bytes 6161152 | tf_op jit(solution)/shard_map/dot_general | solution.py:26
  236.6 4.1 %fusion.6 = bf16[1,192,2048]{2,1,0:T(8,128)(2,1)} fusion(f32[192,2048]{1,0:T(8,128)S(1)} %fusion.4, bf16[192,1024]{1,0:T(8,128)(2,1)S(1)} %reshape.260, bf16[2,1024,2048]{2,1,0:T(8,128)(2,1)} %all-gather.5.cloned.1.call-done, f32[192]{0:T(256)S(1)} %get-tuple-element.33), kind=kOutput, calls=%fused_computation.9 | convolution fusion | flops 806486016 | bytes 6947584 | tf_op jit(solution)/shard_map/dot_general | solution.py:26
  (45 shorter events, 0.6 us)
Async XLA Ops:
  7.2 98.8 %copy-start = (f32[3,512]{1,0:T(4,128)S(1)}, f32[3,512]{1,0:T(4,128)}, u32[]{:S(2)}) copy-start(f32[3,512]{1,0:T(4,128)} %param.23) | copy-start | bytes 18436
  7.2 3.3 %copy-start.6 = (bf16[512,512]{1,0:T(8,128)(2,1)S(1)}, bf16[512,512]{1,0:T(8,128)(2,1)}, u32[]{:S(2)}) copy-start(bf16[512,512]{1,0:T(8,128)(2,1)} %param.18) | copy-start | bytes 1572868
  7.2 3.5 %copy-start.7 = (bf16[512,512]{1,0:T(8,128)(2,1)S(1)}, bf16[512,512]{1,0:T(8,128)(2,1)}, u32[]{:S(2)}) copy-start(bf16[512,512]{1,0:T(8,128)(2,1)} %param.19) | copy-start | bytes 1572868
  7.2 4.5 %copy-start.8 = (bf16[512,512]{1,0:T(8,128)(2,1)S(1)}, bf16[512,512]{1,0:T(8,128)(2,1)}, u32[]{:S(2)}) copy-start(bf16[512,512]{1,0:T(8,128)(2,1)} %param.20) | copy-start | bytes 1572868
  7.2 81.0 %all-gather.3.cloned.1.call-start = ((), (), s32[]{:S(2)}) async-start(), calls=%async_computation.4 | async-start | bytes 7077888 | tf_op jit(solution)/shard_map/all_gather | solution.py:245
  14.8 1.0 copy-start.5
  14.8 1.2 copy-start.4
  14.8 1.4 copy-start.3
  16.2 1.7 copy-start.2
  17.8 67.6 %all-to-all-start = ((bf16[4,512,768]{1,2,0:T(8,128)(2,1)}), bf16[4,512,768]{1,2,0:T(8,128)(2,1)S(1)}, u32[]{:S(2)}, u32[]{:S(2)}) async-start(bf16[4,512,768]{1,2,0:T(8,128)(2,1)} %bitcast.73), calls=%async_computation | async-start | bytes 6291456 | tf_op jit(solution)/shard_map/all_to_all | solution.py:250
  22.7 210.7 %all-gather.5.cloned.1.call-start = ((), (), s32[]{:S(2)}) async-start(), calls=%async_computation.5 | async-start | bytes 12582912 | tf_op jit(solution)/shard_map/all_gather | solution.py:292
  27.8 0.7 copy-start.9
  98.0 35.2 %copy-start.1 = (f32[8]{0:T(128)S(1)}, f32[8]{0:T(128)}, u32[]{:S(2)}) copy-start(f32[8]{0:T(128)} %offset_ref.1) | copy-start | bytes 100
  98.0 35.2 %all-to-all-start.1 = ((bf16[16,480,128]{2,1,0:T(8,128)(2,1)}), bf16[16,480,128]{2,1,0:T(8,128)(2,1)S(1)}, u32[]{:S(2)}, u32[]{:S(2)}) async-start(bf16[16,480,128]{2,1,0:T(8,128)(2,1)} %get-tuple-element.5), calls=%async_computation.1 | async-start | bytes 3932160 | tf_op jit(solution)/shard_map/all_to_all | solution.py:253
  106.0 79.0 %collective-permute-start = (f32[4,2,128]{2,1,0:T(2,128)S(1)}, f32[4,2,128]{2,1,0:T(2,128)S(1)}, u32[]{:S(2)}, u32[]{:S(2)}) collective-permute-start(f32[4,2,128]{2,1,0:T(2,128)S(1)} %slice.126), channel_id=1, source_target_pairs={{0,8},{8,16},{16,24},{24,32},{32,40},{40,48},{48,56},{56,64},{64,7... | collective-permute-start | bytes 12296 | tf_op jit(solution)/shard_map/ppermute | solution.py:261
  179.4 17.7 %all-to-all-start.2 = ((bf16[16,192,128]{2,1,0:T(8,128)(2,1)}), bf16[16,192,128]{2,1,0:T(8,128)(2,1)S(1)}, u32[]{:S(2)}, u32[]{:S(2)}) async-start(bf16[16,192,128]{2,1,0:T(8,128)(2,1)} %attend.1), calls=%async_computation.2 | async-start | bytes 1572864 | tf_op jit(solution)/shard_map/all_to_all | solution.py:258
  205.0 22.3 %all-to-all-start.3 = ((bf16[8,3,192,128]{3,2,1,0:T(8,128)(2,1)}), bf16[8,3,192,128]{3,2,1,0:T(8,128)(2,1)S(1)}, u32[]{:S(2)}, u32[]{:S(2)}) async-start(bf16[8,3,192,128]{3,2,1,0:T(8,128)(2,1)} %pad_maximum_fusion.1), calls=%async_computation.3 | async-start | bytes 2359296 | tf_op jit(solution)/shard_map/all_to_all | solution.py:281
Sparse Core Ops, SparseCore 0:
  9.7 69.1 all-gather.2
  80.5 30.6 all-gather.4

commit v2 on v1

v2 whole, which is shorter than its diff:
```python
import functools

import jax
import jax.numpy as jnp
from jax import lax
from jax.experimental import pallas as pl
from jax.experimental.pallas import tpu as pltpu
from jax.sharding import PartitionSpec as P

D = 2048
CONV_CH = 1024
ATT_WIDTH = 1024
SEQS = 4
ROWS = 384
HALF = 192
BLOCKS = 16
HD = 64
MESSAGE = HALF + HALF // 2
epsilon = 1e-06
LOG2E = 1.4426950408889634
F32 = jnp.float32
BF16 = jnp.bfloat16


def dot(a, b):
    return jnp.dot(a, b, preferred_element_type=F32)


def dot_nt(a, b):
    return lax.dot_general(a, b, (((1,), (1,)), ((), ())), preferred_element_type=F32)


def three_parts(x):
    a = x.astype(BF16)
    rest = x - a.astype(F32)
    b = rest.astype(BF16)
    return a, b, (rest - b.astype(F32)).astype(BF16)


MESH = pl.DeviceIdType.MESH
LEFT, RIGHT = slice(0, 384), slice(384, 768)


def mod4(value):
    return lax.rem(value + 8, 4)


def front_kernel(
    tokens_ref,
    gain_ref,
    wq_ref,
    wk_ref,
    wv_ref,
    wo_ref,
    wi_ref,
    wc_ref,
    att_ref,
    conv_ref,
    own_ref,
    mate_ref,
    gated_ref,
    outgate_ref,
    att_other_ref,
    conv_other_ref,
    tok,
    wts,
    msg,
    recv,
    mate,
    local_sem,
    spread_send,
    spread_recv,
    near_send,
    near_recv,
    far_send,
    far_recv,
    pass_send,
    pass_recv,
    tok_send,
    tok_recv,
    pair_send,
    pair_recv,
    msg_send,
    msg_recv,
    mate_send,
    mate_recv,
    other_send,
    other_recv,
):
    place, x, core = lax.axis_index("sp"), lax.axis_index("fs"), lax.axis_index("tp")
    y, z = lax.rem(place, 4), lax.div(place, 4)
    sibling = (place, x, 1 - core)
    mats = (wq_ref, wk_ref, wv_ref, wo_ref, wi_ref, wc_ref)

    def remote(src, dst, send, recv_sem, device):
        return pltpu.make_async_remote_copy(
            src_ref=src, dst_ref=dst, send_sem=send, recv_sem=recv_sem, device_id=device, device_id_type=MESH
        )

    own_tokens = pltpu.make_async_copy(tokens_ref, tok.at[x, core], local_sem.at[6])
    own_tokens.start()
    own_weights = []
    for m in range(6):
        for part in range(4):
            own_weights.append(
                pltpu.make_async_copy(
                    mats[m].at[pl.ds(part * 128, 128), pl.ds(pl.multiple_of(x * 128, 128), 128)],
                    wts.at[x, part, :, m * 128 : (m + 1) * 128],
                    local_sem.at[7 + 4 * m + part],
                )
            )
    for copy in own_weights:
        copy.start()

    barrier = pltpu.get_barrier_semaphore()
    for k in range(1, 4):
        pl.semaphore_signal(barrier, inc=1, device_id=(place, mod4(x + k), core), device_id_type=MESH)
    pl.semaphore_signal(barrier, inc=1, device_id=sibling, device_id_type=MESH)

    def greet(k, _):
        there = lax.rem(place + k, BLOCKS)
        pl.semaphore_signal(barrier, inc=1, device_id=(there, x, core), device_id_type=MESH)
        pl.semaphore_signal(barrier, inc=1, device_id=(there, x, 1 - core), device_id_type=MESH)
        return 0

    lax.fori_loop(1, BLOCKS, greet, 0)
    pl.semaphore_wait(barrier, 34)

    rows_at = pl.multiple_of(place * 32, 32)

    def spread(k, m):
        there = mod4(x + k)
        return remote(
            mats[m].at[pl.ds(rows_at, 32), pl.ds(pl.multiple_of(there * 128, 128), 128)],
            wts.at[x, z, pl.ds(pl.multiple_of(y * 32, 32), 32), m * 128 : (m + 1) * 128],
            spread_send.at[k - 1, m],
            spread_recv.at[k - 1, m],
            (place, there, core),
        )

    for k in range(1, 4):
        for m in range(6):
            spread(k, m).start()

    own_tokens.wait()
    top, bottom = pl.ds(0, HALF), pl.ds(HALF, HALF)

    def hop(slot, f, rows, by):
        piece = tok.at[f, core, rows]
        return remote(piece, piece, tok_send.at[slot], tok_recv.at[slot], (place, mod4(x + by), core))

    def pair(slot, f, rows):
        piece = tok.at[f, core, rows]
        return remote(piece, piece, pair_send.at[slot], pair_recv.at[slot], sibling)

    right_a, right_b = hop(0, x, top, 1), hop(1, x, bottom, 1)
    left_b, left_a = hop(2, x, bottom, -1), hop(3, x, top, -1)
    before, after, across = mod4(x - 1), mod4(x + 1), mod4(x + 2)
    on_right, on_left = hop(4, before, top, 1), hop(5, after, bottom, -1)
    for copy in (right_a, left_b, right_b, left_a):
        copy.start()
    pairs = [
        pair(0, x, top),
        pair(1, x, bottom),
        pair(2, before, top),
        pair(3, after, bottom),
        pair(4, before, bottom),
        pair(5, after, top),
        pair(6, across, top),
        pair(7, across, bottom),
    ]
    pairs[0].start()
    pairs[1].start()

    for k in range(1, 4):
        for m in range(6):
            spread(k, m).wait_recv()

    my_rows = pl.ds(pl.multiple_of(y * 32, 32), 32)

    def near(k, i, way):
        f = mod4(x + i)
        piece = wts.at[f, z, my_rows, (LEFT, RIGHT)[way]]
        there = (z * 4 + mod4(y + k), x, core) if way == 0 else (mod4(z + k) * 4 + y, x, core)
        at = (3 * way + k - 1) * 3 + i - 1
        return remote(piece, piece, near_send.at[at], near_recv.at[at], there)

    for k in range(1, 4):
        for i in range(1, 4):
            for way in range(2):
                near(k, i, way).start()
    for k in range(1, 4):
        for i in range(1, 4):
            for way in range(2):
                near(k, i, way).wait_recv()

    def far(by, i, way):
        f = mod4(x + i)
        if way == 0:
            piece, there = wts.at[f, z, :, LEFT], (mod4(z + by) * 4 + y, x, core)
        else:
            piece, there = wts.at[f, :, my_rows, RIGHT], (z * 4 + mod4(y + by), x, core)
        at = (2 * way + (by + 1) // 2) * 3 + i - 1
        return remote(piece, piece, far_send.at[at], far_recv.at[at], there)

    def onward(by, i, way):
        f = mod4(x + i)
        start = 0 if by == 1 else 1
        if way == 0:
            piece = wts.at[f, mod4(z - by), 64 * start : 64 * start + 64, LEFT]
            there = (mod4(z + by) * 4 + y, x, core)
        else:
            rows = pl.ds(pl.multiple_of(mod4(y - by) * 32, 32), 32)
            piece = wts.at[f, 2 * start : 2 * start + 2, rows, RIGHT]
            there = (z * 4 + mod4(y + by), x, core)
        at = (2 * way + (by + 1) // 2) * 3 + i - 1
        return remote(piece, piece, pass_send.at[at], pass_recv.at[at], there)

    kinds = [(by, i, way) for i in range(1, 4) for by in (1, -1) for way in range(2)]
    for kind in kinds:
        far(*kind).start()
    right_a.wait_recv()
    on_right.start()
    pairs[2].start()
    left_b.wait_recv()
    on_left.start()
    pairs[3].start()
    for kind in kinds:
        far(*kind).wait_recv()
        onward(*kind).start()
    others = [
        remote(att_ref, att_other_ref, other_send.at[0], other_recv.at[0], sibling),
        remote(conv_ref, conv_other_ref, other_send.at[1], other_recv.at[1], sibling),
    ]
    for copy in own_weights:
        copy.wait()
    for kind in kinds:
        onward(*kind).wait_recv()

    def message(s, j, half):
        number = 2 * core + j
        there = mod4(s + number) * 4 + number
        at = 4 * s + 2 * j + half
        return remote(
            msg.at[at], recv.at[place], msg_send.at[at], msg_recv.at[place], (there, x, half)
        ), lax.abs(there - place) + lax.abs(half - core)

    def step(i, _):
        s = mod4(x + i + lax.div(i, 2) - 2 * lax.div(i, 3))

        @pl.when(i == 0)
        def _():
            pairs[0].wait_recv()
            pairs[1].wait_recv()

        @pl.when(i == 1)
        def _():
            right_b.wait_recv()
            pairs[4].start()
            left_a.wait_recv()
            pairs[5].start()
            pairs[3].wait_recv()
            pairs[5].wait_recv()

        @pl.when(i == 2)
        def _():
            pairs[2].wait_recv()
            pairs[4].wait_recv()

        @pl.when(i == 3)
        def _():
            on_right.wait_recv()
            pairs[6].start()
            on_left.wait_recv()
            pairs[7].start()
            for copy in others:
                copy.start()
            pairs[6].wait_recv()
            pairs[7].wait_recv()

        low = tok[s, 0].astype(F32)
        high = tok[s, 1].astype(F32)
        squares = jnp.sum(low * low, axis=1, keepdims=True) + jnp.sum(high * high, axis=1, keepdims=True)
        scale = lax.rsqrt(squares / D + epsilon)
        total = dot((low * gain_ref[0:1, :]).astype(BF16), wts[0:2].reshape(1024, 768)) + dot(
            (high * gain_ref[1:2, :]).astype(BF16), wts[2:4].reshape(1024, 768)
        )
        out = (total * scale).astype(BF16)
        query, key, value = out[:, 0:128], out[:, 128:256], out[:, 256:384]
        for j in range(2):
            mine = slice(j * HD, (j + 1) * HD)
            both = jnp.concatenate((key[:, mine], value[:, mine]), axis=1)
            for half in range(2):
                r = half * HALF
                folded = jnp.concatenate((query[r : r + 96, mine], query[r + 96 : r + HALF, mine]), axis=1)
                msg[4 * s + 2 * j + half, 0:HALF, :] = both[r : r + HALF]
                msg[4 * s + 2 * j + half, HALF : HALF + 96, :] = folded
        outgate_ref[s] = out[:, 384:512]
        gated_ref[s] = out[:, 512:640].astype(F32) * out[:, 640:768].astype(F32)
        for j in range(2):
            for half in range(2):
                copy, apart = message(s, j, half)

                @pl.when(apart > 0)
                def _():
                    copy.start()

                @pl.when(apart == 0)
                def _():
                    recv[place] = msg[4 * s + 2 * j + half]

        return 0

    lax.fori_loop(0, 4, step, 0)

    def to_mate(block):
        return remote(
            recv.at[block, 0:HALF], mate.at[block], mate_send.at[block], mate_recv.at[block], sibling
        )

    source_core = lax.div(y, 2)

    def arrive(k, _):
        block = lax.rem(place + k, BLOCKS)

        @pl.when(k + lax.abs(source_core - core) > 0)
        def _():
            remote(
                msg.at[0], recv.at[block], msg_send.at[0], msg_recv.at[block], (block, x, source_core)
            ).wait_recv()

        to_mate(block).start()
        return 0

    lax.fori_loop(0, BLOCKS, arrive, 0)
    own_out = pltpu.make_async_copy(recv, own_ref, local_sem.at[0])
    own_out.start()

    def arrived(block, _):
        to_mate(block).wait_recv()
        return 0

    lax.fori_loop(0, BLOCKS, arrived, 0)
    mate_out = pltpu.make_async_copy(mate, mate_ref, local_sem.at[1])
    mate_out.start()

    for k in range(1, 4):
        for m in range(6):
            spread(k, m).wait_send()
        for i in range(1, 4):
            for way in range(2):
                near(k, i, way).wait_send()
    for kind in kinds:
        far(*kind).wait_send()
        onward(*kind).wait_send()
    for copy in [right_a, right_b, left_a, left_b, on_right, on_left] + pairs:
        copy.wait_send()

    def left_here(at, _):
        s = lax.div(at, 4)
        j = lax.div(lax.rem(at, 4), 2)
        copy, apart = message(s, j, lax.rem(at, 2))

        @pl.when(apart > 0)
        def _():
            copy.wait_send()

        to_mate(at).wait_send()
        return 0

    lax.fori_loop(0, BLOCKS, left_here, 0)
    own_out.wait()
    mate_out.wait()
    for copy in others:
        copy.wait()


def front(tokens, gains, mats, out_att, out_conv):
    hbm = pl.BlockSpec(memory_space=pl.ANY)
    vmem = pl.BlockSpec(memory_space=pltpu.VMEM)
    dma = lambda *shape: pltpu.SemaphoreType.DMA(shape)
    return pl.pallas_call(
        front_kernel,
        in_specs=[hbm, vmem] + [hbm] * 8,
        out_specs=[hbm, hbm, vmem, vmem, hbm, hbm],
        out_shape=[
            jax.ShapeDtypeStruct((BLOCKS, MESSAGE, 128), BF16),
            jax.ShapeDtypeStruct((BLOCKS, HALF, 128), BF16),
            jax.ShapeDtypeStruct((SEQS, ROWS, 128), F32),
            jax.ShapeDtypeStruct((SEQS, ROWS, 128), BF16),
            jax.ShapeDtypeStruct(out_att.shape, BF16),
            jax.ShapeDtypeStruct(out_conv.shape, BF16),
        ],
        scratch_shapes=[
            pltpu.VMEM((SEQS, 2, ROWS, 1024), BF16),
            pltpu.VMEM((4, 4, 128, 768), BF16),
            pltpu.VMEM((BLOCKS, MESSAGE, 128), BF16),
            pltpu.VMEM((BLOCKS, MESSAGE, 128), BF16),
            pltpu.VMEM((BLOCKS, HALF, 128), BF16),
            dma(31),
            dma(3, 6), dma(3, 6),
            dma(18), dma(18),
            dma(12), dma(12),
            dma(12), dma(12),
            dma(6), dma(6),
            dma(8), dma(8),
            dma(16), dma(16),
            dma(16), dma(16),
            dma(2), dma(2),
        ],
        compiler_params=pltpu.CompilerParams(
            collective_id=0, has_side_effects=True, vmem_limit_bytes=56 << 20
        ),
        name="front",
    )(tokens, gains, *mats, out_att, out_conv)


def attend_kernel(
    offset_ref, gain_ref, own_ref, mate_ref, out_ref, keys, values, queries, scores, decays, weights, total
):
    half = lax.axis_index("tp")
    lanes = lambda shape: lax.broadcasted_iota(jnp.int32, shape, 1)
    rows = lambda shape: lax.broadcasted_iota(jnp.int32, shape, 0)
    offset = jnp.full((HALF, 128), offset_ref[0] * LOG2E, F32)
    o1, o2, o3 = (part.astype(F32) for part in three_parts(offset))
    lane_q = lanes((HALF, 128))
    offset_row = jnp.where(
        lane_q == 0, -o1, jnp.where(lane_q == 1, -o2, jnp.where(lane_q == 2, -o3, 0.0))
    ).astype(BF16)
    square = (ROWS, HALF)
    source = lax.rem(rows(square), 8) * 48 + rows(square) // 8 - lanes(square)
    permute_own = (source == half * HALF).astype(F32).astype(BF16)
    permute_mate = (source == HALF - half * HALF).astype(F32).astype(BF16)
    shape = (128, 128)
    twice_low = (rows(shape) == lax.rem(lanes(shape), HD)).astype(F32).astype(BF16)
    twice_high = (rows(shape) == lax.rem(lanes(shape), HD) + HD).astype(F32).astype(BF16)
    take_high = (lanes((HD, 128)) == rows((HD, 128)) + HD).astype(F32).astype(BF16)
    ones = (lanes((ROWS, 128)) < 3).astype(F32).astype(BF16)
    for block in range(BLOCKS):
        pair = dot(permute_own, own_ref[block, 0:HALF, :]) + dot(permute_mate, mate_ref[block])
        pair = pair.astype(BF16)
        keys[block * ROWS : (block + 1) * ROWS, 0:128] = dot(pair, twice_low).astype(BF16)
        keys[block * ROWS : (block + 1) * ROWS, 128:256] = ones
        values[block] = dot_nt(take_high, pair).astype(BF16)
        packed = own_ref[block, HALF:MESSAGE, :]
        q = jnp.concatenate((dot(packed, twice_low), dot(packed, twice_high)), axis=0) * (LOG2E / 8)
        q_high = q.astype(BF16).astype(F32)
        at = slice((block % 2) * HALF, (block % 2 + 1) * HALF)
        queries[block // 2, at, 0:128] = jnp.where(lane_q < HD, q_high, q - q_high).astype(BF16)
        queries[block // 2, at, 128:256] = offset_row

    sub = rows((8, ROWS))
    lane = lanes((8, ROWS))
    where_q = lane + half * HALF + jnp.where(lane < HALF, 0, HALF)

    def tile(tile_index, block, carry, ahead, slot):
        begin = pl.multiple_of(block * ROWS, ROWS)
        z_ref, d_ref, w_ref = scores.at[slot], decays.at[slot], weights.at[slot]
        z_ref[...] = dot_nt(keys[pl.ds(begin, ROWS), :], queries[tile_index])
        run = jnp.zeros((8, ROWS), F32)
        for r in reversed(range(48)):
            z = z_ref[8 * r : 8 * r + 8, :]
            soft = jnp.maximum(z, jnp.log2(1.0 + jnp.exp2(jnp.minimum(z, 126.0))))
            if ahead is not None:
                valid = ahead > r
                soft = jnp.where(valid, soft, 0.0)
            run = run + soft
            decay = jnp.exp2(z - run)
            if ahead is not None:
                decay = jnp.where(valid, decay, 0.0)
            d_ref[8 * r : 8 * r + 8, :] = decay
        suffix = run
        for step in (1, 2, 4):
            moved = pltpu.roll(suffix, 8 - step, 0)
            suffix = suffix + jnp.where(sub < 8 - step, moved, 0.0)
        after = jnp.where(sub < 7, pltpu.roll(suffix, 7, 0), 0.0)
        kept = jnp.exp2(-(carry + after))
        for i in range(24):
            both = jnp.concatenate(
                (d_ref[16 * i : 16 * i + 8, :] * kept, d_ref[16 * i + 8 : 16 * i + 16, :] * kept), axis=0
            )
            w_ref[16 * i : 16 * i + 16, :] = both.astype(BF16)
        total[...] += dot(values[block], w_ref[...])
        return carry + jnp.broadcast_to(suffix[0:1], (8, ROWS))

    gain = gain_ref[...]
    gain_lane = lanes((8, 512))
    out_lane = lanes((ROWS, 128))

    def one_tile(m, _):
        total[...] = jnp.zeros_like(total)
        carry = jnp.zeros((8, ROWS), F32)
        carry = tile(m, 2 * m + 1, carry, where_q - ROWS - 48 * sub, 0)
        carry = tile(m, 2 * m, carry, where_q - 48 * sub, 1)

        def before(i, carry):
            at = 2 * (m - 1 - i)
            carry = tile(m, at + 1, carry, None, 0)
            return tile(m, at, carry, None, 1)

        carry = lax.fori_loop(0, m, before, carry)
        attended = total[...]
        squares = jnp.sum(attended * attended, axis=0, keepdims=True)
        parts = [p.astype(F32) for p in three_parts(carry[0:1]) + three_parts(squares)]
        side = jnp.concatenate(parts + [jnp.zeros((HD - 6, ROWS), F32)], axis=0)
        message = jnp.concatenate((attended, side), axis=0).T
        message = message * jnp.where(out_lane < HD, gain, 1.0)
        message = message.astype(BF16)
        out_ref[2 * m] = message[0:HALF]
        out_ref[2 * m + 1] = message[HALF:ROWS]
        return 0

    lax.fori_loop(0, BLOCKS // 2, one_tile, 0)


def attend(own, mate, offset, gain):
    whole = pl.BlockSpec(memory_space=pltpu.VMEM)
    return pl.pallas_call(
        attend_kernel,
        in_specs=[pl.BlockSpec(memory_space=pltpu.SMEM), whole, whole, whole],
        out_specs=whole,
        out_shape=jax.ShapeDtypeStruct((BLOCKS, HALF, 128), BF16),
        scratch_shapes=[
            pltpu.VMEM((BLOCKS * ROWS, 256), BF16),
            pltpu.VMEM((BLOCKS, HD, ROWS), BF16),
            pltpu.VMEM((BLOCKS // 2, ROWS, 256), BF16),
            pltpu.VMEM((2, ROWS, ROWS), F32),
            pltpu.VMEM((2, ROWS, ROWS), F32),
            pltpu.VMEM((2, ROWS, ROWS), BF16),
            pltpu.VMEM((HD, ROWS), F32),
        ],
        compiler_params=pltpu.CompilerParams(vmem_limit_bytes=48 << 20),
        cost_estimate=pl.CostEstimate(
            flops=10_000_000_000, bytes_accessed=3_000_000, transcendentals=30_000_000
        ),
        name="attend",
    )(offset, gain, own, mate)


def per_device(
    tokens,
    in_gain,
    w_query,
    w_key,
    w_value,
    w_outgate,
    w_ingate,
    w_conv_in,
    score_offset,
    conv_taps,
    att_gain,
    conv_gain,
    out_att,
    out_conv,
):
    place = lax.axis_index("sp")
    column = lax.axis_index("fs")
    core = lax.axis_index("tp")
    own, mate, gated, outgate, att_other, conv_other = front(
        tokens[0],
        in_gain.reshape(2, 1024),
        (w_query, w_key, w_value, w_outgate, w_ingate, w_conv_in),
        out_att,
        out_conv,
    )

    number = lax.rem(place, 4)
    both_cores = lax.ppermute(jnp.concatenate((score_offset, att_gain)), "tp", [(0, 1), (1, 0)])
    mine = jnp.where(number // 2 == core, jnp.concatenate((score_offset, att_gain)), both_cores)
    local_head = 2 * column + lax.rem(number, 2)
    offset = lax.dynamic_slice_in_dim(mine, local_head, 1, 0)
    gain = lax.dynamic_slice_in_dim(mine, 8 + local_head * HD, HD, 0)
    gain = jnp.concatenate((gain, jnp.ones((HD,), F32)))[None]
    sent = attend(own, mate, offset, gain)
    back = lax.all_to_all(sent, "sp", 0, 0, tiled=True)

    pairs = [(i, i + 1) for i in range(BLOCKS - 1)]
    before = lax.ppermute(gated[:, ROWS - 2 :], "sp", pairs)
    extended = jnp.concatenate((before, gated), axis=1)
    taps = lax.dynamic_slice_in_dim(conv_taps, column * 128, 128, 1)
    convolved = sum(taps[j] * extended[:, j : j + ROWS] for j in range(3))
    conv_out = outgate.astype(F32) * convolved
    conv_squares = jnp.sum(conv_out * conv_out, axis=2, keepdims=True)
    conv_mine = lax.dynamic_slice_in_dim(conv_gain, column * 128, 128, 0)
    conv_scaled = (conv_out * conv_mine).astype(BF16).reshape(8, HALF, 128)
    pieces = jnp.concatenate(three_parts(conv_squares), axis=2).reshape(8, HALF, 3)
    pieces = jnp.concatenate((pieces, jnp.zeros((8, HALF, 125), BF16)), axis=2)
    conv_home = lax.all_to_all(
        jnp.stack((conv_scaled, pieces), axis=1), ("fs", "tp"), 0, 0, tiled=True
    ).reshape(4, 2, 2, HALF, 128)

    by_head = back.reshape(4, 4, HALF, 128)
    ordered = jnp.stack(
        [jnp.stack([by_head[(s + n) % 4, n] for n in range(4)]) for s in range(SEQS)]
    )
    home = lax.all_to_all(ordered, "fs", 0, 0, tiled=True)
    home = home.reshape(4, 2, 2, HALF, 128)
    extra = home[..., HD : HD + 6].astype(F32)
    kept = extra[..., 0] + extra[..., 1] + extra[..., 2]
    att_sum = jnp.sum(extra[..., 3] + extra[..., 4] + extra[..., 5], axis=(0, 1, 2))
    conv_extra = conv_home[:, :, 1, :, 0:3].astype(F32)
    conv_sum = jnp.sum(conv_extra[..., 0] + conv_extra[..., 1] + conv_extra[..., 2], axis=(0, 1))
    att_scale = lax.rsqrt(att_sum / ATT_WIDTH + epsilon)
    conv_scale = lax.rsqrt(conv_sum / CONV_CH + epsilon)
    att_mat = home[..., :HD].transpose(1, 3, 0, 2, 4).reshape(2, HALF, 512)
    conv_mat = conv_home[:, :, 0].transpose(1, 2, 0, 3).reshape(2, HALF, 512)
    first = core == 0
    near = lambda a: jnp.where(first, a[0], a[1])
    far = lambda a: jnp.where(first, a[1], a[0])
    att_product = dot(near(att_mat), out_att) + dot(far(att_mat), att_other)
    conv_product = dot(near(conv_mat), out_conv) + dot(far(conv_mat), conv_other)
    mixed = att_scale[:, None] * att_product + conv_scale[:, None] * conv_product

    log_mass = jnp.log(2.0 - jnp.exp2(-kept))
    by_core = log_mass.transpose(1, 3, 0, 2).reshape(2, HALF, 8)
    far_rows = lax.ppermute(far(by_core), "tp", [(0, 1), (1, 0)])
    near_rows = near(by_core)
    log_mass = jnp.where(
        first,
        jnp.concatenate((near_rows, far_rows), axis=0),
        jnp.concatenate((far_rows, near_rows), axis=0),
    )
    return (mixed.astype(BF16)[None], log_mass[None])


def solution(mesh):
    return jax.shard_map(
        per_device,
        mesh=mesh,
        in_specs=(
            P("fs", "sp", "tp"),
            P(),
            P("fs", "tp"),
            P("fs", "tp"),
            P("fs", "tp"),
            P("fs", "tp"),
            P("fs", "tp"),
            P("fs", "tp"),
            P("tp"),
            P(None, "tp"),
            P("tp"),
            P("tp"),
            P("tp", None),
            P("tp", None),
        ),
        out_specs=(P("fs", ("sp", "tp"), None), P("fs", "sp", "tp")),
        check_vma=False,
    )
```

time: 248 us -> 177 us (0.71)
  waiting for transfers between devices: 108 us -> 20.4 us
  Pallas kernels: 55.9 us -> 102 us
  between operations: 14.4 us -> 0.97 us
  local copies, waits for them, and re-layouts: 22.2 us -> 11.3 us
  other arithmetic: 13.9 us -> 7.07 us
  starting transfers between devices: 25.9 us -> 29.8 us
  matrix products: 7.32 us -> 4.58 us
    all_to_all x3 -> x2, waiting for transfers between devices: 97.3 us -> 6.65 us  [the longest x1 6.65 us: per_device(): home = lax.all_to_all(ordered, 'fs', 0, 0, tiled=True)]
    pallas_call x1, Pallas kernels: 9.74 us -> 54.1 us  [front(): pl.pallas_call(front_kernel, in_specs=[hbm, vmem] + [hbm] * 8, out_specs=...]
    unnamed x31 -> x21, local copies, waits for them, and re-layouts: 10.5 us -> 3.54 us
    another operation x4 -> x5, other arithmetic: 7.67 us -> 1.33 us  [the longest x3 1.09 us: per_device(): jnp.stack([jnp.stack([by_head[(s + n) % 4, n] for n in range(4)]) for s i...]
    ppermute x0 -> x2, starting transfers between devices: none -> 4.69 us  [the longest x1 3.3 us: per_device(): far_rows = lax.ppermute(far(by_core), 'tp', [(0, 1), (1, 0)])]
    all_to_all x3 -> x2, starting transfers between devices: 17.9 us -> 13.6 us  [the longest x1 9.67 us: per_device(): lax.all_to_all(jnp.stack((conv_scaled, pieces), axis=1), ('fs', 'tp'), 0,...]
    all_to_all x1, waiting for transfers between devices: 9.83 us -> 13.7 us  [per_device(): back = lax.all_to_all(sent, 'sp', 0, 0, tiled=True)]
    concatenate x1, local copies, waits for them, and re-layouts: 3.72 us -> 0.01 us  [per_device(): jnp.concatenate((near_rows, far_rows), axis=0)]
  transfers between devices with their start and end apart: 7 -> 6, of which waited for: 4 -> 2; matrix products, arithmetic and copies ran while one was open for 13% -> 5% of each run, Pallas kernels for 23% -> 58%
where the time goes in v2:
time: 177 us; the launch traced here: 176 us
  Pallas kernels  102 us (58%)
  starting transfers between devices  29.8 us (17%)
  waiting for transfers between devices  20.4 us (12%)
  local copies, waits for them, and re-layouts  11.3 us (6%)
  other arithmetic  7.07 us (4%)
  matrix products  4.58 us (3%)
    pallas_call x1, Pallas kernels, front(): pl.pallas_call(front_kernel, in_specs=[hbm, vmem] + [hbm] * 8, out_specs=...  54.1 us
    pallas_call x1, Pallas kernels, attend(): pl.pallas_call(attend_kernel, in_specs=[pl.BlockSpec(memory_space=pltpu.S...  48.3 us
    all_to_all x1, waiting for transfers between devices, per_device(): back = lax.all_to_all(sent, 'sp', 0, 0, tiled=True)  13.7 us
    all_to_all x1, starting transfers between devices, per_device(): lax.all_to_all(jnp.stack((conv_scaled, pieces), axis=1), ('fs', 'tp'), 0,...  9.67 us
    all_to_all x1, waiting for transfers between devices, per_device(): home = lax.all_to_all(ordered, 'fs', 0, 0, tiled=True)  6.65 us
    ppermute x1, starting transfers between devices, per_device(): before = lax.ppermute(gated[:, ROWS - 2:], 'sp', pairs)  5.93 us
    all_to_all x1, starting transfers between devices, per_device(): back = lax.all_to_all(sent, 'sp', 0, 0, tiled=True)  5.58 us
    dot_general x4, matrix products, dot(): return jnp.dot(a, b, preferred_element_type=F32)  4.58 us
  transfers between devices with their start and end apart: 6, of which 2 were waited for; matrix products, arithmetic and copies ran while one was open for 5% of the time, Pallas kernels for 58%

profile of v2, /device:TPU:1, one launch (start us, length us, event | category | flops | bytes accessed | tf_op | source)
XLA Modules:
  0.0 176.5 jit_solution(1127428950094987808)
XLA Ops:
  0.6 0.0 copy-start
  0.6 0.8 pad_maximum_fusion.3
  1.4 1.4 collective-permute-start
  2.8 1.3 reshape.189.gain_ref
  4.1 54.1 %front.1 = (bf16[16,288,128]{2,1,0:T(8,128)(2,1)}, bf16[16,192,128]{2,1,0:T(8,128)(2,1)}, f32[4,384,128]{2,1,0:T(8,128)}, bf16[4,384,128]{2,1,0:T(8,128)(2,1)}, ...) custom-call(bf16[384,1024]{1,0:T(8,128)(2,1)} %bitcast.105, f32[2,1024]{1,0:T(2,128)} %reshape.189.gain_ref, ...), custom_call_target="tpu_custom_call" | custom-call | tf_op jit(solution)/shard_map/front/pallas_call | solution.py:382
  58.2 0.7 slice.159
  58.9 5.9 %collective-permute-start.1 = (f32[4,2,128]{2,1,0:T(2,128)S(1)}, f32[4,2,128]{2,1,0:T(2,128)S(1)}, u32[]{:S(2)}, u32[]{:S(2)}) collective-permute-start(f32[4,2,128]{2,1,0:T(2,128)S(1)} %slice.159), channel_id=1, source_target_pairs={{0,8},{8,16},{16,24},{24,32},{32,40},{40,48},{48,56},{56,64},{64,7... | collective-permute-start | bytes 12296 | tf_op jit(solution)/shard_map/ppermute | solution.py:578
  64.9 0.8 dynamic_slice.15
  65.7 0.0 collective-permute-done
  65.7 0.1 broadcast_select_fusion.6
  65.8 0.1 dynamic_slice.13
  65.8 0.6 dynamic_slice.12.offset_ref
  66.4 2.4 %multiply_convert_fusion = (bf16[4,384,128]{2,1,0:T(8,128)(2,1)S(1)}, f32[4,384,128]{2,1,0:T(8,128)S(1)}) fusion(f32[128]{0:T(128)S(1)} %dynamic_slice.15, f32[4,384,128]{2,1,0:T(8,128)} %get-tuple-element.12, f32[128]{0:T(128)S(1)} %get-tuple-element.44, f32[4,2,128]{2,1,0:T(2,128)S(1)} %collective-permute-done.1, f32[128]{0:T(128)S(1)} %get-tuple-element.45, ...), kind=kLoop, calls=%fused_computation.27 | loop fusion | flops 2162688 | bytes 2365440 | tf_op jit(solution)/shard_map/convert_element_type | solution.py:585
  68.8 0.3 multiply_reduce_fusion
  69.1 0.1 reduce_sum.31
  69.2 0.4 copy.40
  69.7 0.2 pad_maximum_fusion
  69.9 1.7 copy.41
  71.6 9.7 %all-to-all-start.2 = ((bf16[8,2,192,128]{3,2,1,0:T(8,128)(2,1)}), bf16[8,2,192,128]{3,2,1,0:T(8,128)(2,1)S(1)}, u32[]{:S(2)}, u32[]{:S(2)}) async-start(bf16[8,2,192,128]{3,2,1,0:T(8,128)(2,1)} %copy.41), calls=%async_computation.2 | async-start | bytes 1572864 | tf_op jit(solution)/shard_map/all_to_all | solution.py:588
  81.2 48.3 %attend.1 = bf16[16,192,128]{2,1,0:T(8,128)(2,1)} custom-call(f32[1]{0:T(128)} %dynamic_slice.12.offset_ref, f32[1,128]{1,0:T(1,128)S(1)} %pad_bitcast_fusion.gain_ref, bf16[16,288,128]{2,1,0:T(8,128)(2,1)S(1)} %copy-done.1, bf16[16,192,128]{2,1,0:T(8,128)(2,1)S(1)} %copy-done.2), custom_call_target="tpu_custom_call" | custom-call | flops 10000000000 | bytes 3000000 | tf_op jit(solution)/shard_map/attend/pallas_call | solution.py:518
  129.5 5.6 %all-to-all-start = ((bf16[16,192,128]{2,1,0:T(8,128)(2,1)}), bf16[16,192,128]{2,1,0:T(8,128)(2,1)S(1)}, u32[]{:S(2)}, u32[]{:S(2)}) async-start(bf16[16,192,128]{2,1,0:T(8,128)(2,1)} %attend.1), calls=%async_computation | async-start | bytes 1572864 | tf_op jit(solution)/shard_map/all_to_all | solution.py:575
  135.2 0.1 fusion.18
  135.3 13.7 %all-to-all-done = bf16[16,192,128]{2,1,0:T(8,128)(2,1)S(1)} async-done(((bf16[16,192,128]{2,1,0:T(8,128)(2,1)}), bf16[16,192,128]{2,1,0:T(8,128)(2,1)S(1)}, u32[]{:S(2)}, u32[]{:S(2)}) %all-to-all-start) | async-done | bytes 786464 | tf_op jit(solution)/shard_map/all_to_all | solution.py:575
  149.0 0.1 slice_bitcast_fusion.18
  149.0 0.1 maximum_bitcast_fusion
  149.1 0.1 maximum_bitcast_fusion.2
  149.2 1.0 pad_maximum_fusion.2
  150.1 4.0 %all-to-all-start.1 = ((bf16[4,4,192,128]{3,2,1,0:T(8,128)(2,1)}), bf16[4,4,192,128]{3,2,1,0:T(8,128)(2,1)S(1)}, u32[]{:S(2)}, u32[]{:S(2)}) async-start(bf16[4,4,192,128]{3,2,1,0:T(8,128)(2,1)} %pad_maximum_fusion.2), calls=%async_computation.1 | async-start | bytes 1572864 | tf_op jit(solution)/shard_map/all_to_all | solution.py:596
  154.1 0.6 fusion.13
  154.7 0.2 copy.43
  154.8 0.2 copy.42
  155.0 0.7 copy-done.4
  155.7 1.8 %fusion.21 = f32[192,2048]{1,0:T(8,128)} fusion(bf16[512,2048]{1,0:T(8,128)(2,1)S(1)} %copy-done.4, bf16[24,8,4,128]{3,2,1,0:T(4,128)(2,1)S(1)} %bitcast.106), kind=kOutput, calls=%fused_computation.38 | convolution fusion | flops 402653184 | bytes 3866624 | tf_op jit(solution)/shard_map/dot_general | solution.py:26
  157.5 6.6 %all-to-all-done.1 = bf16[4,4,192,128]{3,2,1,0:T(8,128)(2,1)S(1)} async-done(((bf16[4,4,192,128]{3,2,1,0:T(8,128)(2,1)}), bf16[4,4,192,128]{3,2,1,0:T(8,128)(2,1)S(1)}, u32[]{:S(2)}, u32[]{:S(2)}) %all-to-all-start.1) | async-done | bytes 786464 | tf_op jit(solution)/shard_map/all_to_all | solution.py:596
  164.1 0.1 slice_bitcast_fusion
  164.2 0.3 slice.192
  164.5 0.4 copy.45
  164.9 0.8 broadcast_select_fusion
  165.7 1.2 copy.39
  167.0 3.3 %collective-permute-start.2 = (f32[192,8]{0,1:T(8,128)S(1)}, f32[192,8]{0,1:T(8,128)S(1)}, u32[]{:S(2)}, u32[]{:S(2)}) collective-permute-start(f32[192,8]{0,1:T(8,128)S(1)} %select_n.117), channel_id=1, source_target_pairs={{0,1},{1,0},{2,3},{3,2},{4,5},{5,4},{6,7},{7,6},{8,9},{9,8},{10,11... | collective-permute-start | bytes 18440 | tf_op jit(solution)/shard_map/ppermute | solution.py:616
  170.3 0.2 copy.38
  170.5 0.6 fusion.33
  171.2 1.0 copy-done.7
  172.1 0.6 fusion.2
  172.8 0.8 copy-done.5
  173.5 0.7 copy-done.6
  174.2 1.6 fusion.4
  175.8 0.7 maximum_select_fusion
  (33 shorter events, 0.3 us)
Async XLA Ops:
  0.6 64.2 %copy-start = (f32[3,512]{1,0:T(4,128)S(1)}, f32[3,512]{1,0:T(4,128)}, u32[]{:S(2)}) copy-start(f32[3,512]{1,0:T(4,128)} %param.23) | copy-start | bytes 18436
  1.4 64.3 %collective-permute-start = (f32[520]{0:T(1024)S(1)}, f32[520]{0:T(1024)S(1)}, u32[]{:S(2)}, u32[]{:S(2)}) collective-permute-start(f32[520]{0:T(1024)S(1)} %pad_maximum_fusion.3), channel_id=1, source_target_pairs={{0,1},{1,0},{2,3},{3,2},{4,5},{5,4},{6,7},{7,6},{8,9},{9,8},{10,11... | collective-permute-start | bytes 6248 | tf_op jit(solution)/shard_map/ppermute | solution.py:568
  4.1 61.6 %copy-start.8 = (f32[512]{0:T(512)S(1)}, f32[512]{0:T(512)}, u32[]{:S(2)}) copy-start(f32[512]{0:T(512)} %param.24) | copy-start | bytes 6148
  4.1 61.6 %copy-start.9 = (f32[8]{0:T(128)S(1)}, f32[8]{0:T(128)}, u32[]{:S(2)}) copy-start(f32[8]{0:T(128)} %param.22) | copy-start | bytes 100
  58.9 7.5 %collective-permute-start.1 = (f32[4,2,128]{2,1,0:T(2,128)S(1)}, f32[4,2,128]{2,1,0:T(2,128)S(1)}, u32[]{:S(2)}, u32[]{:S(2)}) collective-permute-start(f32[4,2,128]{2,1,0:T(2,128)S(1)} %slice.159), channel_id=1, source_target_pairs={{0,8},{8,16},{16,24},{24,32},{32,40},{40,48},{48,56},{56,64},{64,7... | collective-permute-start | bytes 12296 | tf_op jit(solution)/shard_map/ppermute | solution.py:578
  69.9 11.4 %copy-start.1 = (bf16[16,288,128]{2,1,0:T(8,128)(2,1)S(1)}, bf16[16,288,128]{2,1,0:T(8,128)(2,1)}, u32[]{:S(2)}) copy-start(bf16[16,288,128]{2,1,0:T(8,128)(2,1)} %get-tuple-element.8.own_ref) | copy-start | bytes 3538948
  69.9 11.4 %copy-start.2 = (bf16[16,192,128]{2,1,0:T(8,128)(2,1)S(1)}, bf16[16,192,128]{2,1,0:T(8,128)(2,1)}, u32[]{:S(2)}) copy-start(bf16[16,192,128]{2,1,0:T(8,128)(2,1)} %get-tuple-element.9.mate_ref) | copy-start | bytes 2359300
  71.6 58.0 %all-to-all-start.2 = ((bf16[8,2,192,128]{3,2,1,0:T(8,128)(2,1)}), bf16[8,2,192,128]{3,2,1,0:T(8,128)(2,1)S(1)}, u32[]{:S(2)}, u32[]{:S(2)}) async-start(bf16[8,2,192,128]{3,2,1,0:T(8,128)(2,1)} %copy.41), calls=%async_computation.2 | async-start | bytes 1572864 | tf_op jit(solution)/shard_map/all_to_all | solution.py:588
  129.5 19.4 %all-to-all-start = ((bf16[16,192,128]{2,1,0:T(8,128)(2,1)}), bf16[16,192,128]{2,1,0:T(8,128)(2,1)S(1)}, u32[]{:S(2)}, u32[]{:S(2)}) async-start(bf16[16,192,128]{2,1,0:T(8,128)(2,1)} %attend.1), calls=%async_computation | async-start | bytes 1572864 | tf_op jit(solution)/shard_map/all_to_all | solution.py:575
  150.1 14.0 %all-to-all-start.1 = ((bf16[4,4,192,128]{3,2,1,0:T(8,128)(2,1)}), bf16[4,4,192,128]{3,2,1,0:T(8,128)(2,1)S(1)}, u32[]{:S(2)}, u32[]{:S(2)}) async-start(bf16[4,4,192,128]{3,2,1,0:T(8,128)(2,1)} %pad_maximum_fusion.2), calls=%async_computation.1 | async-start | bytes 1572864 | tf_op jit(solution)/shard_map/all_to_all | solution.py:596
  154.1 1.6 copy-start.4
  164.9 5.6 %copy-start.3 = (bf16[512,2048]{1,0:T(8,128)(2,1)S(1)}, bf16[512,2048]{1,0:T(8,128)(2,1)}, u32[]{:S(2)}) copy-start(bf16[512,2048]{1,0:T(8,128)(2,1)} %att_ref.1) | copy-start | bytes 6291460
  167.0 8.8 %collective-permute-start.2 = (f32[192,8]{0,1:T(8,128)S(1)}, f32[192,8]{0,1:T(8,128)S(1)}, u32[]{:S(2)}, u32[]{:S(2)}) collective-permute-start(f32[192,8]{0,1:T(8,128)S(1)} %select_n.117), channel_id=1, source_target_pairs={{0,1},{1,0},{2,3},{3,2},{4,5},{5,4},{6,7},{7,6},{8,9},{9,8},{10,11... | collective-permute-start | bytes 18440 | tf_op jit(solution)/shard_map/ppermute | solution.py:616
  170.5 1.6 copy-start.7
  172.1 1.4 copy-start.5
  172.1 2.1 %copy-start.6 = (bf16[512,2048]{1,0:T(8,128)(2,1)S(1)}, bf16[512,2048]{1,0:T(8,128)(2,1)}, u32[]{:S(2)}) copy-start(bf16[512,2048]{1,0:T(8,128)(2,1)} %get-tuple-element.13) | copy-start | bytes 6291460

commit v3 on v2

--- a/solution.py
+++ b/solution.py
@@ -47,7 +47,8 @@
 
 def front_kernel(
     tokens_ref,
-    gain_ref,
+    params_hbm,
+    params_ref,
     wq_ref,
     wk_ref,
     wv_ref,
@@ -58,8 +59,8 @@
     conv_ref,
     own_ref,
     mate_ref,
-    gated_ref,
-    outgate_ref,
+    branch_ref,
+    params_other_ref,
     att_other_ref,
     conv_other_ref,
     tok,
@@ -67,6 +68,10 @@
     msg,
     recv,
     mate,
+    gated,
+    outgate,
+    branch_out,
+    branch_in,
     local_sem,
     spread_send,
     spread_recv,
@@ -86,6 +91,10 @@
     mate_recv,
     other_send,
     other_recv,
+    halo_send,
+    halo_recv,
+    branch_send,
+    branch_recv,
 ):
     place, x, core = lax.axis_index("sp"), lax.axis_index("fs"), lax.axis_index("tp")
     y, z = lax.rem(place, 4), lax.div(place, 4)
@@ -231,6 +240,7 @@
     others = [
         remote(att_ref, att_other_ref, other_send.at[0], other_recv.at[0], sibling),
         remote(conv_ref, conv_other_ref, other_send.at[1], other_recv.at[1], sibling),
+        remote(params_hbm, params_other_ref, other_send.at[2], other_recv.at[2], sibling),
     ]
     for copy in own_weights:
         copy.wait()
@@ -244,6 +254,22 @@
         return remote(
             msg.at[at], recv.at[place], msg_send.at[at], msg_recv.at[place], (there, x, half)
         ), lax.abs(there - place) + lax.abs(half - core)
+
+    def halo(s):
+        return remote(
+            gated.at[s, ROWS : ROWS + 8],
+            gated.at[s, 0:8],
+            halo_send.at[s],
+            halo_recv.at[s],
+            (lax.rem(place + 1, BLOCKS), x, core),
+        )
+
+    def to_home(at):
+        s, half = lax.div(at, 2), lax.rem(at, 2)
+        mine = 2 * x + core
+        return remote(
+            branch_out.at[at], branch_in.at[mine], branch_send.at[at], branch_recv.at[mine], (place, s, half)
+        ), lax.abs(s - x) + lax.abs(half - core)
 
     def step(i, _):
         s = mod4(x + i + lax.div(i, 2) - 2 * lax.div(i, 3))
@@ -282,8 +308,8 @@
         high = tok[s, 1].astype(F32)
         squares = jnp.sum(low * low, axis=1, keepdims=True) + jnp.sum(high * high, axis=1, keepdims=True)
         scale = lax.rsqrt(squares / D + epsilon)
-        total = dot((low * gain_ref[0:1, :]).astype(BF16), wts[0:2].reshape(1024, 768)) + dot(
-            (high * gain_ref[1:2, :]).astype(BF16), wts[2:4].reshape(1024, 768)
+        total = dot((low * params_ref[0:1, :]).astype(BF16), wts[0:2].reshape(1024, 768)) + dot(
+            (high * params_ref[1:2, :]).astype(BF16), wts[2:4].reshape(1024, 768)
         )
         out = (total * scale).astype(BF16)
         query, key, value = out[:, 0:128], out[:, 128:256], out[:, 256:384]
@@ -295,8 +321,17 @@
                 folded = jnp.concatenate((query[r : r + 96, mine], query[r + 96 : r + HALF, mine]), axis=1)
                 msg[4 * s + 2 * j + half, 0:HALF, :] = both[r : r + HALF]
                 msg[4 * s + 2 * j + half, HALF : HALF + 96, :] = folded
-        outgate_ref[s] = out[:, 384:512]
-        gated_ref[s] = out[:, 512:640].astype(F32) * out[:, 640:768].astype(F32)
+        outgate[s] = out[:, 384:512]
+        gated[s, 8 : ROWS + 8, :] = out[:, 512:640].astype(F32) * out[:, 640:768].astype(F32)
+
+        @pl.when(place < BLOCKS - 1)
+        def _():
+            halo(s).start()
+
+        @pl.when(place == 0)
+        def _():
+            gated[s, 0:8, :] = jnp.zeros((8, 128), F32)
+
         for j in range(2):
             for half in range(2):
                 copy, apart = message(s, j, half)
@@ -312,6 +347,34 @@
         return 0
 
     lax.fori_loop(0, 4, step, 0)
+
+    columns = pl.ds(pl.multiple_of(x * 128, 128), 128)
+
+    def convolve(s, _):
+        @pl.when(place > 0)
+        def _():
+            halo(s).wait_recv()
+
+        convolved = sum(
+            params_ref[4 + t : 5 + t, columns] * gated[s, 6 + t : 6 + t + ROWS, :] for t in range(3)
+        )
+        branch = (outgate[s].astype(F32) * convolved).astype(BF16)
+        branch_out[2 * s] = branch[0:HALF]
+        branch_out[2 * s + 1] = branch[HALF:ROWS]
+        for half in range(2):
+            copy, apart = to_home(2 * s + half)
+
+            @pl.when(apart > 0)
+            def _():
+                copy.start()
+
+            @pl.when(apart == 0)
+            def _():
+                branch_in[2 * x + core] = branch[half * HALF : (half + 1) * HALF]
+
+        return 0
+
+    lax.fori_loop(0, SEQS, convolve, 0)
 
     def to_mate(block):
         return remote(
@@ -341,6 +404,21 @@
         return 0
 
     lax.fori_loop(0, BLOCKS, arrived, 0)
+
+    def branch_arrived(k, _):
+        there = lax.rem(2 * x + core + k, 8)
+        remote(
+            branch_out.at[0],
+            branch_in.at[there],
+            branch_send.at[0],
+            branch_recv.at[there],
+            (place, lax.div(there, 2), lax.rem(there, 2)),
+        ).wait_recv()
+        return 0
+
+    lax.fori_loop(1, 8, branch_arrived, 0)
+    home_out = pltpu.make_async_copy(branch_in, branch_ref, local_sem.at[2])
+    home_out.start()
     mate_out = pltpu.make_async_copy(mate, mate_ref, local_sem.at[1])
     mate_out.start()
 
@@ -369,25 +447,43 @@
         return 0
 
     lax.fori_loop(0, BLOCKS, left_here, 0)
+
+    def branch_left(at, _):
+        copy, apart = to_home(at)
+
+        @pl.when(apart > 0)
+        def _():
+            copy.wait_send()
+
+        return 0
+
+    lax.fori_loop(0, 8, branch_left, 0)
+
+    @pl.when(place < BLOCKS - 1)
+    def _():
+        for s in range(SEQS):
+            halo(s).wait_send()
+
+    home_out.wait()
     own_out.wait()
     mate_out.wait()
     for copy in others:
         copy.wait()
 
 
-def front(tokens, gains, mats, out_att, out_conv):
+def front(tokens, params, mats, out_att, out_conv):
     hbm = pl.BlockSpec(memory_space=pl.ANY)
     vmem = pl.BlockSpec(memory_space=pltpu.VMEM)
     dma = lambda *shape: pltpu.SemaphoreType.DMA(shape)
     return pl.pallas_call(
         front_kernel,
-        in_specs=[hbm, vmem] + [hbm] * 8,
-        out_specs=[hbm, hbm, vmem, vmem, hbm, hbm],
+        in_specs=[hbm, hbm, vmem] + [hbm] * 8,
+        out_specs=[hbm] * 6,
         out_shape=[
             jax.ShapeDtypeStruct((BLOCKS, MESSAGE, 128), BF16),
             jax.ShapeDtypeStruct((BLOCKS, HALF, 128), BF16),
-            jax.ShapeDtypeStruct((SEQS, ROWS, 128), F32),
-            jax.ShapeDtypeStruct((SEQS, ROWS, 128), BF16),
+            jax.ShapeDtypeStruct((8, HALF, 128), BF16),
+            jax.ShapeDtypeStruct(params.shape, F32),
             jax.ShapeDtypeStruct(out_att.shape, BF16),
             jax.ShapeDtypeStruct(out_conv.shape, BF16),
         ],
@@ -397,6 +493,10 @@
             pltpu.VMEM((BLOCKS, MESSAGE, 128), BF16),
             pltpu.VMEM((BLOCKS, MESSAGE, 128), BF16),
             pltpu.VMEM((BLOCKS, HALF, 128), BF16),
+            pltpu.VMEM((SEQS, ROWS + 8, 128), F32),
+            pltpu.VMEM((SEQS, ROWS, 128), BF16),
+            pltpu.VMEM((8, HALF, 128), BF16),
+            pltpu.VMEM((8, HALF, 128), BF16),
             dma(31),
             dma(3, 6), dma(3, 6),
             dma(18), dma(18),
@@ -406,19 +506,104 @@
             dma(8), dma(8),
             dma(16), dma(16),
             dma(16), dma(16),
-            dma(2), dma(2),
+            dma(3), dma(3),
+            dma(4), dma(4),
+            dma(8), dma(8),
         ],
         compiler_params=pltpu.CompilerParams(
             collective_id=0, has_side_effects=True, vmem_limit_bytes=56 << 20
         ),
         name="front",
-    )(tokens, gains, *mats, out_att, out_conv)
+    )(tokens, params, params, *mats, out_att, out_conv)
 
 
 def attend_kernel(
-    offset_ref, gain_ref, own_ref, mate_ref, out_ref, keys, values, queries, scores, decays, weights, total
+    offset_ref,
+    own_ref,
+    mate_ref,
+    branch_ref,
+    gain_ref,
+    gain_other_ref,
+    att_ref,
+    att_other_ref,
+    conv_ref,
+    conv_other_ref,
+    mixed_ref,
+    mass_ref,
+    keys,
+    values,
+    queries,
+    scores,
+    decays,
+    weights,
+    total,
+    att_out,
+    att_in,
+    mass_out,
+    mass_in,
+    att_weights,
+    conv_weights,
+    matrix,
+    gains,
+    att_send,
+    att_recv,
+    mass_send,
+    mass_recv,
+    local_sem,
 ):
-    half = lax.axis_index("tp")
+    place, x, half = lax.axis_index("sp"), lax.axis_index("fs"), lax.axis_index("tp")
+    number, row = lax.rem(place, 4), lax.div(place, 4)
+    seq = mod4(row - number)
+
+    barrier = pltpu.get_barrier_semaphore()
+
+    def greet(k, _):
+        n = lax.rem(k, 4)
+        there, column = mod4(x + n) * 4 + n, lax.div(k, 4)
+        for core in range(2):
+            @pl.when(lax.abs(there - place) + lax.abs(column - x) + lax.abs(core - half) > 0)
+            def _():
+                pl.semaphore_signal(barrier, inc=1, device_id=(there, column, core), device_id_type=MESH)
+
+        return 0
+
+    lax.fori_loop(0, 16, greet, 0)
+    fetches = [
+        pltpu.make_async_copy(src, dst, local_sem.at[i])
+        for i, (src, dst) in enumerate(
+            [
+                (att_ref, att_weights.at[half]),
+                (att_other_ref, att_weights.at[1 - half]),
+                (conv_ref, conv_weights.at[half]),
+                (conv_other_ref, conv_weights.at[1 - half]),
+                (gain_ref, gains.at[half]),
+                (gain_other_ref, gains.at[1 - half]),
+            ]
+        )
+    ]
+    for copy in fetches:
+        copy.start()
+
+    def remote(src, dst, send, recv, device):
+        return pltpu.make_async_remote_copy(
+            src_ref=src, dst_ref=dst, send_sem=send, recv_sem=recv, device_id=device, device_id_type=MESH
+        )
+
+    def att_home(block):
+        at = 4 * x + number
+        apart = lax.abs(block - place) + lax.abs(seq - x)
+        return remote(
+            att_out.at[block], att_in.at[at], att_send.at[block], att_recv.at[at], (block, seq, half)
+        ), apart
+
+    def mass_home(block):
+        at = 4 * x + 2 * lax.rem(number, 2) + half
+        core = lax.div(number, 2)
+        apart = lax.abs(block - place) + lax.abs(seq - x) + lax.abs(core - half)
+        return remote(
+            mass_out.at[block], mass_in.at[at], mass_send.at[block], mass_recv.at[at], (block, seq, core)
+        ), apart
+
     lanes = lambda shape: lax.broadcasted_iota(jnp.int32, shape, 1)
     rows = lambda shape: lax.broadcasted_iota(jnp.int32, shape, 0)
     offset = jnp.full((HALF, 128), offset_ref[0] * LOG2E, F32)
@@ -449,6 +634,8 @@
         queries[block // 2, at, 0:128] = jnp.where(lane_q < HD, q_high, q - q_high).astype(BF16)
         queries[block // 2, at, 128:256] = offset_row
 
+    pl.semaphore_wait(barrier, 31 + lax.min(lax.abs(seq - x), 1))
+
     sub = rows((8, ROWS))
     lane = lanes((8, ROWS))
     where_q = lane + half * HALF + jnp.where(lane < HALF, 0, HALF)
@@ -483,11 +670,8 @@
         total[...] += dot(values[block], w_ref[...])
         return carry + jnp.broadcast_to(suffix[0:1], (8, ROWS))
 
-    gain = gain_ref[...]
-    gain_lane = lanes((8, 512))
-    out_lane = lanes((ROWS, 128))
-
-    def one_tile(m, _):
+    def one_tile(step, _):
+        m = BLOCKS // 2 - 1 - step
         total[...] = jnp.zeros_like(total)
         carry = jnp.zeros((8, ROWS), F32)
         carry = tile(m, 2 * m + 1, carry, where_q - ROWS - 48 * sub, 0)
@@ -500,26 +684,129 @@
 
         carry = lax.fori_loop(0, m, before, carry)
         attended = total[...]
-        squares = jnp.sum(attended * attended, axis=0, keepdims=True)
-        parts = [p.astype(F32) for p in three_parts(carry[0:1]) + three_parts(squares)]
-        side = jnp.concatenate(parts + [jnp.zeros((HD - 6, ROWS), F32)], axis=0)
-        message = jnp.concatenate((attended, side), axis=0).T
-        message = message * jnp.where(out_lane < HD, gain, 1.0)
-        message = message.astype(BF16)
-        out_ref[2 * m] = message[0:HALF]
-        out_ref[2 * m + 1] = message[HALF:ROWS]
+        attended = jnp.concatenate((attended, attended), axis=0).T
+        for part in range(2):
+            block = 2 * m + part
+            r = part * HALF
+            folded = jnp.where(lanes((96, 128)) < HD, attended[r : r + 96], attended[r + 96 : r + HALF])
+            folded = folded.astype(BF16)
+            mass = carry[:, r : r + HALF]
+            att_out[block] = folded
+            mass_out[block, :, 0:HALF] = mass
+            copy, apart = att_home(block)
+
+            @pl.when(apart > 0)
+            def _():
+                copy.start()
+
+            @pl.when(apart == 0)
+            def _():
+                att_in[4 * x + number] = folded
+
+            mass_copy, mass_apart = mass_home(block)
+
+            @pl.when(mass_apart > 0)
+            def _():
+                mass_copy.start()
+
+            @pl.when(mass_apart == 0)
+            def _():
+                mass_in[4 * x + 2 * lax.rem(number, 2) + half, :, 0:HALF] = mass
+
         return 0
 
     lax.fori_loop(0, BLOCKS // 2, one_tile, 0)
 
-
-def attend(own, mate, offset, gain):
+    for copy in fetches:
+        copy.wait()
+
+    def branch_product(store, row_gain, projection, load):
+        squares = jnp.zeros((HALF, 128), F32)
+        for core in range(2):
+            for part in range(4):
+                piece = load(core, part)
+                squares = squares + piece * piece
+                gain = gains[core, 2:3, row_gain + 128 * part : row_gain + 128 * part + 128]
+                at = 512 * core + 128 * part
+                store[:, at : at + 128] = (piece * gain).astype(BF16)
+        scale = lax.rsqrt(jnp.sum(squares, axis=1, keepdims=True) / ATT_WIDTH + epsilon)
+        return scale * dot(store[...], projection[...].reshape(1024, D))
+
+    mixed = branch_product(
+        matrix.at[0], 512, conv_weights, lambda core, part: branch_ref[2 * part + core].astype(F32)
+    )
+
+    def landed(at, _):
+        column, n = lax.div(at, 4), lax.rem(at, 4)
+        there = mod4(x + n) * 4 + n
+        apart = lax.abs(there - place) + lax.abs(column - x)
+
+        @pl.when(apart > 0)
+        def _():
+            remote(
+                att_out.at[0], att_in.at[at], att_send.at[0], att_recv.at[at], (there, column, half)
+            ).wait_recv()
+
+        n = 2 * half + lax.div(n, 2)
+        core = lax.rem(at, 2)
+        there = mod4(x + n) * 4 + n
+        apart = lax.abs(there - place) + lax.abs(column - x) + lax.abs(core - half)
+
+        @pl.when(apart > 0)
+        def _():
+            remote(
+                mass_out.at[0], mass_in.at[at], mass_send.at[0], mass_recv.at[at], (there, column, core)
+            ).wait_recv()
+
+        return 0
+
+    lax.fori_loop(0, 16, landed, 0)
+
+    def heads(core, part):
+        a = att_in[4 * part + 2 * core].astype(F32)
+        b = att_in[4 * part + 2 * core + 1].astype(F32)
+        low = lanes((96, 128)) < HD
+        upper = jnp.where(low, a, pltpu.roll(b, HD, 1))
+        lower = jnp.where(low, pltpu.roll(a, HD, 1), b)
+        return jnp.concatenate((upper, lower), axis=0)
+
+    mixed = mixed + branch_product(matrix.at[1], 0, att_weights, heads)
+    mixed_ref[0] = mixed.astype(BF16)
+    for part in range(2):
+        kept = jnp.concatenate([mass_in[2 * n + part, 0:1, :] for n in range(8)], axis=0)
+        mass = jnp.log(2.0 - jnp.exp2(-kept)).T
+        mass_ref[0, part * HALF : (part + 1) * HALF, :] = mass[0:HALF]
+
+    def left(block, _):
+        copy, apart = att_home(block)
+
+        @pl.when(apart > 0)
+        def _():
+            copy.wait_send()
+
+        mass_copy, mass_apart = mass_home(block)
+
+        @pl.when(mass_apart > 0)
+        def _():
+            mass_copy.wait_send()
+
+        return 0
+
+    lax.fori_loop(0, BLOCKS, left, 0)
+
+
+def attend(offset, own, mate, branch, params, params_other, att, att_other, conv, conv_other):
     whole = pl.BlockSpec(memory_space=pltpu.VMEM)
+    hbm = pl.BlockSpec(memory_space=pl.ANY)
+    dma = lambda *shape: pltpu.SemaphoreType.DMA(shape)
     return pl.pallas_call(
         attend_kernel,
-        in_specs=[pl.BlockSpec(memory_space=pltpu.SMEM), whole, whole, whole],
-        out_specs=whole,
-        out_shape=jax.ShapeDtypeStruct((BLOCKS, HALF, 128), BF16),
+        in_specs=[pl.BlockSpec(memory_space=pltpu.SMEM), whole, whole, whole] + [hbm] * 6,
+        out_specs=[whole, whole],
+        out_shape=[
+            jax.ShapeDtypeStruct((1, HALF, D), BF16),
+            jax.ShapeDtypeStruct((1, ROWS, 8), F32),
+        ],
         scratch_shapes=[
             pltpu.VMEM((BLOCKS * ROWS, 256), BF16),
             pltpu.VMEM((BLOCKS, HD, ROWS), BF16),
@@ -528,13 +815,21 @@
             pltpu.VMEM((2, ROWS, ROWS), F32),
             pltpu.VMEM((2, ROWS, ROWS), BF16),
             pltpu.VMEM((HD, ROWS), F32),
+            pltpu.VMEM((BLOCKS, 96, 128), BF16),
+            pltpu.VMEM((BLOCKS, 96, 128), BF16),
+            pltpu.VMEM((BLOCKS, 8, 256), F32),
+            pltpu.VMEM((BLOCKS, 8, 256), F32),
+            pltpu.VMEM((2, 512, D), BF16),
+            pltpu.VMEM((2, 512, D), BF16),
+            pltpu.VMEM((2, HALF, 1024), BF16),
+            pltpu.VMEM((2, 8, 1024), F32),
+            dma(16), dma(16), dma(16), dma(16), dma(6),
         ],
-        compiler_params=pltpu.CompilerParams(vmem_limit_bytes=48 << 20),
-        cost_estimate=pl.CostEstimate(
-            flops=10_000_000_000, bytes_accessed=3_000_000, transcendentals=30_000_000
+        compiler_params=pltpu.CompilerParams(
+            collective_id=1, has_side_effects=True, vmem_limit_bytes=56 << 20
         ),
         name="attend",
-    )(offset, gain, own, mate)
+    )(offset, own, mate, branch, params, params_other, att, att_other, conv, conv_other)
 
 
 def per_device(
@@ -553,74 +848,28 @@
     out_att,
     out_conv,
 ):
-    place = lax.axis_index("sp")
-    column = lax.axis_index("fs")
-    core = lax.axis_index("tp")
-    own, mate, gated, outgate, att_other, conv_other = front(
-        tokens[0],
-        in_gain.reshape(2, 1024),
-        (w_query, w_key, w_value, w_outgate, w_ingate, w_conv_in),
-        out_att,
-        out_conv,
+    wide = lambda a: jnp.pad(a, ((0, 0), (0, 1024 - a.shape[1])))
+    params = jnp.concatenate(
+        (
+            in_gain.reshape(2, 1024),
+            jnp.concatenate((att_gain, conv_gain))[None],
+            wide(score_offset[None]),
+            wide(conv_taps),
+            jnp.zeros((1, 1024), F32),
+        ),
+        axis=0,
     )
-
-    number = lax.rem(place, 4)
-    both_cores = lax.ppermute(jnp.concatenate((score_offset, att_gain)), "tp", [(0, 1), (1, 0)])
-    mine = jnp.where(number // 2 == core, jnp.concatenate((score_offset, att_gain)), both_cores)
-    local_head = 2 * column + lax.rem(number, 2)
-    offset = lax.dynamic_slice_in_dim(mine, local_head, 1, 0)
-    gain = lax.dynamic_slice_in_dim(mine, 8 + local_head * HD, HD, 0)
-    gain = jnp.concatenate((gain, jnp.ones((HD,), F32)))[None]
-    sent = attend(own, mate, offset, gain)
-    back = lax.all_to_all(sent, "sp", 0, 0, tiled=True)
-
-    pairs = [(i, i + 1) for i in range(BLOCKS - 1)]
-    before = lax.ppermute(gated[:, ROWS - 2 :], "sp", pairs)
-    extended = jnp.concatenate((before, gated), axis=1)
-    taps = lax.dynamic_slice_in_dim(conv_taps, column * 128, 128, 1)
-    convolved = sum(taps[j] * extended[:, j : j + ROWS] for j in range(3))
-    conv_out = outgate.astype(F32) * convolved
-    conv_squares = jnp.sum(conv_out * conv_out, axis=2, keepdims=True)
-    conv_mine = lax.dynamic_slice_in_dim(conv_gain, column * 128, 128, 0)
-    conv_scaled = (conv_out * conv_mine).astype(BF16).reshape(8, HALF, 128)
-    pieces = jnp.concatenate(three_parts(conv_squares), axis=2).reshape(8, HALF, 3)
-    pieces = jnp.concatenate((pieces, jnp.zeros((8, HALF, 125), BF16)), axis=2)
-    conv_home = lax.all_to_all(
-        jnp.stack((conv_scaled, pieces), axis=1), ("fs", "tp"), 0, 0, tiled=True
-    ).reshape(4, 2, 2, HALF, 128)
-
-    by_head = back.reshape(4, 4, HALF, 128)
-    ordered = jnp.stack(
-        [jnp.stack([by_head[(s + n) % 4, n] for n in range(4)]) for s in range(SEQS)]
+    own, mate, branch, params_other, att_other, conv_other = front(
+        tokens[0], params, (w_query, w_key, w_value, w_outgate, w_ingate, w_conv_in), out_att, out_conv
     )
-    home = lax.all_to_all(ordered, "fs", 0, 0, tiled=True)
-    home = home.reshape(4, 2, 2, HALF, 128)
-    extra = home[..., HD : HD + 6].astype(F32)
-    kept = extra[..., 0] + extra[..., 1] + extra[..., 2]
-    att_sum = jnp.sum(extra[..., 3] + extra[..., 4] + extra[..., 5], axis=(0, 1, 2))
-    conv_extra = conv_home[:, :, 1, :, 0:3].astype(F32)
-    conv_sum = jnp.sum(conv_extra[..., 0] + conv_extra[..., 1] + conv_extra[..., 2], axis=(0, 1))
-    att_scale = lax.rsqrt(att_sum / ATT_WIDTH + epsilon)
-    conv_scale = lax.rsqrt(conv_sum / CONV_CH + epsilon)
-    att_mat = home[..., :HD].transpose(1, 3, 0, 2, 4).reshape(2, HALF, 512)
-    conv_mat = conv_home[:, :, 0].transpose(1, 2, 0, 3).reshape(2, HALF, 512)
-    first = core == 0
-    near = lambda a: jnp.where(first, a[0], a[1])
-    far = lambda a: jnp.where(first, a[1], a[0])
-    att_product = dot(near(att_mat), out_att) + dot(far(att_mat), att_other)
-    conv_product = dot(near(conv_mat), out_conv) + dot(far(conv_mat), conv_other)
-    mixed = att_scale[:, None] * att_product + conv_scale[:, None] * conv_product
-
-    log_mass = jnp.log(2.0 - jnp.exp2(-kept))
-    by_core = log_mass.transpose(1, 3, 0, 2).reshape(2, HALF, 8)
-    far_rows = lax.ppermute(far(by_core), "tp", [(0, 1), (1, 0)])
-    near_rows = near(by_core)
-    log_mass = jnp.where(
-        first,
-        jnp.concatenate((near_rows, far_rows), axis=0),
-        jnp.concatenate((far_rows, near_rows), axis=0),
+    number = lax.rem(lax.axis_index("sp"), 4)
+    offsets = jnp.where(number // 2 == lax.axis_index("tp"), score_offset, params_other[3, :8])
+    offset = lax.dynamic_slice_in_dim(offsets, 2 * lax.axis_index("fs") + lax.rem(number, 2), 1, 0)
+    return tuple(
+        attend(
+            offset, own, mate, branch, params, params_other, out_att, att_other, out_conv, conv_other
+        )
     )
-    return (mixed.astype(BF16)[None], log_mass[None])
 
 
 def solution(mesh):

time: 177 us -> 134 us (0.76)
  starting transfers between devices: 29.8 us -> 0 us
  Pallas kernels: 102 us -> 124 us
  waiting for transfers between devices: 20.4 us -> 0 us
  other arithmetic: 7.07 us -> 1.39 us
  matrix products: 4.58 us -> 0 us
  local copies, waits for them, and re-layouts: 11.3 us -> 7.02 us
    pallas_call x1, Pallas kernels: 48.3 us -> 69.8 us  [attend(): pl.pallas_call(attend_kernel, in_specs=[pl.BlockSpec(memory_space=pltpu.S...]
    all_to_all x3 -> x0, waiting for transfers between devices: 20.4 us -> none  [the longest x1 13.7 us: per_device(): back = lax.all_to_all(sent, 'sp', 0, 0, tiled=True)]
    all_to_all x3 -> x0, starting transfers between devices: 19.2 us -> none  [the longest x1 9.67 us: per_device(): lax.all_to_all(jnp.stack((conv_scaled, pieces), axis=1), ('fs', 'tp'), 0,...]
    ppermute x3 -> x0, starting transfers between devices: 10.6 us -> none  [the longest x1 5.93 us: per_device(): before = lax.ppermute(gated[:, ROWS - 2:], 'sp', pairs)]
    dot_general x4 -> x0, matrix products: 4.58 us -> none  [dot(): return jnp.dot(a, b, preferred_element_type=F32)]
    convert_element_type x4 -> x0, other arithmetic: 2.48 us -> none  [the longest x1 2.41 us: per_device(): conv_scaled = (conv_out * conv_mine).astype(BF16).reshape(8, HALF, 128)]
    another operation x3 -> x0, local copies, waits for them, and re-layouts: 2.13 us -> none  [the longest x2 2.08 us: per_device(): jnp.stack((conv_scaled, pieces), axis=1)]
    unnamed x21 -> x3, local copies, waits for them, and re-layouts: 3.54 us -> 2.09 us
  transfers between devices with their start and end apart: 6 -> 0, of which waited for: 2 -> 0; matrix products, arithmetic and copies ran while one was open for 5% -> 0% of each run, Pallas kernels for 58% -> 0%
where the time goes in v3:
time: 134 us
  Pallas kernels  124 us (93%)
  local copies, waits for them, and re-layouts  7.02 us (5%)
  other arithmetic  1.39 us (1%)
    pallas_call x1, Pallas kernels, attend(): pl.pallas_call(attend_kernel, in_specs=[pl.BlockSpec(memory_space=pltpu.S...  69.8 us
    pallas_call x1, Pallas kernels, front(): pl.pallas_call(front_kernel, in_specs=[hbm, hbm, vmem] + [hbm] * 8, out_s...  54.6 us

profile of v3, /device:TPU:1, one launch (start us, length us, event | category | flops | bytes accessed | tf_op | source)
XLA Modules:
  0.0 133.6 jit_solution(9699977161295272019)
XLA Ops:
  0.7 0.7 pad_maximum_fusion
  1.4 0.7 pad.8
  2.0 0.7 reshape.7
  2.7 0.7 pad.9
  3.4 0.6 concatenate.7.params_hbm.params_ref.gain_ref
  4.1 0.0 copy-start
  4.1 54.6 %front.1 = (bf16[16,288,128]{2,1,0:T(8,128)(2,1)}, bf16[16,192,128]{2,1,0:T(8,128)(2,1)}, bf16[8,192,128]{2,1,0:T(8,128)(2,1)}, f32[8,1024]{1,0:T(8,128)}, bf16[...) custom-call(bf16[384,1024]{1,0:T(8,128)(2,1)} %bitcast.5, f32[8,1024]{1,0:T(8,128)} %concatenate.7.params_hbm.params_ref.gain_ref, ...), custom_call_target="tpu_custom_call" | custom-call | tf_op jit(solution)/shard_map/front/pallas_call | solution.py:478
  58.7 0.0 copy-done
  58.7 0.7 broadcast_select_fusion
  59.4 0.6 dynamic_slice.3.offset_ref
  60.0 69.8 %attend.1 = (bf16[1,192,2048]{2,1,0:T(8,128)(2,1)}, f32[1,384,8]{2,1,0:T(8,128)}) custom-call(f32[1]{0:T(128)} %dynamic_slice.3.offset_ref, bf16[16,288,128]{2,1,0:T(8,128)(2,1)} %get-tuple-element.9.own_ref, bf16[16,192,128]{2,1,0:T(8,128)(2,1)} %get-tuple-element.10.mate_ref, bf16[8,192,128]{2,1,0:T(8,128)(2,1)} %get-tuple-element.11.branch_ref, ...), custom_call_target="tpu_custom_call" | custom-call | tf_op jit(solution)/shard_map/attend/pallas_call | solution.py:802
  129.8 1.6 %copy.16 = f32[1,384,8]{1,2,0:T(8,128)} copy(f32[1,384,8]{2,1,0:T(8,128)} %get-tuple-element.15) | data formatting | bytes 24576 | tf_op jit(solution)/shard_map/attend/pallas_call | solution.py:802
  131.5 2.1 %copy.18 = bf16[1,192,2048]{2,1,0:T(8,128)(2,1)} copy(bf16[1,192,2048]{2,1,0:T(8,128)(2,1)} %get-tuple-element.18) | data formatting | bytes 1572864
  (1 shorter events, 0.0 us)
Async XLA Ops:
  4.1 54.6 %copy-start = (f32[8]{0:T(128)S(1)}, f32[8]{0:T(128)}, u32[]{:S(2)}) copy-start(f32[8]{0:T(128)} %param.22) | copy-start | bytes 100

commit v4 on v3

--- a/solution.py
+++ b/solution.py
@@ -311,8 +311,9 @@
         total = dot((low * params_ref[0:1, :]).astype(BF16), wts[0:2].reshape(1024, 768)) + dot(
             (high * params_ref[1:2, :]).astype(BF16), wts[2:4].reshape(1024, 768)
         )
-        out = (total * scale).astype(BF16)
-        query, key, value = out[:, 0:128], out[:, 128:256], out[:, 256:384]
+        out = (total[:, 128:] * scale).astype(BF16)
+        key, value = out[:, 0:128], out[:, 128:256]
+        query = (total[:, 0:128] * (scale * (LOG2E / 8))).astype(BF16)
         for j in range(2):
             mine = slice(j * HD, (j + 1) * HD)
             both = jnp.concatenate((key[:, mine], value[:, mine]), axis=1)
@@ -321,8 +322,8 @@
                 folded = jnp.concatenate((query[r : r + 96, mine], query[r + 96 : r + HALF, mine]), axis=1)
                 msg[4 * s + 2 * j + half, 0:HALF, :] = both[r : r + HALF]
                 msg[4 * s + 2 * j + half, HALF : HALF + 96, :] = folded
-        outgate[s] = out[:, 384:512]
-        gated[s, 8 : ROWS + 8, :] = out[:, 512:640].astype(F32) * out[:, 640:768].astype(F32)
+        outgate[s] = out[:, 256:384]
+        gated[s, 8 : ROWS + 8, :] = out[:, 384:512].astype(F32) * out[:, 512:640].astype(F32)
 
         @pl.when(place < BLOCKS - 1)
         def _():
@@ -533,9 +534,12 @@
     keys,
     values,
     queries,
-    scores,
-    decays,
-    weights,
+    score_a,
+    score_b,
+    decay_a,
+    decay_b,
+    weight_a,
+    weight_b,
     total,
     att_out,
     att_in,
@@ -616,23 +620,22 @@
     source = lax.rem(rows(square), 8) * 48 + rows(square) // 8 - lanes(square)
     permute_own = (source == half * HALF).astype(F32).astype(BF16)
     permute_mate = (source == HALF - half * HALF).astype(F32).astype(BF16)
-    shape = (128, 128)
-    twice_low = (rows(shape) == lax.rem(lanes(shape), HD)).astype(F32).astype(BF16)
-    twice_high = (rows(shape) == lax.rem(lanes(shape), HD) + HD).astype(F32).astype(BF16)
     take_high = (lanes((HD, 128)) == rows((HD, 128)) + HD).astype(F32).astype(BF16)
     ones = (lanes((ROWS, 128)) < 3).astype(F32).astype(BF16)
+    low_lane = lanes((96, 128)) < HD
     for block in range(BLOCKS):
         pair = dot(permute_own, own_ref[block, 0:HALF, :]) + dot(permute_mate, mate_ref[block])
         pair = pair.astype(BF16)
-        keys[block * ROWS : (block + 1) * ROWS, 0:128] = dot(pair, twice_low).astype(BF16)
+        keys[block * ROWS : (block + 1) * ROWS, 0:128] = pair
         keys[block * ROWS : (block + 1) * ROWS, 128:256] = ones
         values[block] = dot_nt(take_high, pair).astype(BF16)
-        packed = own_ref[block, HALF:MESSAGE, :]
-        q = jnp.concatenate((dot(packed, twice_low), dot(packed, twice_high)), axis=0) * (LOG2E / 8)
-        q_high = q.astype(BF16).astype(F32)
-        at = slice((block % 2) * HALF, (block % 2 + 1) * HALF)
-        queries[block // 2, at, 0:128] = jnp.where(lane_q < HD, q_high, q - q_high).astype(BF16)
-        queries[block // 2, at, 128:256] = offset_row
+        packed = own_ref[block, HALF:MESSAGE, :].astype(F32)
+        at = (block % 2) * HALF
+        queries[block // 2, at : at + 96, 0:128] = jnp.where(low_lane, packed, 0.0).astype(BF16)
+        queries[block // 2, at + 96 : at + HALF, 0:128] = jnp.where(
+            low_lane, pltpu.roll(packed, HD, 1), 0.0
+        ).astype(BF16)
+        queries[block // 2, at : at + HALF, 128:256] = offset_row
 
     pl.semaphore_wait(barrier, 31 + lax.min(lax.abs(seq - x), 1))
 
@@ -640,22 +643,29 @@
     lane = lanes((8, ROWS))
     where_q = lane + half * HALF + jnp.where(lane < HALF, 0, HALF)
 
-    def tile(tile_index, block, carry, ahead, slot):
+    def score(z_ref, tile_index, block):
         begin = pl.multiple_of(block * ROWS, ROWS)
-        z_ref, d_ref, w_ref = scores.at[slot], decays.at[slot], weights.at[slot]
         z_ref[...] = dot_nt(keys[pl.ds(begin, ROWS), :], queries[tile_index])
+
+    def fold(w_ref, block):
+        total[...] += dot(values[block], w_ref[...])
+
+    def decay(z_ref, d_ref, ahead):
         run = jnp.zeros((8, ROWS), F32)
         for r in reversed(range(48)):
             z = z_ref[8 * r : 8 * r + 8, :]
-            soft = jnp.maximum(z, jnp.log2(1.0 + jnp.exp2(jnp.minimum(z, 126.0))))
+            soft = jnp.maximum(z, lax.log2(1.0 + jnp.exp2(jnp.minimum(z, 126.0))))
             if ahead is not None:
                 valid = ahead > r
                 soft = jnp.where(valid, soft, 0.0)
             run = run + soft
-            decay = jnp.exp2(z - run)
+            value = jnp.exp2(z - run)
             if ahead is not None:
-                decay = jnp.where(valid, decay, 0.0)
-            d_ref[8 * r : 8 * r + 8, :] = decay
+                value = jnp.where(valid, value, 0.0)
+            d_ref[8 * r : 8 * r + 8, :] = value
+        return run
+
+    def weigh(d_ref, w_ref, run, carry):
         suffix = run
         for step in (1, 2, 4):
             moved = pltpu.roll(suffix, 8 - step, 0)
@@ -667,22 +677,39 @@
                 (d_ref[16 * i : 16 * i + 8, :] * kept, d_ref[16 * i + 8 : 16 * i + 16, :] * kept), axis=0
             )
             w_ref[16 * i : 16 * i + 16, :] = both.astype(BF16)
-        total[...] += dot(values[block], w_ref[...])
         return carry + jnp.broadcast_to(suffix[0:1], (8, ROWS))
 
+    def two_blocks(tile, pair, carry, run, aheads, next_tile, next_pair):
+        score(score_b, tile, 2 * pair)
+        if run is not None:
+            carry = weigh(decay_b, weight_b, run, carry)
+        run_a = decay(score_a, decay_a, aheads[0])
+        if run is not None:
+            fold(weight_b, 2 * pair + 2)
+        score(score_a, next_tile, 2 * next_pair + 1)
+        carry = weigh(decay_a, weight_a, run_a, carry)
+        run_b = decay(score_b, decay_b, aheads[1])
+        fold(weight_a, 2 * pair + 1)
+        return carry, run_b
+
+    last = BLOCKS // 2 - 1
+    score(score_a, last, BLOCKS - 1)
+
     def one_tile(step, _):
-        m = BLOCKS // 2 - 1 - step
+        m = last - step
         total[...] = jnp.zeros_like(total)
-        carry = jnp.zeros((8, ROWS), F32)
-        carry = tile(m, 2 * m + 1, carry, where_q - ROWS - 48 * sub, 0)
-        carry = tile(m, 2 * m, carry, where_q - 48 * sub, 1)
-
-        def before(i, carry):
-            at = 2 * (m - 1 - i)
-            carry = tile(m, at + 1, carry, None, 0)
-            return tile(m, at, carry, None, 1)
-
-        carry = lax.fori_loop(0, m, before, carry)
+        aheads = (where_q - ROWS - 48 * sub, where_q - 48 * sub)
+        below = lax.max(m - 1, 0)
+        state = two_blocks(m, m, jnp.zeros((8, ROWS), F32), None, aheads, m, below)
+
+        def before(i, state):
+            pair = m - 1 - i
+            end = 1 - lax.min(pair, 1)
+            return two_blocks(m, pair, *state, (None, None), m - end, pair - 1 + end * m)
+
+        carry, run = lax.fori_loop(0, m, before, state)
+        carry = weigh(decay_b, weight_b, run, carry)
+        fold(weight_b, 0)
         attended = total[...]
         attended = jnp.concatenate((attended, attended), axis=0).T
         for part in range(2):
@@ -811,9 +838,12 @@
             pltpu.VMEM((BLOCKS * ROWS, 256), BF16),
             pltpu.VMEM((BLOCKS, HD, ROWS), BF16),
             pltpu.VMEM((BLOCKS // 2, ROWS, 256), BF16),
-            pltpu.VMEM((2, ROWS, ROWS), F32),
-            pltpu.VMEM((2, ROWS, ROWS), F32),
-            pltpu.VMEM((2, ROWS, ROWS), BF16),
+            pltpu.VMEM((ROWS, ROWS), F32),
+            pltpu.VMEM((ROWS, ROWS), F32),
+            pltpu.VMEM((ROWS, ROWS), F32),
+            pltpu.VMEM((ROWS, ROWS), F32),
+            pltpu.VMEM((ROWS, ROWS), BF16),
+            pltpu.VMEM((ROWS, ROWS), BF16),
             pltpu.VMEM((HD, ROWS), F32),
             pltpu.VMEM((BLOCKS, 96, 128), BF16),
             pltpu.VMEM((BLOCKS, 96, 128), BF16),

time: 134 us -> 126 us (0.940)
  Pallas kernels: 124 us -> 117 us
    pallas_call x1, Pallas kernels: 69.8 us -> 62 us  [attend(): pl.pallas_call(attend_kernel, in_specs=[pl.BlockSpec(memory_space=pltpu.S...]
where the time goes in v4:
time: 126 us
  Pallas kernels  117 us (93%)
  local copies, waits for them, and re-layouts  7.02 us (6%)
  other arithmetic  1.39 us (1%)
    pallas_call x1, Pallas kernels, attend(): pl.pallas_call(attend_kernel, in_specs=[pl.BlockSpec(memory_space=pltpu.S...  62 us
    pallas_call x1, Pallas kernels, front(): pl.pallas_call(front_kernel, in_specs=[hbm, hbm, vmem] + [hbm] * 8, out_s...  54.8 us

profile of v4, /device:TPU:1, one launch (start us, length us, event | category | flops | bytes accessed | tf_op | source)
XLA Modules:
  0.0 125.8 jit_solution(5005343114687820044)
XLA Ops:
  0.7 0.7 pad_maximum_fusion
  1.4 0.7 pad.8
  2.0 0.7 reshape.7
  2.7 0.7 pad.9
  3.4 0.6 concatenate.7.params_hbm.params_ref.gain_ref
  4.1 0.0 copy-start
  4.1 54.8 %front.1 = (bf16[16,288,128]{2,1,0:T(8,128)(2,1)}, bf16[16,192,128]{2,1,0:T(8,128)(2,1)}, bf16[8,192,128]{2,1,0:T(8,128)(2,1)}, f32[8,1024]{1,0:T(8,128)}, bf16[...) custom-call(bf16[384,1024]{1,0:T(8,128)(2,1)} %bitcast.5, f32[8,1024]{1,0:T(8,128)} %concatenate.7.params_hbm.params_ref.gain_ref, ...), custom_call_target="tpu_custom_call" | custom-call | tf_op jit(solution)/shard_map/front/pallas_call | solution.py:479
  58.9 0.0 copy-done
  58.9 0.7 broadcast_select_fusion
  59.5 0.6 dynamic_slice.3.offset_ref
  60.1 62.0 %attend.1 = (bf16[1,192,2048]{2,1,0:T(8,128)(2,1)}, f32[1,384,8]{2,1,0:T(8,128)}) custom-call(f32[1]{0:T(128)} %dynamic_slice.3.offset_ref, bf16[16,288,128]{2,1,0:T(8,128)(2,1)} %get-tuple-element.9.own_ref, bf16[16,192,128]{2,1,0:T(8,128)(2,1)} %get-tuple-element.10.mate_ref, bf16[8,192,128]{2,1,0:T(8,128)(2,1)} %get-tuple-element.11.branch_ref, ...), custom_call_target="tpu_custom_call" | custom-call | tf_op jit(solution)/shard_map/attend/pallas_call | solution.py:829
  122.1 1.6 %copy.16 = f32[1,384,8]{1,2,0:T(8,128)} copy(f32[1,384,8]{2,1,0:T(8,128)} %get-tuple-element.15) | data formatting | bytes 24576 | tf_op jit(solution)/shard_map/attend/pallas_call | solution.py:829
  123.7 2.1 %copy.18 = bf16[1,192,2048]{2,1,0:T(8,128)(2,1)} copy(bf16[1,192,2048]{2,1,0:T(8,128)(2,1)} %get-tuple-element.18) | data formatting | bytes 1572864
  (1 shorter events, 0.0 us)
Async XLA Ops:
  4.1 54.8 %copy-start = (f32[8]{0:T(128)S(1)}, f32[8]{0:T(128)}, u32[]{:S(2)}) copy-start(f32[8]{0:T(128)} %param.22) | copy-start | bytes 100

commit v5 on v4

--- a/solution.py
+++ b/solution.py
@@ -45,10 +45,11 @@
     return lax.rem(value + 8, 4)
 
 
-def front_kernel(
+def layer_kernel(
     tokens_ref,
-    params_hbm,
-    params_ref,
+    gain_ref,
+    side_ref,
+    taps_ref,
     wq_ref,
     wk_ref,
     wv_ref,
@@ -57,12 +58,8 @@
     wc_ref,
     att_ref,
     conv_ref,
-    own_ref,
-    mate_ref,
-    branch_ref,
-    params_other_ref,
-    att_other_ref,
-    conv_other_ref,
+    mixed_ref,
+    mass_ref,
     tok,
     wts,
     msg,
@@ -72,6 +69,24 @@
     outgate,
     branch_out,
     branch_in,
+    keys,
+    values,
+    queries,
+    score_a,
+    score_b,
+    decay_a,
+    decay_b,
+    weight_a,
+    weight_b,
+    total,
+    att_out,
+    att_in,
+    mass_out,
+    mass_in,
+    att_weights,
+    conv_weights,
+    matrix,
+    sides,
     local_sem,
     spread_send,
     spread_recv,
@@ -95,6 +110,10 @@
     halo_recv,
     branch_send,
     branch_recv,
+    att_send,
+    att_recv,
+    mass_send,
+    mass_recv,
 ):
     place, x, core = lax.axis_index("sp"), lax.axis_index("fs"), lax.axis_index("tp")
     y, z = lax.rem(place, 4), lax.div(place, 4)
@@ -133,7 +152,22 @@
         return 0
 
     lax.fori_loop(1, BLOCKS, greet, 0)
-    pl.semaphore_wait(barrier, 34)
+    number, row = y, z
+    seq = mod4(row - number)
+
+    def greet_far(k, _):
+        n = lax.rem(k, 4)
+        there, column = mod4(x + n) * 4 + n, lax.div(k, 4)
+        for other in range(2):
+
+            @pl.when(lax.abs(there - place) + lax.abs(column - x) + lax.abs(other - core) > 0)
+            def _():
+                pl.semaphore_signal(barrier, inc=1, device_id=(there, column, other), device_id_type=MESH)
+
+        return 0
+
+    lax.fori_loop(0, 16, greet_far, 0)
+    pl.semaphore_wait(barrier, 65 + lax.min(lax.abs(seq - x), 1))
 
     rows_at = pl.multiple_of(place * 32, 32)
 
@@ -151,6 +185,9 @@
         for m in range(6):
             spread(k, m).start()
 
+    side_out = remote(side_ref, sides.at[core], other_send.at[2], other_recv.at[2], sibling)
+    side_out.start()
+    sides[core] = side_ref[...]
     own_tokens.wait()
     top, bottom = pl.ds(0, HALF), pl.ds(HALF, HALF)
 
@@ -238,9 +275,12 @@
         far(*kind).wait_recv()
         onward(*kind).start()
     others = [
-        remote(att_ref, att_other_ref, other_send.at[0], other_recv.at[0], sibling),
-        remote(conv_ref, conv_other_ref, other_send.at[1], other_recv.at[1], sibling),
-        remote(params_hbm, params_other_ref, other_send.at[2], other_recv.at[2], sibling),
+        remote(att_ref, att_weights.at[core], other_send.at[0], other_recv.at[0], sibling),
+        remote(conv_ref, conv_weights.at[core], other_send.at[1], other_recv.at[1], sibling),
+    ]
+    fetches = [
+        pltpu.make_async_copy(att_ref, att_weights.at[core], local_sem.at[0]),
+        pltpu.make_async_copy(conv_ref, conv_weights.at[core], local_sem.at[1]),
     ]
     for copy in own_weights:
         copy.wait()
@@ -299,7 +339,7 @@
             pairs[6].start()
             on_left.wait_recv()
             pairs[7].start()
-            for copy in others:
+            for copy in others + fetches:
                 copy.start()
             pairs[6].wait_recv()
             pairs[7].wait_recv()
@@ -308,12 +348,12 @@
         high = tok[s, 1].astype(F32)
         squares = jnp.sum(low * low, axis=1, keepdims=True) + jnp.sum(high * high, axis=1, keepdims=True)
         scale = lax.rsqrt(squares / D + epsilon)
-        total = dot((low * params_ref[0:1, :]).astype(BF16), wts[0:2].reshape(1024, 768)) + dot(
-            (high * params_ref[1:2, :]).astype(BF16), wts[2:4].reshape(1024, 768)
+        product = dot((low * gain_ref[0:1, 0:1024]).astype(BF16), wts[0:2].reshape(1024, 768)) + dot(
+            (high * gain_ref[0:1, 1024:2048]).astype(BF16), wts[2:4].reshape(1024, 768)
         )
-        out = (total[:, 128:] * scale).astype(BF16)
+        out = (product[:, 128:] * scale).astype(BF16)
         key, value = out[:, 0:128], out[:, 128:256]
-        query = (total[:, 0:128] * (scale * (LOG2E / 8))).astype(BF16)
+        query = (product[:, 0:128] * (scale * (LOG2E / 8))).astype(BF16)
         for j in range(2):
             mine = slice(j * HD, (j + 1) * HD)
             both = jnp.concatenate((key[:, mine], value[:, mine]), axis=1)
@@ -357,7 +397,7 @@
             halo(s).wait_recv()
 
         convolved = sum(
-            params_ref[4 + t : 5 + t, columns] * gated[s, 6 + t : 6 + t + ROWS, :] for t in range(3)
+            taps_ref[t : t + 1, columns] * gated[s, 6 + t : 6 + t + ROWS, :] for t in range(3)
         )
         branch = (outgate[s].astype(F32) * convolved).astype(BF16)
         branch_out[2 * s] = branch[0:HALF]
@@ -384,233 +424,13 @@
 
     source_core = lax.div(y, 2)
 
-    def arrive(k, _):
-        block = lax.rem(place + k, BLOCKS)
-
-        @pl.when(k + lax.abs(source_core - core) > 0)
-        def _():
-            remote(
-                msg.at[0], recv.at[block], msg_send.at[0], msg_recv.at[block], (block, x, source_core)
-            ).wait_recv()
-
-        to_mate(block).start()
-        return 0
-
-    lax.fori_loop(0, BLOCKS, arrive, 0)
-    own_out = pltpu.make_async_copy(recv, own_ref, local_sem.at[0])
-    own_out.start()
-
-    def arrived(block, _):
-        to_mate(block).wait_recv()
-        return 0
-
-    lax.fori_loop(0, BLOCKS, arrived, 0)
-
-    def branch_arrived(k, _):
-        there = lax.rem(2 * x + core + k, 8)
-        remote(
-            branch_out.at[0],
-            branch_in.at[there],
-            branch_send.at[0],
-            branch_recv.at[there],
-            (place, lax.div(there, 2), lax.rem(there, 2)),
-        ).wait_recv()
-        return 0
-
-    lax.fori_loop(1, 8, branch_arrived, 0)
-    home_out = pltpu.make_async_copy(branch_in, branch_ref, local_sem.at[2])
-    home_out.start()
-    mate_out = pltpu.make_async_copy(mate, mate_ref, local_sem.at[1])
-    mate_out.start()
-
-    for k in range(1, 4):
-        for m in range(6):
-            spread(k, m).wait_send()
-        for i in range(1, 4):
-            for way in range(2):
-                near(k, i, way).wait_send()
-    for kind in kinds:
-        far(*kind).wait_send()
-        onward(*kind).wait_send()
-    for copy in [right_a, right_b, left_a, left_b, on_right, on_left] + pairs:
-        copy.wait_send()
-
-    def left_here(at, _):
-        s = lax.div(at, 4)
-        j = lax.div(lax.rem(at, 4), 2)
-        copy, apart = message(s, j, lax.rem(at, 2))
-
-        @pl.when(apart > 0)
-        def _():
-            copy.wait_send()
-
-        to_mate(at).wait_send()
-        return 0
-
-    lax.fori_loop(0, BLOCKS, left_here, 0)
-
-    def branch_left(at, _):
-        copy, apart = to_home(at)
-
-        @pl.when(apart > 0)
-        def _():
-            copy.wait_send()
-
-        return 0
-
-    lax.fori_loop(0, 8, branch_left, 0)
-
-    @pl.when(place < BLOCKS - 1)
-    def _():
-        for s in range(SEQS):
-            halo(s).wait_send()
-
-    home_out.wait()
-    own_out.wait()
-    mate_out.wait()
-    for copy in others:
-        copy.wait()
-
-
-def front(tokens, params, mats, out_att, out_conv):
-    hbm = pl.BlockSpec(memory_space=pl.ANY)
-    vmem = pl.BlockSpec(memory_space=pltpu.VMEM)
-    dma = lambda *shape: pltpu.SemaphoreType.DMA(shape)
-    return pl.pallas_call(
-        front_kernel,
-        in_specs=[hbm, hbm, vmem] + [hbm] * 8,
-        out_specs=[hbm] * 6,
-        out_shape=[
-            jax.ShapeDtypeStruct((BLOCKS, MESSAGE, 128), BF16),
-            jax.ShapeDtypeStruct((BLOCKS, HALF, 128), BF16),
-            jax.ShapeDtypeStruct((8, HALF, 128), BF16),
-            jax.ShapeDtypeStruct(params.shape, F32),
-            jax.ShapeDtypeStruct(out_att.shape, BF16),
-            jax.ShapeDtypeStruct(out_conv.shape, BF16),
-        ],
-        scratch_shapes=[
-            pltpu.VMEM((SEQS, 2, ROWS, 1024), BF16),
-            pltpu.VMEM((4, 4, 128, 768), BF16),
-            pltpu.VMEM((BLOCKS, MESSAGE, 128), BF16),
-            pltpu.VMEM((BLOCKS, MESSAGE, 128), BF16),
-            pltpu.VMEM((BLOCKS, HALF, 128), BF16),
-            pltpu.VMEM((SEQS, ROWS + 8, 128), F32),
-            pltpu.VMEM((SEQS, ROWS, 128), BF16),
-            pltpu.VMEM((8, HALF, 128), BF16),
-            pltpu.VMEM((8, HALF, 128), BF16),
-            dma(31),
-            dma(3, 6), dma(3, 6),
-            dma(18), dma(18),
-            dma(12), dma(12),
-            dma(12), dma(12),
-            dma(6), dma(6),
-            dma(8), dma(8),
-            dma(16), dma(16),
-            dma(16), dma(16),
-            dma(3), dma(3),
-            dma(4), dma(4),
-            dma(8), dma(8),
-        ],
-        compiler_params=pltpu.CompilerParams(
-            collective_id=0, has_side_effects=True, vmem_limit_bytes=56 << 20
-        ),
-        name="front",
-    )(tokens, params, params, *mats, out_att, out_conv)
-
-
-def attend_kernel(
-    offset_ref,
-    own_ref,
-    mate_ref,
-    branch_ref,
-    gain_ref,
-    gain_other_ref,
-    att_ref,
-    att_other_ref,
-    conv_ref,
-    conv_other_ref,
-    mixed_ref,
-    mass_ref,
-    keys,
-    values,
-    queries,
-    score_a,
-    score_b,
-    decay_a,
-    decay_b,
-    weight_a,
-    weight_b,
-    total,
-    att_out,
-    att_in,
-    mass_out,
-    mass_in,
-    att_weights,
-    conv_weights,
-    matrix,
-    gains,
-    att_send,
-    att_recv,
-    mass_send,
-    mass_recv,
-    local_sem,
-):
-    place, x, half = lax.axis_index("sp"), lax.axis_index("fs"), lax.axis_index("tp")
-    number, row = lax.rem(place, 4), lax.div(place, 4)
-    seq = mod4(row - number)
-
-    barrier = pltpu.get_barrier_semaphore()
-
-    def greet(k, _):
-        n = lax.rem(k, 4)
-        there, column = mod4(x + n) * 4 + n, lax.div(k, 4)
-        for core in range(2):
-            @pl.when(lax.abs(there - place) + lax.abs(column - x) + lax.abs(core - half) > 0)
-            def _():
-                pl.semaphore_signal(barrier, inc=1, device_id=(there, column, core), device_id_type=MESH)
-
-        return 0
-
-    lax.fori_loop(0, 16, greet, 0)
-    fetches = [
-        pltpu.make_async_copy(src, dst, local_sem.at[i])
-        for i, (src, dst) in enumerate(
-            [
-                (att_ref, att_weights.at[half]),
-                (att_other_ref, att_weights.at[1 - half]),
-                (conv_ref, conv_weights.at[half]),
-                (conv_other_ref, conv_weights.at[1 - half]),
-                (gain_ref, gains.at[half]),
-                (gain_other_ref, gains.at[1 - half]),
-            ]
-        )
-    ]
-    for copy in fetches:
-        copy.start()
-
-    def remote(src, dst, send, recv, device):
-        return pltpu.make_async_remote_copy(
-            src_ref=src, dst_ref=dst, send_sem=send, recv_sem=recv, device_id=device, device_id_type=MESH
-        )
-
-    def att_home(block):
-        at = 4 * x + number
-        apart = lax.abs(block - place) + lax.abs(seq - x)
-        return remote(
-            att_out.at[block], att_in.at[at], att_send.at[block], att_recv.at[at], (block, seq, half)
-        ), apart
-
-    def mass_home(block):
-        at = 4 * x + 2 * lax.rem(number, 2) + half
-        core = lax.div(number, 2)
-        apart = lax.abs(block - place) + lax.abs(seq - x) + lax.abs(core - half)
-        return remote(
-            mass_out.at[block], mass_in.at[at], mass_send.at[block], mass_recv.at[at], (block, seq, core)
-        ), apart
-
     lanes = lambda shape: lax.broadcasted_iota(jnp.int32, shape, 1)
     rows = lambda shape: lax.broadcasted_iota(jnp.int32, shape, 0)
-    offset = jnp.full((HALF, 128), offset_ref[0] * LOG2E, F32)
+    side_out.wait_recv()
+    place_of_head = lanes((1, 128)) == 2 * x + lax.rem(number, 2)
+    offset_lane = sides[lax.div(number, 2), 0:1, 1024:1152]
+    offset = jnp.sum(jnp.where(place_of_head, offset_lane, 0.0), axis=1, keepdims=True) * LOG2E
+    offset = jnp.broadcast_to(offset, (HALF, 128))
     o1, o2, o3 = (part.astype(F32) for part in three_parts(offset))
     lane_q = lanes((HALF, 128))
     offset_row = jnp.where(
@@ -618,30 +438,74 @@
     ).astype(BF16)
     square = (ROWS, HALF)
     source = lax.rem(rows(square), 8) * 48 + rows(square) // 8 - lanes(square)
-    permute_own = (source == half * HALF).astype(F32).astype(BF16)
-    permute_mate = (source == HALF - half * HALF).astype(F32).astype(BF16)
+    permute_own = (source == core * HALF).astype(F32).astype(BF16)
+    permute_mate = (source == HALF - core * HALF).astype(F32).astype(BF16)
     take_high = (lanes((HD, 128)) == rows((HD, 128)) + HD).astype(F32).astype(BF16)
     ones = (lanes((ROWS, 128)) < 3).astype(F32).astype(BF16)
     low_lane = lanes((96, 128)) < HD
-    for block in range(BLOCKS):
-        pair = dot(permute_own, own_ref[block, 0:HALF, :]) + dot(permute_mate, mate_ref[block])
+
+    def prepare(block):
+        pair = dot(permute_own, recv[block, 0:HALF, :]) + dot(permute_mate, mate[block])
         pair = pair.astype(BF16)
-        keys[block * ROWS : (block + 1) * ROWS, 0:128] = pair
-        keys[block * ROWS : (block + 1) * ROWS, 128:256] = ones
+        at = pl.ds(pl.multiple_of(block * ROWS, ROWS), ROWS)
+        keys[at, 0:128] = pair
+        keys[at, 128:256] = ones
         values[block] = dot_nt(take_high, pair).astype(BF16)
-        packed = own_ref[block, HALF:MESSAGE, :].astype(F32)
-        at = (block % 2) * HALF
-        queries[block // 2, at : at + 96, 0:128] = jnp.where(low_lane, packed, 0.0).astype(BF16)
-        queries[block // 2, at + 96 : at + HALF, 0:128] = jnp.where(
+        packed = recv[block, HALF:MESSAGE, :].astype(F32)
+        tile, first = lax.div(block, 2), lax.rem(block, 2) * HALF
+        rows_of = lambda start, size: pl.ds(pl.multiple_of(first + start, 32), size)
+        queries[tile, rows_of(0, 96), 0:128] = jnp.where(low_lane, packed, 0.0).astype(BF16)
+        queries[tile, rows_of(96, 96), 0:128] = jnp.where(
             low_lane, pltpu.roll(packed, HD, 1), 0.0
         ).astype(BF16)
-        queries[block // 2, at : at + HALF, 128:256] = offset_row
-
-    pl.semaphore_wait(barrier, 31 + lax.min(lax.abs(seq - x), 1))
+        queries[tile, rows_of(0, HALF), 128:256] = offset_row
+
+    def arrive(k):
+        block = lax.rem(place + k, BLOCKS)
+
+        @pl.when(k + lax.abs(source_core - core) > 0)
+        def _():
+            remote(
+                msg.at[0], recv.at[block], msg_send.at[0], msg_recv.at[block], (block, x, source_core)
+            ).wait_recv()
+
+        to_mate(block).start()
+
+    def use(k):
+        block = lax.rem(place + k, BLOCKS)
+        to_mate(block).wait_recv()
+        prepare(block)
+
+    arrive(0)
+    arrive(1)
+
+    def arrive_and_use(k, _):
+        arrive(k)
+        use(k - 2)
+        return 0
+
+    lax.fori_loop(2, BLOCKS, arrive_and_use, 0)
+    use(BLOCKS - 2)
+    use(BLOCKS - 1)
+
+    def att_home(block):
+        at = 4 * x + number
+        apart = lax.abs(block - place) + lax.abs(seq - x)
+        return remote(
+            att_out.at[block], att_in.at[at], att_send.at[block], att_recv.at[at], (block, seq, core)
+        ), apart
+
+    def mass_home(block):
+        at = 4 * x + 2 * lax.rem(number, 2) + core
+        goal = lax.div(number, 2)
+        apart = lax.abs(block - place) + lax.abs(seq - x) + lax.abs(goal - core)
+        return remote(
+            mass_out.at[block], mass_in.at[at], mass_send.at[block], mass_recv.at[at], (block, seq, goal)
+        ), apart
 
     sub = rows((8, ROWS))
     lane = lanes((8, ROWS))
-    where_q = lane + half * HALF + jnp.where(lane < HALF, 0, HALF)
+    where_q = lane + core * HALF + jnp.where(lane < HALF, 0, HALF)
 
     def score(z_ref, tile_index, block):
         begin = pl.multiple_of(block * ROWS, ROWS)
@@ -702,12 +566,12 @@
         below = lax.max(m - 1, 0)
         state = two_blocks(m, m, jnp.zeros((8, ROWS), F32), None, aheads, m, below)
 
-        def before(i, state):
+        def earlier(i, state):
             pair = m - 1 - i
             end = 1 - lax.min(pair, 1)
             return two_blocks(m, pair, *state, (None, None), m - end, pair - 1 + end * m)
 
-        carry, run = lax.fori_loop(0, m, before, state)
+        carry, run = lax.fori_loop(0, m, earlier, state)
         carry = weigh(decay_b, weight_b, run, carry)
         fold(weight_b, 0)
         attended = total[...]
@@ -738,7 +602,7 @@
 
             @pl.when(mass_apart == 0)
             def _():
-                mass_in[4 * x + 2 * lax.rem(number, 2) + half, :, 0:HALF] = mass
+                mass_in[4 * x + 2 * lax.rem(number, 2) + core, :, 0:HALF] = mass
 
         return 0
 
@@ -746,21 +610,35 @@
 
     for copy in fetches:
         copy.wait()
+    for copy in others:
+        copy.wait_recv()
+    def branch_arrived(k, _):
+        there = lax.rem(2 * x + core + k, 8)
+        remote(
+            branch_out.at[0],
+            branch_in.at[there],
+            branch_send.at[0],
+            branch_recv.at[there],
+            (place, lax.div(there, 2), lax.rem(there, 2)),
+        ).wait_recv()
+        return 0
+
+    lax.fori_loop(1, 8, branch_arrived, 0)
 
     def branch_product(store, row_gain, projection, load):
         squares = jnp.zeros((HALF, 128), F32)
-        for core in range(2):
+        for owner in range(2):
             for part in range(4):
-                piece = load(core, part)
+                piece = load(owner, part)
                 squares = squares + piece * piece
-                gain = gains[core, 2:3, row_gain + 128 * part : row_gain + 128 * part + 128]
-                at = 512 * core + 128 * part
+                gain = sides[owner, 0:1, row_gain + 128 * part : row_gain + 128 * part + 128]
+                at = 512 * owner + 128 * part
                 store[:, at : at + 128] = (piece * gain).astype(BF16)
         scale = lax.rsqrt(jnp.sum(squares, axis=1, keepdims=True) / ATT_WIDTH + epsilon)
         return scale * dot(store[...], projection[...].reshape(1024, D))
 
     mixed = branch_product(
-        matrix.at[0], 512, conv_weights, lambda core, part: branch_ref[2 * part + core].astype(F32)
+        matrix.at[0], 512, conv_weights, lambda owner, part: branch_in[2 * part + owner].astype(F32)
     )
 
     def landed(at, _):
@@ -771,27 +649,27 @@
         @pl.when(apart > 0)
         def _():
             remote(
-                att_out.at[0], att_in.at[at], att_send.at[0], att_recv.at[at], (there, column, half)
+                att_out.at[0], att_in.at[at], att_send.at[0], att_recv.at[at], (there, column, core)
             ).wait_recv()
 
-        n = 2 * half + lax.div(n, 2)
-        core = lax.rem(at, 2)
+        n = 2 * core + lax.div(n, 2)
+        owner = lax.rem(at, 2)
         there = mod4(x + n) * 4 + n
-        apart = lax.abs(there - place) + lax.abs(column - x) + lax.abs(core - half)
+        apart = lax.abs(there - place) + lax.abs(column - x) + lax.abs(owner - core)
 
         @pl.when(apart > 0)
         def _():
             remote(
-                mass_out.at[0], mass_in.at[at], mass_send.at[0], mass_recv.at[at], (there, column, core)
+                mass_out.at[0], mass_in.at[at], mass_send.at[0], mass_recv.at[at], (there, column, owner)
             ).wait_recv()
 
         return 0
 
     lax.fori_loop(0, 16, landed, 0)
 
-    def heads(core, part):
-        a = att_in[4 * part + 2 * core].astype(F32)
-        b = att_in[4 * part + 2 * core + 1].astype(F32)
+    def heads(owner, part):
+        a = att_in[4 * part + 2 * owner].astype(F32)
+        b = att_in[4 * part + 2 * owner + 1].astype(F32)
         low = lanes((96, 128)) < HD
         upper = jnp.where(low, a, pltpu.roll(b, HD, 1))
         lower = jnp.where(low, pltpu.roll(a, HD, 1), b)
@@ -801,8 +679,8 @@
     mixed_ref[0] = mixed.astype(BF16)
     for part in range(2):
         kept = jnp.concatenate([mass_in[2 * n + part, 0:1, :] for n in range(8)], axis=0)
-        mass = jnp.log(2.0 - jnp.exp2(-kept)).T
-        mass_ref[0, part * HALF : (part + 1) * HALF, :] = mass[0:HALF]
+        mass = jnp.log(2.0 - jnp.exp2(-kept))
+        mass_ref[0, :, part * HALF : (part + 1) * HALF] = mass[:, 0:HALF]
 
     def left(block, _):
         copy, apart = att_home(block)
@@ -822,19 +700,75 @@
     lax.fori_loop(0, BLOCKS, left, 0)
 
 
-def attend(offset, own, mate, branch, params, params_other, att, att_other, conv, conv_other):
-    whole = pl.BlockSpec(memory_space=pltpu.VMEM)
+    for k in range(1, 4):
+        for m in range(6):
+            spread(k, m).wait_send()
+        for i in range(1, 4):
+            for way in range(2):
+                near(k, i, way).wait_send()
+    for kind in kinds:
+        far(*kind).wait_send()
+        onward(*kind).wait_send()
+    for copy in [right_a, right_b, left_a, left_b, on_right, on_left] + pairs:
+        copy.wait_send()
+
+    def left_here(at, _):
+        s = lax.div(at, 4)
+        j = lax.div(lax.rem(at, 4), 2)
+        copy, apart = message(s, j, lax.rem(at, 2))
+
+        @pl.when(apart > 0)
+        def _():
+            copy.wait_send()
+
+        to_mate(at).wait_send()
+        return 0
+
+    lax.fori_loop(0, BLOCKS, left_here, 0)
+
+    def branch_left(at, _):
+        copy, apart = to_home(at)
+
+        @pl.when(apart > 0)
+        def _():
+            copy.wait_send()
+
+        return 0
+
+    lax.fori_loop(0, 8, branch_left, 0)
+
+    @pl.when(place < BLOCKS - 1)
+    def _():
+        for s in range(SEQS):
+            halo(s).wait_send()
+
+    side_out.wait_send()
+    for copy in others:
+        copy.wait_send()
+
+
+def layer(tokens, gain, side, taps, mats, out_att, out_conv):
     hbm = pl.BlockSpec(memory_space=pl.ANY)
+    vmem = pl.BlockSpec(memory_space=pltpu.VMEM)
     dma = lambda *shape: pltpu.SemaphoreType.DMA(shape)
     return pl.pallas_call(
-        attend_kernel,
-        in_specs=[pl.BlockSpec(memory_space=pltpu.SMEM), whole, whole, whole] + [hbm] * 6,
-        out_specs=[whole, whole],
+        layer_kernel,
+        in_specs=[hbm, vmem, vmem, vmem] + [hbm] * 8,
+        out_specs=[vmem, vmem],
         out_shape=[
             jax.ShapeDtypeStruct((1, HALF, D), BF16),
-            jax.ShapeDtypeStruct((1, ROWS, 8), F32),
+            jax.ShapeDtypeStruct((1, 8, ROWS), F32),
         ],
         scratch_shapes=[
+            pltpu.VMEM((SEQS, 2, ROWS, 1024), BF16),
+            pltpu.VMEM((4, 4, 128, 768), BF16),
+            pltpu.VMEM((BLOCKS, MESSAGE, 128), BF16),
+            pltpu.VMEM((BLOCKS, MESSAGE, 128), BF16),
+            pltpu.VMEM((BLOCKS, HALF, 128), BF16),
+            pltpu.VMEM((SEQS, ROWS + 8, 128), F32),
+            pltpu.VMEM((SEQS, ROWS, 128), BF16),
+            pltpu.VMEM((8, HALF, 128), BF16),
+            pltpu.VMEM((8, HALF, 128), BF16),
             pltpu.VMEM((BLOCKS * ROWS, 256), BF16),
             pltpu.VMEM((BLOCKS, HD, ROWS), BF16),
             pltpu.VMEM((BLOCKS // 2, ROWS, 256), BF16),
@@ -852,14 +786,27 @@
             pltpu.VMEM((2, 512, D), BF16),
             pltpu.VMEM((2, 512, D), BF16),
             pltpu.VMEM((2, HALF, 1024), BF16),
-            pltpu.VMEM((2, 8, 1024), F32),
-            dma(16), dma(16), dma(16), dma(16), dma(6),
+            pltpu.VMEM((2, 1, 1152), F32),
+            dma(31),
+            dma(3, 6), dma(3, 6),
+            dma(18), dma(18),
+            dma(12), dma(12),
+            dma(12), dma(12),
+            dma(6), dma(6),
+            dma(8), dma(8),
+            dma(16), dma(16),
+            dma(16), dma(16),
+            dma(3), dma(3),
+            dma(4), dma(4),
+            dma(8), dma(8),
+            dma(16), dma(16),
+            dma(16), dma(16),
         ],
         compiler_params=pltpu.CompilerParams(
-            collective_id=1, has_side_effects=True, vmem_limit_bytes=56 << 20
+            collective_id=0, has_side_effects=True, vmem_limit_bytes=58 << 20
         ),
-        name="attend",
-    )(offset, own, mate, branch, params, params_other, att, att_other, conv, conv_other)
+        name="layer",
+    )(tokens, gain, side, taps, *mats, out_att, out_conv)
 
 
 def per_device(
@@ -878,28 +825,17 @@
     out_att,
     out_conv,
 ):
-    wide = lambda a: jnp.pad(a, ((0, 0), (0, 1024 - a.shape[1])))
-    params = jnp.concatenate(
-        (
-            in_gain.reshape(2, 1024),
-            jnp.concatenate((att_gain, conv_gain))[None],
-            wide(score_offset[None]),
-            wide(conv_taps),
-            jnp.zeros((1, 1024), F32),
-        ),
-        axis=0,
+    side = jnp.concatenate((att_gain, conv_gain, score_offset, jnp.zeros((120,), F32)))
+    mixed, mass = layer(
+        tokens[0],
+        in_gain.reshape(1, D),
+        side.reshape(1, 1152),
+        conv_taps,
+        (w_query, w_key, w_value, w_outgate, w_ingate, w_conv_in),
+        out_att,
+        out_conv,
     )
-    own, mate, branch, params_other, att_other, conv_other = front(
-        tokens[0], params, (w_query, w_key, w_value, w_outgate, w_ingate, w_conv_in), out_att, out_conv
-    )
-    number = lax.rem(lax.axis_index("sp"), 4)
-    offsets = jnp.where(number // 2 == lax.axis_index("tp"), score_offset, params_other[3, :8])
-    offset = lax.dynamic_slice_in_dim(offsets, 2 * lax.axis_index("fs") + lax.rem(number, 2), 1, 0)
-    return tuple(
-        attend(
-            offset, own, mate, branch, params, params_other, out_att, att_other, out_conv, conv_other
-        )
-    )
+    return mixed, jnp.swapaxes(mass, 1, 2)
 
 
 def solution(mesh):

time: 126 us -> 116 us (0.921)
  Pallas kernels: 117 us -> 110 us
  local copies, waits for them, and re-layouts: 7.02 us -> 4.77 us
  other arithmetic: 1.39 us -> 0 us
    pallas_call x2 -> x1, Pallas kernels: 117 us -> 110 us  [layer(): pl.pallas_call(layer_kernel, in_specs=[hbm, vmem, vmem, vmem] + [hbm] * 8...]
    pallas_call x1 -> x0, local copies, waits for them, and re-layouts: 1.63 us -> none  [attend(): pl.pallas_call(attend_kernel, in_specs=[pl.BlockSpec(memory_space=pltpu.S...]
    pad x2 -> x0, local copies, waits for them, and re-layouts: 1.36 us -> none  [per_device(): wide = lambda a: jnp.pad(a, ((0, 0), (0, 1024 - a.shape[1])))]
    unnamed x3 -> x2, local copies, waits for them, and re-layouts: 2.09 us -> 3.4 us
where the time goes in v5:
time: 116 us
  Pallas kernels  110 us (95%)
  local copies, waits for them, and re-layouts  4.77 us (4%)
    pallas_call x1, Pallas kernels, layer(): pl.pallas_call(layer_kernel, in_specs=[hbm, vmem, vmem, vmem] + [hbm] * 8...  110 us
    unnamed x2, local copies, waits for them, and re-layouts  3.4 us

profile of v5, /device:TPU:1, one launch (start us, length us, event | category | flops | bytes accessed | tf_op | source)
XLA Modules:
  0.0 115.8 jit_solution(1762656597661824722)
XLA Ops:
  0.6 0.8 concatenate.3
  1.4 0.6 reshape.11.side_ref
  2.0 110.4 %layer.1 = (bf16[1,192,2048]{2,1,0:T(8,128)(2,1)}, f32[1,8,384]{2,1,0:T(8,128)}) custom-call(bf16[384,1024]{1,0:T(8,128)(2,1)} %bitcast.3, f32[1,2048]{1,0:T(1,128)} %bitcast.5, f32[1,1152]{1,0:T(1,128)} %reshape.11.side_ref, f32[3,512]{1,0:T(4,128)} %taps_ref.1, bf16[512,512]{1,0:T(8,128)(2,1)} %wq_ref.1, bf16[512,512]{1,0:T(8,128)(2,1)} %wk_ref.1, ...), custom_call_target="tpu_custom_call" | custom-call | tf_op jit(solution)/shard_map/layer/pallas_call | solution.py:754
  112.4 2.1 %copy.18 = bf16[1,192,2048]{2,1,0:T(8,128)(2,1)} copy(bf16[1,192,2048]{2,1,0:T(8,128)(2,1)} %get-tuple-element.8) | data formatting | bytes 1572864
  114.5 1.3 %copy.19 = f32[1,384,8]{1,2,0:T(8,128)} copy(f32[1,384,8]{1,2,0:T(8,128)} %bitcast.4) | data formatting | bytes 24576
  (1 shorter events, 0.0 us)

commit v6 on v5

--- a/solution.py
+++ b/solution.py
@@ -48,7 +48,9 @@
 def layer_kernel(
     tokens_ref,
     gain_ref,
-    side_ref,
+    att_gain_ref,
+    conv_gain_ref,
+    offset_ref,
     taps_ref,
     wq_ref,
     wk_ref,
@@ -72,12 +74,9 @@
     keys,
     values,
     queries,
-    score_a,
-    score_b,
-    decay_a,
-    decay_b,
-    weight_a,
-    weight_b,
+    scores,
+    decays,
+    weights,
     total,
     att_out,
     att_in,
@@ -86,6 +85,7 @@
     att_weights,
     conv_weights,
     matrix,
+    side,
     sides,
     local_sem,
     spread_send,
@@ -140,6 +140,11 @@
     for copy in own_weights:
         copy.start()
 
+    side[:, 0:512] = att_gain_ref[...]
+    side[:, 512:1024] = conv_gain_ref[...]
+    side[:, 1024:1152] = jnp.zeros((1, 128), F32)
+    side[:, 1024:1032] = offset_ref[...]
+    sides[core] = side[...]
     barrier = pltpu.get_barrier_semaphore()
     for k in range(1, 4):
         pl.semaphore_signal(barrier, inc=1, device_id=(place, mod4(x + k), core), device_id_type=MESH)
@@ -185,9 +190,8 @@
         for m in range(6):
             spread(k, m).start()
 
-    side_out = remote(side_ref, sides.at[core], other_send.at[2], other_recv.at[2], sibling)
+    side_out = remote(side, sides.at[core], other_send.at[2], other_recv.at[2], sibling)
     side_out.start()
-    sides[core] = side_ref[...]
     own_tokens.wait()
     top, bottom = pl.ds(0, HALF), pl.ds(HALF, HALF)
 
@@ -543,37 +547,54 @@
             w_ref[16 * i : 16 * i + 16, :] = both.astype(BF16)
         return carry + jnp.broadcast_to(suffix[0:1], (8, ROWS))
 
-    def two_blocks(tile, pair, carry, run, aheads, next_tile, next_pair):
-        score(score_b, tile, 2 * pair)
+    def run_blocks(tile, top, carry, run, aheads, next_tile, next_top):
+        count = len(aheads)
+        slots = (0, 1, 2, 3) if count == 4 else (0, 3)
+        if count == 4:
+            score(scores[3], tile, top - 3)
+        else:
+            score(scores[2], next_tile, lax.max(next_top - 2, 0))
         if run is not None:
-            carry = weigh(decay_b, weight_b, run, carry)
-        run_a = decay(score_a, decay_a, aheads[0])
-        if run is not None:
-            fold(weight_b, 2 * pair + 2)
-        score(score_a, next_tile, 2 * next_pair + 1)
-        carry = weigh(decay_a, weight_a, run_a, carry)
-        run_b = decay(score_b, decay_b, aheads[1])
-        fold(weight_a, 2 * pair + 1)
-        return carry, run_b
+            carry = weigh(decays[3], weights[3], run, carry)
+        for i in range(count):
+            slot = slots[i]
+            run = decay(scores[i], decays[slot], aheads[i])
+            if i > 0:
+                fold(weights[slots[i - 1]], top - i + 1)
+            elif aheads[0] is None:
+                fold(weights[3], top + 1)
+            if i < 3:
+                score(scores[i], next_tile, lax.max(next_top - i, 0))
+            if i < count - 1:
+                carry = weigh(decays[slot], weights[slot], run, carry)
+        return carry, run
 
     last = BLOCKS // 2 - 1
-    score(score_a, last, BLOCKS - 1)
-
-    def one_tile(step, _):
-        m = last - step
+    for i in range(3):
+        score(scores[i], last, BLOCKS - 1 - i)
+
+    def one_tile(m, odd):
         total[...] = jnp.zeros_like(total)
         aheads = (where_q - ROWS - 48 * sub, where_q - 48 * sub)
+        aheads = aheads + (None, None) if odd else aheads
+        begin = 2 * m - 3 if odd else 2 * m - 1
+        rest = lax.div(m, 2)
+        more = lax.min(rest, 1)
         below = lax.max(m - 1, 0)
-        state = two_blocks(m, m, jnp.zeros((8, ROWS), F32), None, aheads, m, below)
+
+        def following(top, stay):
+            return stay * m + (1 - stay) * below, stay * top + (1 - stay) * (2 * m - 1)
+
+        state = run_blocks(m, 2 * m + 1, jnp.zeros((8, ROWS), F32), None, aheads, *following(begin, more))
 
         def earlier(i, state):
-            pair = m - 1 - i
-            end = 1 - lax.min(pair, 1)
-            return two_blocks(m, pair, *state, (None, None), m - end, pair - 1 + end * m)
-
-        carry, run = lax.fori_loop(0, m, earlier, state)
-        carry = weigh(decay_b, weight_b, run, carry)
-        fold(weight_b, 0)
+            top = begin - 4 * i
+            stay = lax.min(lax.div(top, 4), 1)
+            return run_blocks(m, top, *state, (None,) * 4, *following(top - 4, stay))
+
+        carry, run = lax.fori_loop(0, rest, earlier, state)
+        carry = weigh(decays[3], weights[3], run, carry)
+        fold(weights[3], 0)
         attended = total[...]
         attended = jnp.concatenate((attended, attended), axis=0).T
         for part in range(2):
@@ -604,9 +625,12 @@
             def _():
                 mass_in[4 * x + 2 * lax.rem(number, 2) + core, :, 0:HALF] = mass
 
-        return 0
-
-    lax.fori_loop(0, BLOCKS // 2, one_tile, 0)
+    def two_tiles(step, _):
+        one_tile(last - 2 * step, True)
+        one_tile(last - 1 - 2 * step, False)
+        return 0
+
+    lax.fori_loop(0, BLOCKS // 4, two_tiles, 0)
 
     for copy in fetches:
         copy.wait()
@@ -747,13 +771,13 @@
         copy.wait_send()
 
 
-def layer(tokens, gain, side, taps, mats, out_att, out_conv):
+def layer(tokens, gain, att_gain, conv_gain, offset, taps, mats, out_att, out_conv):
     hbm = pl.BlockSpec(memory_space=pl.ANY)
     vmem = pl.BlockSpec(memory_space=pltpu.VMEM)
     dma = lambda *shape: pltpu.SemaphoreType.DMA(shape)
     return pl.pallas_call(
         layer_kernel,
-        in_specs=[hbm, vmem, vmem, vmem] + [hbm] * 8,
+        in_specs=[hbm] + [vmem] * 5 + [hbm] * 8,
         out_specs=[vmem, vmem],
         out_shape=[
             jax.ShapeDtypeStruct((1, HALF, D), BF16),
@@ -772,12 +796,9 @@
             pltpu.VMEM((BLOCKS * ROWS, 256), BF16),
             pltpu.VMEM((BLOCKS, HD, ROWS), BF16),
             pltpu.VMEM((BLOCKS // 2, ROWS, 256), BF16),
-            pltpu.VMEM((ROWS, ROWS), F32),
-            pltpu.VMEM((ROWS, ROWS), F32),
-            pltpu.VMEM((ROWS, ROWS), F32),
-            pltpu.VMEM((ROWS, ROWS), F32),
-            pltpu.VMEM((ROWS, ROWS), BF16),
-            pltpu.VMEM((ROWS, ROWS), BF16),
+            [pltpu.VMEM((ROWS, ROWS), F32)] * 4,
+            [pltpu.VMEM((ROWS, ROWS), F32)] * 4,
+            [pltpu.VMEM((ROWS, ROWS), BF16)] * 4,
             pltpu.VMEM((HD, ROWS), F32),
             pltpu.VMEM((BLOCKS, 96, 128), BF16),
             pltpu.VMEM((BLOCKS, 96, 128), BF16),
@@ -786,6 +807,7 @@
             pltpu.VMEM((2, 512, D), BF16),
             pltpu.VMEM((2, 512, D), BF16),
             pltpu.VMEM((2, HALF, 1024), BF16),
+            pltpu.VMEM((1, 1152), F32),
             pltpu.VMEM((2, 1, 1152), F32),
             dma(31),
             dma(3, 6), dma(3, 6),
@@ -806,7 +828,7 @@
             collective_id=0, has_side_effects=True, vmem_limit_bytes=58 << 20
         ),
         name="layer",
-    )(tokens, gain, side, taps, *mats, out_att, out_conv)
+    )(tokens, gain, att_gain, conv_gain, offset, taps, *mats, out_att, out_conv)
 
 
 def per_device(
@@ -825,11 +847,12 @@
     out_att,
     out_conv,
 ):
-    side = jnp.concatenate((att_gain, conv_gain, score_offset, jnp.zeros((120,), F32)))
     mixed, mass = layer(
         tokens[0],
         in_gain.reshape(1, D),
-        side.reshape(1, 1152),
+        att_gain.reshape(1, 512),
+        conv_gain.reshape(1, 512),
+        score_offset.reshape(1, 8),
         conv_taps,
         (w_query, w_key, w_value, w_outgate, w_ingate, w_conv_in),
         out_att,

time: 116 us -> 112 us (0.966)
  Pallas kernels: 110 us -> 107 us
  local copies, waits for them, and re-layouts: 4.77 us -> 3.4 us
    pallas_call x1, Pallas kernels: 110 us -> 107 us  [layer(): pl.pallas_call(layer_kernel, in_specs=[hbm] + [vmem] * 5 + [hbm] * 8, out...]
where the time goes in v6:
time: 112 us; the launch traced here: 111 us
  Pallas kernels  107 us (96%)
  local copies, waits for them, and re-layouts  3.4 us (3%)
    pallas_call x1, Pallas kernels, layer(): pl.pallas_call(layer_kernel, in_specs=[hbm] + [vmem] * 5 + [hbm] * 8, out...  107 us
    unnamed x2, local copies, waits for them, and re-layouts  3.4 us

profile of v6, /device:TPU:1, one launch (start us, length us, event | category | flops | bytes accessed | tf_op | source)
XLA Modules:
  0.0 111.3 jit_solution(6204700520854677168)
XLA Ops:
  0.6 107.2 %layer.1 = (bf16[1,192,2048]{2,1,0:T(8,128)(2,1)}, f32[1,8,384]{2,1,0:T(8,128)}) custom-call(bf16[384,1024]{1,0:T(8,128)(2,1)} %bitcast.6, f32[1,2048]{1,0:T(1,128)} %bitcast.8, f32[1,512]{1,0:T(1,128)} %bitcast.9, f32[1,512]{1,0:T(1,128)} %bitcast.10, f32[1,8]{1,0:T(1,128)} %bitcast.11, f32[3,512]{1,0:T(4,128)} %taps_ref.1, bf16[512,512]{1,0:T(8,128)(2,1)} %wq_ref.1, ...), custom_call_target="tpu_custom_call" | custom-call | tf_op jit(solution)/shard_map/layer/pallas_call | solution.py:778
  107.9 2.1 %copy.18 = bf16[1,192,2048]{2,1,0:T(8,128)(2,1)} copy(bf16[1,192,2048]{2,1,0:T(8,128)(2,1)} %get-tuple-element.8) | data formatting | bytes 1572864
  110.0 1.3 %copy.19 = f32[1,384,8]{1,2,0:T(8,128)} copy(f32[1,384,8]{1,2,0:T(8,128)} %bitcast.7) | data formatting | bytes 24576

commit v7 on v6

--- a/solution.py
+++ b/solution.py
@@ -194,6 +194,8 @@
     side_out.start()
     own_tokens.wait()
     top, bottom = pl.ds(0, HALF), pl.ds(HALF, HALF)
+    quarters = [pl.ds(96 * i, 96) for i in range(4)]
+    odd = lax.rem(y + z, 2)
 
     def hop(slot, f, rows, by):
         piece = tok.at[f, core, rows]
@@ -203,12 +205,19 @@
         piece = tok.at[f, core, rows]
         return remote(piece, piece, pair_send.at[slot], pair_recv.at[slot], sibling)
 
-    right_a, right_b = hop(0, x, top, 1), hop(1, x, bottom, 1)
-    left_b, left_a = hop(2, x, bottom, -1), hop(3, x, top, -1)
+    right_a, left_b = hop(0, x, top, 1), hop(2, x, bottom, -1)
+    right_next, right_last = hop(1, x, quarters[2], 1), hop(6, x, quarters[3], 1)
+    left_next, left_last = hop(3, x, quarters[1], -1), hop(7, x, quarters[0], -1)
     before, after, across = mod4(x - 1), mod4(x + 1), mod4(x + 2)
     on_right, on_left = hop(4, before, top, 1), hop(5, after, bottom, -1)
-    for copy in (right_a, left_b, right_b, left_a):
+    for copy in (right_a, left_b, right_next, left_next):
         copy.start()
+
+    @pl.when(odd == 0)
+    def _():
+        right_last.start()
+        left_last.start()
+
     pairs = [
         pair(0, x, top),
         pair(1, x, bottom),
@@ -271,9 +280,19 @@
         far(*kind).start()
     right_a.wait_recv()
     on_right.start()
+
+    @pl.when(odd == 1)
+    def _():
+        right_last.start()
+
     pairs[2].start()
     left_b.wait_recv()
     on_left.start()
+
+    @pl.when(odd == 1)
+    def _():
+        left_last.start()
+
     pairs[3].start()
     for kind in kinds:
         far(*kind).wait_recv()
@@ -316,35 +335,48 @@
         ), lax.abs(s - x) + lax.abs(half - core)
 
     def step(i, _):
-        s = mod4(x + i + lax.div(i, 2) - 2 * lax.div(i, 3))
+        usual = i + lax.div(i, 2) - 2 * lax.div(i, 3)
+        other = lax.rem(2 * i, 3) + 3 * lax.div(i, 3)
+        s = mod4(x + (1 - odd) * usual + odd * other)
 
         @pl.when(i == 0)
         def _():
             pairs[0].wait_recv()
             pairs[1].wait_recv()
 
-        @pl.when(i == 1)
-        def _():
-            right_b.wait_recv()
+        @pl.when(i == 1 + odd)
+        def _():
+            right_next.wait_recv()
+            right_last.wait_recv()
             pairs[4].start()
-            left_a.wait_recv()
+            left_next.wait_recv()
+            left_last.wait_recv()
             pairs[5].start()
-            pairs[3].wait_recv()
-            pairs[5].wait_recv()
-
-        @pl.when(i == 2)
-        def _():
-            pairs[2].wait_recv()
-            pairs[4].wait_recv()
-
-        @pl.when(i == 3)
+
+        @pl.when(i == 3 - 2 * odd)
         def _():
             on_right.wait_recv()
             pairs[6].start()
             on_left.wait_recv()
             pairs[7].start()
+
+        @pl.when(i == 3)
+        def _():
             for copy in others + fetches:
                 copy.start()
+
+        @pl.when(i == 1 + odd)
+        def _():
+            pairs[3].wait_recv()
+            pairs[5].wait_recv()
+
+        @pl.when(i == 2 + odd)
+        def _():
+            pairs[2].wait_recv()
+            pairs[4].wait_recv()
+
+        @pl.when(i == 3 - 2 * odd)
+        def _():
             pairs[6].wait_recv()
             pairs[7].wait_recv()
 
@@ -733,7 +765,7 @@
     for kind in kinds:
         far(*kind).wait_send()
         onward(*kind).wait_send()
-    for copy in [right_a, right_b, left_a, left_b, on_right, on_left] + pairs:
+    for copy in [right_a, right_next, right_last, left_b, left_next, left_last, on_right, on_left] + pairs:
         copy.wait_send()
 
     def left_here(at, _):
@@ -814,7 +846,7 @@
             dma(18), dma(18),
             dma(12), dma(12),
             dma(12), dma(12),
-            dma(6), dma(6),
+            dma(8), dma(8),
             dma(8), dma(8),
             dma(16), dma(16),
             dma(16), dma(16),

time: 112 us -> 109 us (0.973)
  Pallas kernels: 107 us -> 105 us
    pallas_call x1, Pallas kernels: 107 us -> 105 us  [layer(): pl.pallas_call(layer_kernel, in_specs=[hbm] + [vmem] * 5 + [hbm] * 8, out...]
where the time goes in v7:
time: 109 us
  Pallas kernels  105 us (96%)
  local copies, waits for them, and re-layouts  3.4 us (3%)
    pallas_call x1, Pallas kernels, layer(): pl.pallas_call(layer_kernel, in_specs=[hbm] + [vmem] * 5 + [hbm] * 8, out...  105 us
    unnamed x2, local copies, waits for them, and re-layouts  3.4 us

profile of v7, /device:TPU:1, one launch (start us, length us, event | category | flops | bytes accessed | tf_op | source)
XLA Modules:
  0.0 108.6 jit_solution(13030411211915343347)
XLA Ops:
  0.6 104.6 %layer.1 = (bf16[1,192,2048]{2,1,0:T(8,128)(2,1)}, f32[1,8,384]{2,1,0:T(8,128)}) custom-call(bf16[384,1024]{1,0:T(8,128)(2,1)} %bitcast.6, f32[1,2048]{1,0:T(1,128)} %bitcast.8, f32[1,512]{1,0:T(1,128)} %bitcast.9, f32[1,512]{1,0:T(1,128)} %bitcast.10, f32[1,8]{1,0:T(1,128)} %bitcast.11, f32[3,512]{1,0:T(4,128)} %taps_ref.1, bf16[512,512]{1,0:T(8,128)(2,1)} %wq_ref.1, ...), custom_call_target="tpu_custom_call" | custom-call | tf_op jit(solution)/shard_map/layer/pallas_call | solution.py:810
  105.3 2.1 %copy.18 = bf16[1,192,2048]{2,1,0:T(8,128)(2,1)} copy(bf16[1,192,2048]{2,1,0:T(8,128)(2,1)} %get-tuple-element.8) | data formatting | bytes 1572864
  107.3 1.3 %copy.19 = f32[1,384,8]{1,2,0:T(8,128)} copy(f32[1,384,8]{1,2,0:T(8,128)} %bitcast.7) | data formatting | bytes 24576

commit v8 on v7

--- a/solution.py
+++ b/solution.py
@@ -360,11 +360,6 @@
             on_left.wait_recv()
             pairs[7].start()
 
-        @pl.when(i == 3)
-        def _():
-            for copy in others + fetches:
-                copy.start()
-
         @pl.when(i == 1 + odd)
         def _():
             pairs[3].wait_recv()
@@ -521,6 +516,8 @@
         return 0
 
     lax.fori_loop(2, BLOCKS, arrive_and_use, 0)
+    for copy in others + fetches:
+        copy.start()
     use(BLOCKS - 2)
     use(BLOCKS - 1)
 
@@ -550,10 +547,14 @@
     def fold(w_ref, block):
         total[...] += dot(values[block], w_ref[...])
 
-    def decay(z_ref, d_ref, ahead):
-        run = jnp.zeros((8, ROWS), F32)
+    def decay(z_ref, d_ref, ahead, last_block):
+        skip = 128 if last_block else 0
+        if last_block:
+            ahead = ahead[:, skip:]
+            d_ref[:, 0:skip] = jnp.zeros((ROWS, skip), F32)
+        run = jnp.zeros((8, ROWS - skip), F32)
         for r in reversed(range(48)):
-            z = z_ref[8 * r : 8 * r + 8, :]
+            z = z_ref[8 * r : 8 * r + 8, skip:]
             soft = jnp.maximum(z, lax.log2(1.0 + jnp.exp2(jnp.minimum(z, 126.0))))
             if ahead is not None:
                 valid = ahead > r
@@ -562,7 +563,9 @@
             value = jnp.exp2(z - run)
             if ahead is not None:
                 value = jnp.where(valid, value, 0.0)
-            d_ref[8 * r : 8 * r + 8, :] = value
+            d_ref[8 * r : 8 * r + 8, skip:] = value
+        if last_block:
+            run = jnp.concatenate((jnp.zeros((8, skip), F32), run), axis=1)
         return run
 
     def weigh(d_ref, w_ref, run, carry):
@@ -590,7 +593,7 @@
             carry = weigh(decays[3], weights[3], run, carry)
         for i in range(count):
             slot = slots[i]
-            run = decay(scores[i], decays[slot], aheads[i])
+            run = decay(scores[i], decays[slot], aheads[i], i == 0 and aheads[0] is not None)
             if i > 0:
                 fold(weights[slots[i - 1]], top - i + 1)
             elif aheads[0] is None:

time: 109 us -> 109 us (level)
  no operation moved by 1% of the time
where the time goes in v8:
time: 109 us; the launch traced here: 108 us
  Pallas kernels  104 us (95%)
  local copies, waits for them, and re-layouts  3.4 us (3%)
    pallas_call x1, Pallas kernels, layer(): pl.pallas_call(layer_kernel, in_specs=[hbm] + [vmem] * 5 + [hbm] * 8, out...  104 us
    unnamed x2, local copies, waits for them, and re-layouts  3.4 us

profile of v8, /device:TPU:1, one launch (start us, length us, event | category | flops | bytes accessed | tf_op | source)
XLA Modules:
  0.0 108.4 jit_solution(5151644326222845178)
XLA Ops:
  0.6 104.3 %layer.1 = (bf16[1,192,2048]{2,1,0:T(8,128)(2,1)}, f32[1,8,384]{2,1,0:T(8,128)}) custom-call(bf16[384,1024]{1,0:T(8,128)(2,1)} %bitcast.6, f32[1,2048]{1,0:T(1,128)} %bitcast.8, f32[1,512]{1,0:T(1,128)} %bitcast.9, f32[1,512]{1,0:T(1,128)} %bitcast.10, f32[1,8]{1,0:T(1,128)} %bitcast.11, f32[3,512]{1,0:T(4,128)} %taps_ref.1, bf16[512,512]{1,0:T(8,128)(2,1)} %wq_ref.1, ...), custom_call_target="tpu_custom_call" | custom-call | tf_op jit(solution)/shard_map/layer/pallas_call | solution.py:813
  105.0 2.1 %copy.18 = bf16[1,192,2048]{2,1,0:T(8,128)(2,1)} copy(bf16[1,192,2048]{2,1,0:T(8,128)(2,1)} %get-tuple-element.8) | data formatting | bytes 1572864
  107.0 1.3 %copy.19 = f32[1,384,8]{1,2,0:T(8,128)} copy(f32[1,384,8]{1,2,0:T(8,128)} %bitcast.7) | data formatting | bytes 24576

commit v9 on v8

--- a/solution.py
+++ b/solution.py
@@ -231,10 +231,6 @@
     pairs[0].start()
     pairs[1].start()
 
-    for k in range(1, 4):
-        for m in range(6):
-            spread(k, m).wait_recv()
-
     my_rows = pl.ds(pl.multiple_of(y * 32, 32), 32)
 
     def near(k, i, way):
@@ -244,14 +240,13 @@
         at = (3 * way + k - 1) * 3 + i - 1
         return remote(piece, piece, near_send.at[at], near_recv.at[at], there)
 
-    for k in range(1, 4):
-        for i in range(1, 4):
+    pieces = (3, 1, 2)
+    for i in pieces:
+        for m in range(6):
+            spread(4 - i, m).wait_recv()
+        for k in range(1, 4):
             for way in range(2):
                 near(k, i, way).start()
-    for k in range(1, 4):
-        for i in range(1, 4):
-            for way in range(2):
-                near(k, i, way).wait_recv()
 
     def far(by, i, way):
         f = mod4(x + i)
@@ -275,9 +270,14 @@
         at = (2 * way + (by + 1) // 2) * 3 + i - 1
         return remote(piece, piece, pass_send.at[at], pass_recv.at[at], there)
 
-    kinds = [(by, i, way) for i in range(1, 4) for by in (1, -1) for way in range(2)]
-    for kind in kinds:
-        far(*kind).start()
+    kinds = [(by, i, way) for i in pieces for by in (1, -1) for way in range(2)]
+    for i in pieces:
+        for k in range(1, 4):
+            for way in range(2):
+                near(k, i, way).wait_recv()
+        for by in (1, -1):
+            for way in range(2):
+                far(by, i, way).start()
     right_a.wait_recv()
     on_right.start()
 

time: 109 us -> 108 us (level)
  no operation moved by 1% of the time
where the time goes in v9:
time: 108 us
  Pallas kernels  104 us (96%)
  local copies, waits for them, and re-layouts  3.4 us (3%)
    pallas_call x1, Pallas kernels, layer(): pl.pallas_call(layer_kernel, in_specs=[hbm] + [vmem] * 5 + [hbm] * 8, out...  104 us
    unnamed x2, local copies, waits for them, and re-layouts  3.4 us

profile of v9, /device:TPU:1, one launch (start us, length us, event | category | flops | bytes accessed | tf_op | source)
XLA Modules:
  0.0 107.6 jit_solution(7194333690236431188)
XLA Ops:
  0.6 103.6 %layer.1 = (bf16[1,192,2048]{2,1,0:T(8,128)(2,1)}, f32[1,8,384]{2,1,0:T(8,128)}) custom-call(bf16[384,1024]{1,0:T(8,128)(2,1)} %bitcast.6, f32[1,2048]{1,0:T(1,128)} %bitcast.8, f32[1,512]{1,0:T(1,128)} %bitcast.9, f32[1,512]{1,0:T(1,128)} %bitcast.10, f32[1,8]{1,0:T(1,128)} %bitcast.11, f32[3,512]{1,0:T(4,128)} %taps_ref.1, bf16[512,512]{1,0:T(8,128)(2,1)} %wq_ref.1, ...), custom_call_target="tpu_custom_call" | custom-call | tf_op jit(solution)/shard_map/layer/pallas_call | solution.py:813
  104.2 2.1 %copy.18 = bf16[1,192,2048]{2,1,0:T(8,128)(2,1)} copy(bf16[1,192,2048]{2,1,0:T(8,128)(2,1)} %get-tuple-element.8) | data formatting | bytes 1572864
  106.3 1.3 %copy.19 = f32[1,384,8]{1,2,0:T(8,128)} copy(f32[1,384,8]{1,2,0:T(8,128)} %bitcast.7) | data formatting | bytes 24576

commit v10 on v9

--- a/solution.py
+++ b/solution.py
@@ -448,6 +448,18 @@
 
     lax.fori_loop(0, SEQS, convolve, 0)
 
+    for k in range(1, 4):
+        for m in range(6):
+            spread(k, m).wait_send()
+        for i in range(1, 4):
+            for way in range(2):
+                near(k, i, way).wait_send()
+    for kind in kinds:
+        far(*kind).wait_send()
+        onward(*kind).wait_send()
+    for copy in [right_a, right_next, right_last, left_b, left_next, left_last, on_right, on_left] + pairs:
+        copy.wait_send()
+
     def to_mate(block):
         return remote(
             recv.at[block, 0:HALF], mate.at[block], mate_send.at[block], mate_recv.at[block], sibling
@@ -758,18 +770,6 @@
 
     lax.fori_loop(0, BLOCKS, left, 0)
 
-
-    for k in range(1, 4):
-        for m in range(6):
-            spread(k, m).wait_send()
-        for i in range(1, 4):
-            for way in range(2):
-                near(k, i, way).wait_send()
-    for kind in kinds:
-        far(*kind).wait_send()
-        onward(*kind).wait_send()
-    for copy in [right_a, right_next, right_last, left_b, left_next, left_last, on_right, on_left] + pairs:
-        copy.wait_send()
 
     def left_here(at, _):
         s = lax.div(at, 4)

time: 108 us -> 108 us (level)
  no operation moved by 1% of the time
where the time goes in v10:
time: 108 us
  Pallas kernels  104 us (96%)
  local copies, waits for them, and re-layouts  3.4 us (3%)
    pallas_call x1, Pallas kernels, layer(): pl.pallas_call(layer_kernel, in_specs=[hbm] + [vmem] * 5 + [hbm] * 8, out...  104 us
    unnamed x2, local copies, waits for them, and re-layouts  3.4 us

profile of v10, /device:TPU:1, one launch (start us, length us, event | category | flops | bytes accessed | tf_op | source)
XLA Modules:
  0.0 107.6 jit_solution(9646190054272428362)
XLA Ops:
  0.6 103.6 %layer.1 = (bf16[1,192,2048]{2,1,0:T(8,128)(2,1)}, f32[1,8,384]{2,1,0:T(8,128)}) custom-call(bf16[384,1024]{1,0:T(8,128)(2,1)} %bitcast.6, f32[1,2048]{1,0:T(1,128)} %bitcast.8, f32[1,512]{1,0:T(1,128)} %bitcast.9, f32[1,512]{1,0:T(1,128)} %bitcast.10, f32[1,8]{1,0:T(1,128)} %bitcast.11, f32[3,512]{1,0:T(4,128)} %taps_ref.1, bf16[512,512]{1,0:T(8,128)(2,1)} %wq_ref.1, ...), custom_call_target="tpu_custom_call" | custom-call | tf_op jit(solution)/shard_map/layer/pallas_call | solution.py:813
  104.2 2.1 %copy.18 = bf16[1,192,2048]{2,1,0:T(8,128)(2,1)} copy(bf16[1,192,2048]{2,1,0:T(8,128)(2,1)} %get-tuple-element.8) | data formatting | bytes 1572864
  106.3 1.3 %copy.19 = f32[1,384,8]{1,2,0:T(8,128)} copy(f32[1,384,8]{1,2,0:T(8,128)} %bitcast.7) | data formatting | bytes 24576
